TPU v7x, 512 devices: a whole 4x8x8 slice. The times are simulated.
512 devices in a mesh: sp: 32 (over z, x), tp: 16 (over y, core).
Axes of the slice: x: 4, y: 8, z: 8, core: 2. Of those that a mesh axis runs over, the one named last changes fastest.
Arguments:
- cotangent: bfloat16 [4096, 2048], P('sp'), may hold values from -6 to 6
- mixer_out: bfloat16 [4096, 2048], P('sp'), may hold values from -6 to 6
- expert_ids: int32 [4096, 2], P('sp'), may hold values from 0 to 31, all different within a row; in each aligned block of 128 rows (0 to 127, 128 to 255, ...) at most 16 rows name the same one
- route_weight: float32 [4096, 2], P('sp'), may hold values from 0.3 to 1.5
- saved_normalized: bfloat16 [4096, 2048], P('sp', 'tp'), may hold values from -6 to 6
- inverse_deviation: float32 [4096], P('sp'), may hold values from 0.3 to 3
- channel_norm_gain: float32 [2048], P('tp'), may hold values from 0.1 to 1.9
- taps: float32 [31, 2048], P(None, 'tp'), may hold values from -1 to 1
- proj_weight: bfloat16 [2048, 2048], P('tp'), may hold values from -0.125 to 0.125
- gate_weight: bfloat16 [32, 2048, 2048], P('sp', None, 'tp'), may hold values from -0.125 to 0.125
- up_weight: bfloat16 [32, 2048, 2048], P('sp', None, 'tp'), may hold values from -0.125 to 0.125
- down_weight: bfloat16 [32, 2048, 2048], P('sp', 'tp'), may hold values from -0.125 to 0.125
Outputs:
- grad_mixer_in: bfloat16 [4096, 2048], P('sp', 'tp')
- grad_proj: float32 [2048, 2048], P('sp', 'tp')
- grad_gate: bfloat16 [32, 2048, 2048], P('sp', None, 'tp')
- grad_up: bfloat16 [32, 2048, 2048], P('sp', None, 'tp')
- grad_down: bfloat16 [32, 2048, 2048], P('sp', 'tp')
Inputs may be any that keep to these rules, and one draw needn't show every extreme that they name: `expert_ids`: each row names 2 different experts. Within the rows of one index of sp no expert is named more than 16 times, a bound that some block reaches.
All inputs are finite; a program needn't handle non-finite values.
Results may differ from a plain program's by a relative error of at most 0.02.
Values may be sent and summed in bfloat16 or wider, within the bound.
No kernel may reach another device: no remote copies, remote signals or barrier semaphores. Data moves between devices by JAX's collectives and lax.ppermute only.
A program may use at most 64 MiB of HBM per device.

v0:
```python
import jax
import jax.numpy as jnp
from jax import lax
from jax.sharding import PartitionSpec as P


def sent_together(arrays, axis, split_dim, concat_dim, along):
    both = jnp.concatenate(arrays, axis=along)
    filled, at, finished = (
        lax.all_to_all(both, axis, split_axis=split_dim, concat_axis=concat_dim, tiled=True),
        0,
        [],
    )
    for a in arrays:
        finished.append(lax.slice_in_dim(filled, at, at + a.shape[along], axis=along))
        at += a.shape[along]
    return tuple(finished)


def side_by_side(arrays, axis, dim, along):
    ends, at = ([], 0)
    for a in arrays[:-1]:
        at += a.shape[along]
        ends.append(at)
    both = jnp.concatenate(arrays, axis=along)
    return tuple(jnp.split(lax.all_gather(both, axis, axis=dim, tiled=True), ends, axis=along))


def in_blocks(value, dim, size):
    dims = value.shape
    pieces = value.reshape(*dims[:dim], size, dims[dim] // size, *dims[dim + 1 :])
    return jnp.moveaxis(pieces, dim, 0)


def sent_and_summed(value, axis, dim):
    pieces = in_blocks(value, dim, lax.axis_size(axis))
    arrived = lax.all_to_all(pieces, axis, split_axis=0, concat_axis=0, tiled=True)
    return arrived.astype(jnp.float32).sum(axis=0)


def sent_to_all(value, axis):
    size = lax.axis_size(axis)
    return lax.all_to_all(
        jnp.broadcast_to(value[None], (size, *value.shape)), axis, 0, 0, tiled=True
    )


def taken_together(value, axis):
    everything = sent_to_all(value, axis)
    return jnp.sum(everything, axis=0)


def packed_total(arrays, axis):
    ends = [0]
    for a in arrays:
        ends.append(ends[-1] + a.size)
    running = taken_together(jnp.concatenate([a.ravel() for a in arrays]), axis)
    return tuple((running[b:e].reshape(a.shape) for a, b, e in zip(arrays, ends, ends[1:])))


def from_behind(value, axis, steps):
    count = lax.axis_size(axis)
    leading, last = (max(0, -steps), min(count, count - steps))
    return lax.ppermute(value, axis, [(source, source + steps) for source in range(leading, last)])


def route_table(expert_ids, route_weight, slot_start, slot_span, capacity, experts):
    onehot = (expert_ids[:, :, None] == jnp.arange(experts, dtype=jnp.int32)[None, None, :]).astype(
        jnp.int32
    )
    flat_hot = onehot.reshape(-1, experts)
    ranks = jnp.cumsum(flat_hot, axis=0) - flat_hot
    rank_pair = jnp.sum(ranks * flat_hot, axis=1).reshape(expert_ids.shape)
    slot_index = expert_ids * capacity + rank_pair
    targets = (
        jnp.arange(experts, dtype=jnp.int32)[:, None] * capacity
        + slot_start
        + jnp.arange(slot_span, dtype=jnp.int32)[None, :]
    ).reshape(-1)
    matched = slot_index[None, :, :] == targets[:, None, None]
    dispatch = jnp.any(matched, axis=2).astype(jnp.bfloat16)
    slot_weight = jnp.sum(jnp.where(matched, route_weight[None, :, :], 0.0), axis=(1, 2))
    return (dispatch, slot_weight)


def shards(
    cotangent,
    mixer_out,
    expert_ids,
    route_weight,
    saved_normalized,
    inverse_deviation,
    channel_norm_gain,
    taps,
    proj_weight,
    gate_weight,
    up_weight,
    down_weight,
):
    experts = lax.axis_size("sp")
    groups = lax.axis_size("tp")
    tok_rows, model_width = cotangent.shape
    capacity = groups * max(1, 4 * tok_rows // (experts * groups))
    slot_span = capacity // groups
    slot_start = lax.axis_index("tp") * slot_span
    dispatch, slot_weight = route_table(
        expert_ids, route_weight, slot_start, slot_span, capacity, experts
    )
    sent_rows = jnp.dot(dispatch, mixer_out, preferred_element_type=jnp.float32).astype(
        jnp.bfloat16
    )
    sent_grad = (
        slot_weight[:, None] * jnp.dot(dispatch, cotangent, preferred_element_type=jnp.float32)
    ).astype(jnp.bfloat16)
    sent_rows = sent_rows.reshape(experts, slot_span, model_width)
    sent_grad = sent_grad.reshape(experts, slot_span, model_width)
    shared_rows = sent_together((sent_rows, sent_grad), "sp", 0, 0, 1)
    routed_rows, routed_grad = side_by_side((shared_rows[0], shared_rows[1]), "tp", 1, 0)
    full_table, unused_weight = route_table(
        expert_ids, route_weight, 0, capacity, capacity, experts
    )
    routed_rows = routed_rows.reshape(-1, model_width)
    routed_grad = routed_grad.reshape(-1, model_width)
    w_first = gate_weight[0]
    w_third = up_weight[0]
    w_second = down_weight[0]
    contract_last = (((1,), (1,)), ((), ()))
    contract_first = (((0,), (0,)), ((), ()))
    hidden_gate = jnp.dot(routed_rows, w_first, preferred_element_type=jnp.float32)
    hidden_up = jnp.dot(routed_rows, w_third, preferred_element_type=jnp.float32)
    sigma = jax.nn.sigmoid(hidden_gate)
    swish = hidden_gate * sigma
    activ = (swish * hidden_up).astype(jnp.bfloat16)
    grad_second = lax.dot_general(
        activ, routed_grad, contract_first, preferred_element_type=jnp.float32
    ).astype(jnp.bfloat16)
    grad_activ = lax.dot_general(
        routed_grad, w_second, contract_last, preferred_element_type=jnp.float32
    )
    grad_gpre = (grad_activ * hidden_up * sigma * (1.0 + hidden_gate * (1.0 - sigma))).astype(
        jnp.bfloat16
    )
    grad_upre = (grad_activ * swish).astype(jnp.bfloat16)
    grad_first = lax.dot_general(
        routed_rows, grad_gpre, contract_first, preferred_element_type=jnp.float32
    ).astype(jnp.bfloat16)
    grad_third = lax.dot_general(
        routed_rows, grad_upre, contract_first, preferred_element_type=jnp.float32
    ).astype(jnp.bfloat16)
    partial_value = lax.dot_general(
        grad_gpre, w_first, contract_last, preferred_element_type=jnp.float32
    ) + lax.dot_general(grad_upre, w_third, contract_last, preferred_element_type=jnp.float32)
    scattered = sent_and_summed(partial_value.astype(jnp.bfloat16), "tp", 1).astype(jnp.bfloat16)
    home_parts = lax.all_to_all(
        scattered.reshape(experts, capacity, -1), "sp", split_axis=0, concat_axis=0, tiled=True
    )
    home_rows = lax.all_gather(home_parts, "tp", axis=2, tiled=True)
    returned = lax.dot_general(
        full_table,
        home_rows.reshape(-1, model_width),
        contract_first,
        preferred_element_type=jnp.float32,
    )
    mixer_grad = (cotangent.astype(jnp.float32) + returned).astype(jnp.bfloat16)
    normalized_input = saved_normalized.astype(jnp.float32)
    normalized_values = normalized_input * channel_norm_gain[None, :]
    gate_sig = jax.nn.sigmoid(normalized_values)
    act_conv = (normalized_values * gate_sig).astype(jnp.bfloat16)
    grad_proj = sent_and_summed(
        lax.dot_general(
            mixer_grad, act_conv, contract_first, preferred_element_type=jnp.float32
        ).astype(jnp.bfloat16),
        "sp",
        0,
    )
    grad_act = lax.dot_general(
        mixer_grad, proj_weight, contract_last, preferred_element_type=jnp.float32
    )
    norm_output_gradient = (
        grad_act
        * gate_sig
        * (1.0 + normalized_values * (1.0 - gate_sig))
        * channel_norm_gain[None, :]
    )
    reduced_totals = packed_total(
        (
            jnp.sum(norm_output_gradient, axis=1),
            jnp.sum(norm_output_gradient * normalized_input, axis=1),
        ),
        "tp",
    )
    channel_count = saved_normalized.shape[1] * groups
    conv_output_gradient = inverse_deviation[:, None] * (
        norm_output_gradient
        - reduced_totals[0][:, None] / channel_count
        - normalized_input * (reduced_totals[1][:, None] / channel_count)
    )
    reach = taps.shape[0] - 1
    beyond = from_behind(conv_output_gradient[:reach], "sp", -1)
    extended = jnp.concatenate([conv_output_gradient, beyond], axis=0)
    result = jnp.zeros_like(conv_output_gradient)
    for tap_index in range(taps.shape[0]):
        result = result + taps[tap_index][None, :] * extended[tap_index : tap_index + tok_rows]
    return (
        result.astype(jnp.bfloat16),
        grad_proj,
        grad_first[None],
        grad_third[None],
        grad_second[None],
    )


def solution(mesh):
    return jax.shard_map(
        shards,
        mesh=mesh,
        in_specs=(
            P("sp", None),
            P("sp", None),
            P("sp", None),
            P("sp", None),
            P("sp", "tp"),
            P("sp"),
            P("tp"),
            P(None, "tp"),
            P("tp", None),
            P("sp", None, "tp"),
            P("sp", None, "tp"),
            P("sp", "tp", None),
        ),
        out_specs=(
            P("sp", "tp"),
            P("sp", "tp"),
            P("sp", None, "tp"),
            P("sp", None, "tp"),
            P("sp", "tp", None),
        ),
        check_vma=False,
    )
```

profile of v0, /device:TPU:1, one launch (start us, length us, event | category | flops | bytes accessed | tf_op | source)
XLA Modules:
  0.0 256.7 jit_solution(6382690411300353336)
XLA Ops:
  11.6 1.2 fusion.5
  12.9 1.2 fusion.6
  14.5 24.8 %all_to_all.26 = bf16[32,2,2048]{2,1,0:T(2,128)(2,1)S(1)} all-to-all(bf16[32,2,2048]{2,1,0:T(2,128)(2,1)S(1)} %copy.68), channel_id=1, replica_groups=mesh['sp'=32,'tp'=16] {'sp'}, dimensions={0} | all-to-all | bytes 524288 | tf_op jit(solution)/shard_map/all_to_all | solution.py:10
  41.3 42.1 %all-gather.3.cloned.1.call-done = bf16[64,16,2048]{2,0,1:T(8,128)(2,1)} async-done(((bf16[64,1,2048]{2,0,1:T(8,128)(2,1)}), bf16[64,16,2048]{2,0,1:T(8,128)(2,1)}) %all-gather.3.cloned.1.call-update) | async-done | bytes 4194320 | tf_op jit(solution)/shard_map/all_gather | solution.py:26
  83.4 2.7 %fusion.133 = (bf16[32,16,2048]{2,0,1:T(8,128)(2,1)S(1)}, bf16[32,16,2048]{2,0,1:T(8,128)(2,1)S(1)}) fusion(bf16[64,16,2048]{2,0,1:T(8,128)(2,1)} %all-gather.3.cloned.1.call-done), kind=kLoop, calls=%fused_computation.256 | loop fusion | bytes 8388608 | tf_op jit(solution)/shard_map/split | solution.py:26
  86.1 1.2 copy.75
  93.3 55.3 %all_to_all.27 = bf16[16,512,128]{2,1,0:T(8,128)(2,1)} all-to-all(bf16[16,512,128]{2,1,0:T(8,128)(2,1)S(1)} %bitcast.144), channel_id=1, replica_groups=mesh['sp'=32,'tp'=16] {'tp'}, dimensions={0} | all-to-all | bytes 4194304 | tf_op jit(solution)/shard_map/all_to_all | solution.py:37
  148.5 2.6 reduce_sum.72
  151.1 20.5 %all_to_all.28 = bf16[32,16,128]{2,1,0:T(8,128)(2,1)} all-to-all(bf16[32,16,128]{2,1,0:T(8,128)(2,1)} %bitcast.146), channel_id=1, replica_groups=mesh['sp'=32,'tp'=16] {'sp'}, dimensions={0} | all-to-all | bytes 262144 | tf_op jit(solution)/shard_map/all_to_all | solution.py:154
  172.4 1.5 compare_reduce_fusion
  173.9 1.6 slice_bitcast_fusion.29
  175.4 1.6 slice_bitcast_fusion.30
  177.1 3.0 %fusion.3 = bf16[1,128,2048]{2,1,0:T(8,128)(2,1)} fusion(bf16[512,2048]{1,0:T(8,128)(2,1)} %bitcast.143, f32[512,128]{1,0:T(8,128)} %copy-done.5, f32[512,128]{1,0:T(8,128)S(1)} %fusion.12), kind=kOutput, calls=%fused_computation.9 | convolution fusion | flops 269090816 | bytes 3145728 | tf_op jit(solution)/shard_map/dot_general | solution.py:134
  180.1 26.1 %all-gather.5.cloned.1.call-done = bf16[32,16,2048]{2,1,0:T(8,128)(2,1)} async-done(((bf16[32,16,128]{2,1,0:T(8,128)(2,1)}), bf16[32,16,2048]{2,1,0:T(8,128)(2,1)}) %all-gather.5.cloned.1.call-update) | async-done | bytes 2097168 | tf_op jit(solution)/shard_map/all_gather | solution.py:157
  206.2 2.2 fusion
  210.2 5.1 %all-to-all-start.3 = ((f32[16,1,256]{2,1,0:T(1,128)}), f32[16,1,256]{2,1,0:T(1,128)S(1)}, u32[]{:S(2)}, u32[]{:S(2)}) async-start(f32[16,1,256]{2,1,0:T(1,128)} %broadcast_in_dim.22), calls=%async_computation.3 | async-start | bytes 32768 | tf_op jit(solution)/shard_map/all_to_all | solution.py:43
  215.3 2.2 convolution_convert_fusion.3
  217.5 5.2 %all-to-all-done.3 = f32[16,1,256]{2,1,0:T(1,128)S(1)} async-done(((f32[16,1,256]{2,1,0:T(1,128)}), f32[16,1,256]{2,1,0:T(1,128)S(1)}, u32[]{:S(2)}, u32[]{:S(2)}) %all-to-all-start.3) | async-done | bytes 16416 | tf_op jit(solution)/shard_map/all_to_all | solution.py:43
  222.7 9.9 %all-to-all-start.4 = ((bf16[32,64,128]{2,1,0:T(8,128)(2,1)}), bf16[32,64,128]{2,1,0:T(8,128)(2,1)S(1)}, u32[]{:S(2)}, u32[]{:S(2)}) async-start(bf16[32,64,128]{2,1,0:T(8,128)(2,1)} %bitcast.42), calls=%async_computation.4 | async-start | bytes 1048576 | tf_op jit(solution)/shard_map/all_to_all | solution.py:37
  232.6 1.6 fusion.2
  234.6 1.3 collective-permute-start
  235.9 1.6 fusion.1
  237.5 2.3 collective-permute-done
  240.9 8.3 %all-to-all-done.4 = bf16[32,64,128]{2,1,0:T(8,128)(2,1)S(1)} async-done(((bf16[32,64,128]{2,1,0:T(8,128)(2,1)}), bf16[32,64,128]{2,1,0:T(8,128)(2,1)S(1)}, u32[]{:S(2)}, u32[]{:S(2)}) %all-to-all-start.4) | async-done | bytes 524320 | tf_op jit(solution)/shard_map/all_to_all | solution.py:37
  (125 shorter events, 17.0 us)
Async XLA Ops:
  7.2 81.3 %copy-start = (bf16[1,2048,128]{2,1,0:T(8,128)(2,1)S(1)}, bf16[1,2048,128]{2,1,0:T(8,128)(2,1)}, u32[]{:S(2)}) copy-start(bf16[1,2048,128]{2,1,0:T(8,128)(2,1)} %param.21) | copy-start | bytes 1572868
  7.2 76.2 %all-gather.3.cloned.1.call-start = ((), (), s32[]{:S(2)}) async-start(), calls=%async_computation.5 | async-start | bytes 4456448 | tf_op jit(solution)/shard_map/all_gather | solution.py:26
  41.2 165.0 %all-gather.5.cloned.1.call-start = ((), (), s32[]{:S(2)}) async-start(), calls=%async_computation.6 | async-start | bytes 2228224 | tf_op jit(solution)/shard_map/all_gather | solution.py:157
  151.1 55.1 %copy-start.2 = (bf16[128,2048]{1,0:T(8,128)(2,1)S(1)}, bf16[128,2048]{1,0:T(8,128)(2,1)}, u32[]{:S(2)}) copy-start(bf16[128,2048]{1,0:T(8,128)(2,1)} %param.12) | copy-start | bytes 1572868
  180.1 29.1 %copy-start.8 = (bf16[128,128]{1,0:T(8,128)(2,1)S(1)}, bf16[128,128]{1,0:T(8,128)(2,1)}, u32[]{:S(2)}) copy-start(bf16[128,128]{1,0:T(8,128)(2,1)} %param.16) | copy-start | bytes 98308
  180.1 29.1 %copy-start.37 = (f32[128]{0:T(128)S(1)}, f32[128]{0:T(128)}, u32[]{:S(2)}) copy-start(f32[128]{0:T(128)} %param.18) | copy-start | bytes 1540
  209.2 23.4 %copy-start.7 = (bf16[512,128]{1,0:T(8,128)(2,1)S(1)}, bf16[512,128]{1,0:T(8,128)(2,1)}, u32[]{:S(2)}) copy-start(bf16[512,128]{1,0:T(8,128)(2,1)} %copy-done.6) | copy-start | bytes 393220
  210.2 12.5 %all-to-all-start.3 = ((f32[16,1,256]{2,1,0:T(1,128)}), f32[16,1,256]{2,1,0:T(1,128)S(1)}, u32[]{:S(2)}, u32[]{:S(2)}) async-start(f32[16,1,256]{2,1,0:T(1,128)} %broadcast_in_dim.22), calls=%async_computation.3 | async-start | bytes 32768 | tf_op jit(solution)/shard_map/all_to_all | solution.py:43
  222.7 26.5 %all-to-all-start.4 = ((bf16[32,64,128]{2,1,0:T(8,128)(2,1)}), bf16[32,64,128]{2,1,0:T(8,128)(2,1)S(1)}, u32[]{:S(2)}, u32[]{:S(2)}) async-start(bf16[32,64,128]{2,1,0:T(8,128)(2,1)} %bitcast.42), calls=%async_computation.4 | async-start | bytes 1048576 | tf_op jit(solution)/shard_map/all_to_all | solution.py:37
  234.3 5.4 %copy-start.10 = (f32[128]{0:T(128)S(1)}, f32[128]{0:T(128)}, u32[]{:S(2)}) copy-start(f32[128]{0:T(128)} %get-tuple-element.36) | copy-start | bytes 1540
  234.3 5.4 %copy-start.11 = (f32[128]{0:T(128)S(1)}, f32[128]{0:T(128)}, u32[]{:S(2)}) copy-start(f32[128]{0:T(128)} %get-tuple-element.37) | copy-start | bytes 1540
  234.4 5.4 %copy-start.12 = (f32[128]{0:T(128)S(1)}, f32[128]{0:T(128)}, u32[]{:S(2)}) copy-start(f32[128]{0:T(128)} %get-tuple-element.38) | copy-start | bytes 1540
  234.4 5.4 %copy-start.13 = (f32[128]{0:T(128)S(1)}, f32[128]{0:T(128)}, u32[]{:S(2)}) copy-start(f32[128]{0:T(128)} %get-tuple-element.39) | copy-start | bytes 1540
  234.4 5.4 %copy-start.14 = (f32[128]{0:T(128)S(1)}, f32[128]{0:T(128)}, u32[]{:S(2)}) copy-start(f32[128]{0:T(128)} %get-tuple-element.40) | copy-start | bytes 1540
  234.4 5.4 %copy-start.15 = (f32[128]{0:T(128)S(1)}, f32[128]{0:T(128)}, u32[]{:S(2)}) copy-start(f32[128]{0:T(128)} %get-tuple-element.41) | copy-start | bytes 1540
  234.4 5.4 %copy-start.16 = (f32[128]{0:T(128)S(1)}, f32[128]{0:T(128)}, u32[]{:S(2)}) copy-start(f32[128]{0:T(128)} %get-tuple-element.42) | copy-start | bytes 1540
  234.4 5.4 %copy-start.17 = (f32[128]{0:T(128)S(1)}, f32[128]{0:T(128)}, u32[]{:S(2)}) copy-start(f32[128]{0:T(128)} %get-tuple-element.43) | copy-start | bytes 1540
  234.4 5.4 %copy-start.18 = (f32[128]{0:T(128)S(1)}, f32[128]{0:T(128)}, u32[]{:S(2)}) copy-start(f32[128]{0:T(128)} %get-tuple-element.13) | copy-start | bytes 1540
  234.4 5.4 %copy-start.19 = (f32[128]{0:T(128)S(1)}, f32[128]{0:T(128)}, u32[]{:S(2)}) copy-start(f32[128]{0:T(128)} %get-tuple-element.14) | copy-start | bytes 1540
  234.4 5.4 %copy-start.20 = (f32[128]{0:T(128)S(1)}, f32[128]{0:T(128)}, u32[]{:S(2)}) copy-start(f32[128]{0:T(128)} %get-tuple-element.15) | copy-start | bytes 1540
  234.4 5.4 %copy-start.21 = (f32[128]{0:T(128)S(1)}, f32[128]{0:T(128)}, u32[]{:S(2)}) copy-start(f32[128]{0:T(128)} %get-tuple-element.16) | copy-start | bytes 1540
  234.5 5.4 %copy-start.22 = (f32[128]{0:T(128)S(1)}, f32[128]{0:T(128)}, u32[]{:S(2)}) copy-start(f32[128]{0:T(128)} %get-tuple-element.17) | copy-start | bytes 1540
  234.5 5.4 %copy-start.23 = (f32[128]{0:T(128)S(1)}, f32[128]{0:T(128)}, u32[]{:S(2)}) copy-start(f32[128]{0:T(128)} %get-tuple-element.18) | copy-start | bytes 1540
  234.6 5.2 %collective-permute-start = (f32[30,128]{1,0:T(8,128)S(1)}, f32[30,128]{1,0:T(8,128)S(1)}, u32[]{:S(2)}, u32[]{:S(2)}) collective-permute-start(f32[30,128]{1,0:T(8,128)S(1)} %slice.275), channel_id=1, source_target_pairs={{16,0},{32,16},{48,32},{64,48},{80,64},{96,80},{112,96},{128,112},... | collective-permute-start | bytes 46088 | tf_op jit(solution)/shard_map/ppermute | solution.py:64
  (22 other events, 83.3 us)
Sparse Core Ops, SparseCore 0:
  41.3 42.0 all-gather.2
  171.8 34.3 all-gather.4
where the time goes:
time: 258 us; the launch traced here: 257 us
  blocking collectives  101 us (39%)
  waiting for transfers between devices  84 us (33%)
  matrix products  16.9 us (7%)
  starting transfers between devices  16.4 us (6%)
  local copies, waits for them, and re-layouts  15.1 us (6%)
  between operations  14.8 us (6%)
  other arithmetic  8.92 us (3%)
    all_to_all x1, blocking collectives, sent_and_summed(): lax.all_to_all(pieces, axis, split_axis=0, concat_axis=0, tiled=True)  55.3 us
    all_gather x1, waiting for transfers between devices, side_by_side(): lax.all_gather(both, axis, axis=dim, tiled=True)  42.1 us
    all_gather x1, waiting for transfers between devices, shards(): home_rows = lax.all_gather(home_parts, 'tp', axis=2, tiled=True)  26.1 us
    all_to_all x1, blocking collectives, sent_together(): lax.all_to_all(both, axis, split_axis=split_dim, concat_axis=concat_dim,...  24.8 us
    all_to_all x1, blocking collectives, shards(): lax.all_to_all(scattered.reshape(experts, capacity, -1), 'sp', split_axis...  20.5 us
    all_to_all x1, starting transfers between devices, sent_and_summed(): lax.all_to_all(pieces, axis, split_axis=0, concat_axis=0, tiled=True)  9.9 us
    all_to_all x1, waiting for transfers between devices, sent_and_summed(): lax.all_to_all(pieces, axis, split_axis=0, concat_axis=0, tiled=True)  8.31 us
    unnamed x85, local copies, waits for them, and re-layouts  5.2 us
  transfers between devices with their start and end apart: 5, of which 5 were waited for; matrix products, arithmetic and copies ran while one was open for 6% of the time, Pallas kernels for 0%

commit v1 on v0

v1 whole, which is shorter than its diff:
```python
import jax
import jax.numpy as jnp
from jax import lax
from jax.sharding import Mesh, PartitionSpec as P

BF, F32 = jnp.bfloat16, jnp.float32
SWAP = [(0, 1), (1, 0)]
LAST = (((1,), (1,)), ((), ()))
FIRST = (((0,), (0,)), ((), ()))


def mm(a, b, dims=(((1,), (0,)), ((), ()))):
    return lax.dot_general(a, b, dims, preferred_element_type=F32)


def flip_y(value, bit):
    return lax.ppermute(value, "y", [(i, i ^ bit) for i in range(lax.axis_size("y"))])


def flip_c(value):
    return lax.ppermute(value, "c", SWAP)


def shards(
    cotangent,
    mixer_out,
    expert_ids,
    route_weight,
    saved_normalized,
    inverse_deviation,
    channel_norm_gain,
    taps,
    proj_weight,
    gate_weight,
    up_weight,
    down_weight,
):
    sp = ("z", "x")
    experts = lax.axis_size(sp)
    ny = lax.axis_size("y")
    yi, ci = lax.axis_index("y"), lax.axis_index("c")
    tok, width = cotangent.shape
    span = 4
    group = (yi % 2) * 2 + ci
    own = (gate_weight[0], up_weight[0], down_weight[0])

    by_c = tuple(flip_c(w) for w in own)
    by_y = tuple(flip_y(w, 1) for w in own)
    by_yc = tuple(flip_c(w) for w in by_y)

    lane_e = jnp.arange(experts, dtype=jnp.int32)[None, :]
    hot = [(expert_ids[:, k : k + 1] == lane_e) for k in range(2)]
    both = (hot[0] | hot[1]).astype(BF)
    before = (
        jnp.arange(tok, dtype=jnp.int32)[:, None] > jnp.arange(tok, dtype=jnp.int32)[None, :]
    ).astype(BF)
    rank = mm(before, both)
    slot_of = jnp.where(both > 0, rank, -1.0)
    targets = group * span + jnp.arange(span, dtype=jnp.int32)
    picked = slot_of.T[:, None, :] == targets.astype(F32)[None, :, None]
    dispatch = picked.astype(BF).reshape(experts * span, tok)
    wte = sum(jnp.where(hot[k], route_weight[:, k : k + 1], 0.0) for k in range(2))
    slot_weight = jnp.sum(jnp.where(picked, wte.T[:, None, :], 0.0), axis=2)
    rows = mm(dispatch, mixer_out).astype(BF).reshape(experts, span, width)
    grads = (slot_weight.reshape(-1, 1) * mm(dispatch, cotangent)).astype(BF)
    sent = jnp.concatenate([rows, grads.reshape(experts, span, width)], axis=1)
    got = lax.all_to_all(sent, sp, 0, 0, tiled=True)
    x = got[:, :span].reshape(-1, width)
    g = got[:, span:].reshape(-1, width)

    col = jnp.arange(ny * 2 * span, dtype=jnp.int32)
    col_y, col_h, col_r = col // (2 * span), (col // span) % 2, col % span
    col_rank = ((col_y % 2) * 2 + ci) * span + col_r
    hit = (slot_of[:, :, None] == col_rank.astype(F32)[None, None, :])
    halves = jnp.stack([ci, 1 - ci])
    table = (hit[None] & (col_h[None, :] == halves[:, None])[:, None, None, :]).astype(BF)
    table = table.reshape(2 * tok, -1)

    hidden = []
    partial = jnp.zeros((x.shape[0], width), F32)
    for w1, w3, w2 in (own, by_c, by_y, by_yc):
        hg, hu = mm(x, w1), mm(x, w3)
        sigma = jax.nn.sigmoid(hg)
        swish = hg * sigma
        act = (swish * hu).astype(BF)
        gact = mm(g, w2, LAST)
        ghg = (gact * hu * sigma * (1.0 + hg * (1.0 - sigma))).astype(BF)
        ghu = (gact * swish).astype(BF)
        partial = partial + mm(ghg, w1, LAST) + mm(ghu, w3, LAST)
        hidden.append((act, ghg, ghu))
    back = partial.astype(BF).reshape(experts, span, ny, 2, 128)
    back = back.transpose(0, 2, 3, 1, 4).reshape(experts * ny, 2 * span, 128)
    home = lax.all_to_all(back, ("z", "x", "y"), 0, 0, tiled=True).reshape(-1, 128)

    def weight_grads(q):
        act, ghg, ghu = hidden[q]
        return mm(x, ghg, FIRST), mm(x, ghu, FIRST), mm(act, g, FIRST)

    mine, theirs_c, mine_y, theirs_yc = (weight_grads(q) for q in range(4))
    final = []
    for a, b, o, p in zip(mine, mine_y, theirs_c, theirs_yc):
        a = a + flip_c(o.astype(BF)).astype(F32)
        b = b + flip_c(p.astype(BF)).astype(F32)
        final.append((a + flip_y(b.astype(BF), 1).astype(F32)).astype(BF))

    combined = mm(table, home)
    other = flip_c(combined[tok:].astype(BF))
    feat = (yi * 2 + ci) * 128
    cot = lax.dynamic_slice_in_dim(cotangent, feat, 128, axis=1)
    mix = (cot.astype(F32) + combined[:tok] + other.astype(F32)).astype(BF)
    mine_all = lax.all_to_all(jnp.broadcast_to(mix[None], (ny, *mix.shape)), "y", 0, 0, tiled=True)
    other_all = flip_c(mine_all)
    first = jnp.where(ci == 0, mine_all, other_all)
    second = jnp.where(ci == 0, other_all, mine_all)
    mixer_grad = jnp.stack([first, second], axis=1).transpose(2, 0, 1, 3).reshape(tok, width)

    normalized = saved_normalized.astype(F32)
    values = normalized * channel_norm_gain[None, :]
    gate = jax.nn.sigmoid(values)
    act_conv = (values * gate).astype(BF)
    slope = gate * (1.0 + values * (1.0 - gate)) * channel_norm_gain[None, :]
    proj = mm(mixer_grad, act_conv, FIRST).astype(BF).reshape(experts, -1, 128)
    proj = lax.all_to_all(proj, sp, 0, 0, tiled=True)
    grad_proj = jnp.sum(proj.astype(F32), axis=0)

    grad_norm = mm(mixer_grad, proj_weight, LAST) * slope
    sums = jnp.stack([jnp.sum(grad_norm, axis=1), jnp.sum(grad_norm * normalized, axis=1)])
    sums = sums + flip_c(sums)
    for bit in (1, 2, 4):
        sums = sums + flip_y(sums, bit)
    mean = sums / (128 * 2 * ny)
    conv = inverse_deviation[:, None] * (
        grad_norm - mean[0][:, None] - normalized * mean[1][:, None]
    )
    reach = taps.shape[0] - 1
    beyond = lax.ppermute(conv[:reach], sp, [(i + 1, i) for i in range(experts - 1)])
    extended = jnp.concatenate([conv, beyond], axis=0)
    result = jnp.zeros_like(conv)
    for j in range(reach + 1):
        result = result + taps[j][None, :] * extended[j : j + tok]
    return (result.astype(BF), grad_proj, final[0][None], final[1][None], final[2][None])


def solution(mesh):
    fine = Mesh(mesh.devices.reshape(8, 4, 8, 2), ("z", "x", "y", "c"))
    sp, tp = ("z", "x"), ("y", "c")
    return jax.shard_map(
        shards,
        mesh=fine,
        in_specs=(
            P(sp, None),
            P(sp, None),
            P(sp, None),
            P(sp, None),
            P(sp, tp),
            P(sp),
            P(tp),
            P(None, tp),
            P(tp, None),
            P(sp, None, tp),
            P(sp, None, tp),
            P(sp, tp, None),
        ),
        out_specs=(
            P(sp, tp),
            P(sp, tp),
            P(sp, None, tp),
            P(sp, None, tp),
            P(sp, tp, None),
        ),
        check_vma=False,
    )
```

time: 258 us -> 238 us (0.922)
  blocking collectives: 101 us -> 0 us
  starting transfers between devices: 16.4 us -> 107 us
  matrix products: 16.9 us -> 40.9 us
  waiting for transfers between devices: 84 us -> 60.4 us
  between operations: 14.8 us -> 1.93 us
  local copies, waits for them, and re-layouts: 15.1 us -> 12 us
  other arithmetic: 8.92 us -> 11.8 us
    all_to_all x3 -> x0, blocking collectives: 101 us -> none  [the longest x1 55.3 us: sent_and_summed(): lax.all_to_all(pieces, axis, split_axis=0, concat_axis=0, tiled=True)]
    all_gather x2 -> x0, waiting for transfers between devices: 68.2 us -> none  [the longest x1 42.1 us: side_by_side(): lax.all_gather(both, axis, axis=dim, tiled=True)]
    ppermute x1 -> x25, starting transfers between devices: 1.29 us -> 66.1 us  [the longest x15 41.5 us: flip_c(): return lax.ppermute(value, 'c', SWAP)]
    ppermute x1 -> x25, waiting for transfers between devices: 2.31 us -> 29.9 us  [the longest x9 28.2 us: flip_y(): lax.ppermute(value, 'y', [(i, i ^ bit) for i in range(lax.axis_size('y'))])]
    all_to_all x2 -> x4, starting transfers between devices: 15 us -> 41.2 us  [the longest x1 19.9 us: shards(): lax.all_to_all(back, ('z', 'x', 'y'), 0, 0, tiled=True).reshape(-1, 128)]
    dot_general x13 -> x38, matrix products: 16.9 us -> 40.9 us  [mm(): return lax.dot_general(a, b, dims, preferred_element_type=F32)]
    all_to_all x2 -> x4, waiting for transfers between devices: 13.5 us -> 30.6 us  [the longest x1 15.3 us: shards(): lax.all_to_all(back, ('z', 'x', 'y'), 0, 0, tiled=True).reshape(-1, 128)]
    broadcast_in_dim x0 -> x3, other arithmetic: none -> 6.04 us  [the longest x1 2.02 us: shards(): final[2][None]]
  transfers between devices with their start and end apart: 5 -> 29, of which waited for: 5 -> 10; matrix products, arithmetic and copies ran while one was open for 6% -> 25% of each run, Pallas kernels for 0% -> 0%
where the time goes in v1:
time: 238 us; the launch traced here: 234 us
  starting transfers between devices  107 us (45%)
  waiting for transfers between devices  60.4 us (25%)
  matrix products  40.9 us (17%)
  local copies, waits for them, and re-layouts  12 us (5%)
  other arithmetic  11.8 us (5%)
    ppermute x15, starting transfers between devices, flip_c(): return lax.ppermute(value, 'c', SWAP)  41.5 us
    dot_general x38, matrix products, mm(): return lax.dot_general(a, b, dims, preferred_element_type=F32)  40.9 us
    ppermute x9, waiting for transfers between devices, flip_y(): lax.ppermute(value, 'y', [(i, i ^ bit) for i in range(lax.axis_size('y'))])  28.2 us
    ppermute x9, starting transfers between devices, flip_y(): lax.ppermute(value, 'y', [(i, i ^ bit) for i in range(lax.axis_size('y'))])  23.3 us
    all_to_all x1, starting transfers between devices, shards(): lax.all_to_all(back, ('z', 'x', 'y'), 0, 0, tiled=True).reshape(-1, 128)  19.9 us
    all_to_all x1, waiting for transfers between devices, shards(): lax.all_to_all(back, ('z', 'x', 'y'), 0, 0, tiled=True).reshape(-1, 128)  15.3 us
    all_to_all x1, starting transfers between devices, shards(): got = lax.all_to_all(sent, sp, 0, 0, tiled=True)  13.8 us
    all_to_all x1, waiting for transfers between devices, shards(): proj = lax.all_to_all(proj, sp, 0, 0, tiled=True)  8.38 us
  transfers between devices with their start and end apart: 29, of which 10 were waited for; matrix products, arithmetic and copies ran while one was open for 25% of the time, Pallas kernels for 0%

profile of v1, /device:TPU:1, one launch (start us, length us, event | category | flops | bytes accessed | tf_op | source)
XLA Modules:
  0.0 234.3 jit_solution(10153904562066753439)
XLA Ops:
  6.4 13.8 %all-to-all-start = ((bf16[32,8,2048]{2,1,0:T(8,128)(2,1)}), bf16[32,8,2048]{2,1,0:T(8,128)(2,1)S(1)}, u32[]{:S(2)}, u32[]{:S(2)}) async-start(bf16[32,8,2048]{2,1,0:T(8,128)(2,1)} %pad_maximum_fusion), calls=%async_computation | async-start | bytes 2097152 | tf_op jit(solution)/shard_map/all_to_all | solution.py:67
  20.3 3.2 %collective-permute-start.4 = (bf16[2048,128]{1,0:T(8,128)(2,1)}, bf16[2048,128]{1,0:T(8,128)(2,1)}, u32[]{:S(2)}, u32[]{:S(2)}) collective-permute-start(bf16[2048,128]{1,0:T(8,128)(2,1)} %bitcast.10), channel_id=1, source_target_pairs={{0,2},{2,0},{4,6},{6,4},{8,10},{10,8},{12,14},{14,12},{1,3},{3,1},... | collective-permute-start | bytes 1572872 | tf_op jit(solution)/shard_map/ppermute | solution.py:17
  23.5 3.1 %collective-permute-start.1 = (bf16[2048,128]{1,0:T(8,128)(2,1)}, bf16[2048,128]{1,0:T(8,128)(2,1)}, u32[]{:S(2)}, u32[]{:S(2)}) collective-permute-start(bf16[2048,128]{1,0:T(8,128)(2,1)} %bitcast.10), channel_id=1, source_target_pairs={{0,1},{1,0},{2,3},{3,2},{4,5},{5,4},{6,7},{7,6},{8,9},{9,8},{10,11... | collective-permute-start | bytes 1572872 | tf_op jit(solution)/shard_map/ppermute | solution.py:21
  31.0 3.2 %collective-permute-start.3 = (bf16[128,2048]{1,0:T(8,128)(2,1)}, bf16[128,2048]{1,0:T(8,128)(2,1)}, u32[]{:S(2)}, u32[]{:S(2)}) collective-permute-start(bf16[128,2048]{1,0:T(8,128)(2,1)} %bitcast.9), channel_id=1, source_target_pairs={{0,2},{2,0},{4,6},{6,4},{8,10},{10,8},{12,14},{14,12},{1,3},{3,1},... | collective-permute-start | bytes 1572872 | tf_op jit(solution)/shard_map/ppermute | solution.py:17
  36.3 3.8 %collective-permute-start.7 = (bf16[2048,128]{1,0:T(8,128)(2,1)}, bf16[2048,128]{1,0:T(8,128)(2,1)}, u32[]{:S(2)}, u32[]{:S(2)}) collective-permute-start(bf16[2048,128]{1,0:T(8,128)(2,1)} %collective-permute-done.4), channel_id=1, source_target_pairs={{0,1},{1,0},{2,3},{3,2},{4,5},{5,4},{6,7},{7,6},{8,9},{9,8},{10,11... | collective-permute-start | bytes 1572872 | tf_op jit(solution)/shard_map/ppermute | solution.py:21
  40.8 3.2 %and.97 = pred[256,2048]{1,0:T(32,128)(4,1)} reshape(pred[2,128,32,64]{3,2,1,0:T(32,128)(4,1)S(1)} %broadcast_and_fusion) | data formatting | bytes 1048576 | tf_op jit(solution)/shard_map/and | solution.py:76
  46.3 5.1 %collective-permute-start.8 = (bf16[2048,128]{1,0:T(8,128)(2,1)}, bf16[2048,128]{1,0:T(8,128)(2,1)S(1)}, u32[]{:S(2)}, u32[]{:S(2)}) collective-permute-start(bf16[2048,128]{1,0:T(8,128)(2,1)} %collective-permute-done.5), channel_id=1, source_target_pairs={{0,1},{1,0},{2,3},{3,2},{4,5},{5,4},{6,7},{7,6},{8,9},{9,8},{10,11... | collective-permute-start | bytes 1572872 | tf_op jit(solution)/shard_map/ppermute | solution.py:21
  54.1 3.4 %collective-permute-done.3 = bf16[128,2048]{1,0:T(8,128)(2,1)} collective-permute-done((bf16[128,2048]{1,0:T(8,128)(2,1)}, bf16[128,2048]{1,0:T(8,128)(2,1)}, u32[]{:S(2)}, u32[]{:S(2)}) %collective-permute-start.3) | collective-permute-done | bytes 524320 | tf_op jit(solution)/shard_map/ppermute | solution.py:17
  57.5 3.7 %collective-permute-start = (bf16[128,2048]{1,0:T(8,128)(2,1)}, bf16[128,2048]{1,0:T(8,128)(2,1)S(1)}, u32[]{:S(2)}, u32[]{:S(2)}) collective-permute-start(bf16[128,2048]{1,0:T(8,128)(2,1)} %bitcast.9), channel_id=1, source_target_pairs={{0,1},{1,0},{2,3},{3,2},{4,5},{5,4},{6,7},{7,6},{8,9},{9,8},{10,11... | collective-permute-start | bytes 1572872 | tf_op jit(solution)/shard_map/ppermute | solution.py:21
  66.3 2.6 %collective-permute-start.23 = (bf16[128,2048]{1,0:T(8,128)(2,1)}, bf16[128,2048]{1,0:T(8,128)(2,1)}, u32[]{:S(2)}, u32[]{:S(2)}) collective-permute-start(bf16[128,2048]{1,0:T(8,128)(2,1)} %convolution_convert_fusion), channel_id=1, source_target_pairs={{0,1},{1,0},{2,3},{3,2},{4,5},{5,4},{6,7},{7,6},{8,9},{9,8},{10,11... | collective-permute-start | bytes 1572872 | tf_op jit(solution)/shard_map/ppermute | solution.py:21
  91.6 19.9 %all-to-all-start.1 = ((bf16[256,8,128]{2,1,0:T(8,128)(2,1)}), bf16[256,8,128]{2,1,0:T(8,128)(2,1)}, u32[]{:S(2)}, u32[]{:S(2)}) async-start(bf16[256,8,128]{2,1,0:T(8,128)(2,1)} %copy.42), calls=%async_computation.1 | async-start | bytes 1048576 | tf_op jit(solution)/shard_map/all_to_all | solution.py:93
  115.6 15.3 %all-to-all-done.1 = bf16[256,8,128]{2,1,0:T(8,128)(2,1)} async-done(((bf16[256,8,128]{2,1,0:T(8,128)(2,1)}), bf16[256,8,128]{2,1,0:T(8,128)(2,1)}, u32[]{:S(2)}, u32[]{:S(2)}) %all-to-all-start.1) | async-done | bytes 524320 | tf_op jit(solution)/shard_map/all_to_all | solution.py:93
  132.5 3.5 %collective-permute-start.9 = (bf16[128,128]{1,0:T(8,128)(2,1)S(1)}, bf16[128,128]{1,0:T(8,128)(2,1)S(1)}, u32[]{:S(2)}, u32[]{:S(2)}) collective-permute-start(bf16[128,128]{1,0:T(8,128)(2,1)S(1)} %slice.789), channel_id=1, source_target_pairs={{0,1},{1,0},{2,3},{3,2},{4,5},{5,4},{6,7},{7,6},{8,9},{9,8},{10,11... | collective-permute-start | bytes 98312 | tf_op jit(solution)/shard_map/ppermute | solution.py:21
  139.0 2.4 %collective-permute-start.20 = (bf16[2048,128]{1,0:T(8,128)(2,1)}, bf16[2048,128]{1,0:T(8,128)(2,1)}, u32[]{:S(2)}, u32[]{:S(2)}) collective-permute-start(bf16[2048,128]{1,0:T(8,128)(2,1)} %convolution_convert_fusion.2), channel_id=1, source_target_pairs={{0,1},{1,0},{2,3},{3,2},{4,5},{5,4},{6,7},{7,6},{8,9},{9,8},{10,11... | collective-permute-start | bytes 1572872 | tf_op jit(solution)/shard_map/ppermute | solution.py:21
  143.4 2.4 %collective-permute-start.17 = (bf16[2048,128]{1,0:T(8,128)(2,1)}, bf16[2048,128]{1,0:T(8,128)(2,1)}, u32[]{:S(2)}, u32[]{:S(2)}) collective-permute-start(bf16[2048,128]{1,0:T(8,128)(2,1)} %convolution_convert_fusion.4), channel_id=1, source_target_pairs={{0,1},{1,0},{2,3},{3,2},{4,5},{5,4},{6,7},{7,6},{8,9},{9,8},{10,11... | collective-permute-start | bytes 1572872 | tf_op jit(solution)/shard_map/ppermute | solution.py:21
  147.4 3.4 %all-to-all-start.2 = ((bf16[8,128,128]{1,2,0:T(8,128)(2,1)}), bf16[8,128,128]{1,2,0:T(8,128)(2,1)S(1)}, u32[]{:S(2)}, u32[]{:S(2)}) async-start(bf16[8,128,128]{1,2,0:T(8,128)(2,1)} %broadcast_in_dim.79), calls=%async_computation.2 | async-start | bytes 524288 | tf_op jit(solution)/shard_map/all_to_all | solution.py:111
  156.3 6.8 %all-to-all-done.2 = bf16[8,128,128]{1,2,0:T(8,128)(2,1)S(1)} async-done(((bf16[8,128,128]{1,2,0:T(8,128)(2,1)}), bf16[8,128,128]{1,2,0:T(8,128)(2,1)S(1)}, u32[]{:S(2)}, u32[]{:S(2)}) %all-to-all-start.2) | async-done | bytes 262176 | tf_op jit(solution)/shard_map/all_to_all | solution.py:111
  169.9 2.4 %collective-permute-start.11 = (f32[2,128]{1,0:T(2,128)S(1)}, f32[2,128]{1,0:T(2,128)S(1)}, u32[]{:S(2)}, u32[]{:S(2)}) collective-permute-start(f32[2,128]{1,0:T(2,128)S(1)} %pad_maximum_fusion.3), channel_id=1, source_target_pairs={{0,1},{1,0},{2,3},{3,2},{4,5},{5,4},{6,7},{7,6},{8,9},{9,8},{10,11... | collective-permute-start | bytes 3080 | tf_op jit(solution)/shard_map/ppermute | solution.py:21
  174.5 3.1 %collective-permute-start.21 = (bf16[2048,128]{1,0:T(8,128)(2,1)S(1)}, bf16[2048,128]{1,0:T(8,128)(2,1)S(1)}, u32[]{:S(2)}, u32[]{:S(2)}) collective-permute-start(bf16[2048,128]{1,0:T(8,128)(2,1)S(1)} %add_convert_fusion.3), channel_id=1, source_target_pairs={{0,2},{2,0},{4,6},{6,4},{8,10},{10,8},{12,14},{14,12},{1,3},{3,1},... | collective-permute-start | bytes 1572872 | tf_op jit(solution)/shard_map/ppermute | solution.py:17
  179.9 2.7 %collective-permute-done.24 = bf16[128,2048]{1,0:T(8,128)(2,1)S(1)} collective-permute-done((bf16[128,2048]{1,0:T(8,128)(2,1)}, bf16[128,2048]{1,0:T(8,128)(2,1)S(1)}, u32[]{:S(2)}, u32[]{:S(2)}) %collective-permute-start.24) | collective-permute-done | bytes 524320 | tf_op jit(solution)/shard_map/ppermute | solution.py:17
  186.9 18.3 %collective-permute-done.12 = f32[2,128]{1,0:T(2,128)S(1)} collective-permute-done((f32[2,128]{1,0:T(2,128)S(1)}, f32[2,128]{1,0:T(2,128)S(1)}, u32[]{:S(2)}, u32[]{:S(2)}) %collective-permute-start.12) | collective-permute-done | bytes 1056 | tf_op jit(solution)/shard_map/ppermute | solution.py:17
  210.4 2.9 %collective-permute-start.14 = (f32[2,128]{1,0:T(2,128)S(1)}, f32[2,128]{1,0:T(2,128)S(1)}, u32[]{:S(2)}, u32[]{:S(2)}) collective-permute-start(f32[2,128]{1,0:T(2,128)S(1)} %add.304), channel_id=1, source_target_pairs={{0,8},{2,10},{4,12},{6,14},{8,0},{10,2},{12,4},{14,6},{1,9},{3,11}... | collective-permute-start | bytes 3080 | tf_op jit(solution)/shard_map/ppermute | solution.py:17
  214.5 4.0 %all-to-all-start.3 = ((bf16[32,64,128]{2,1,0:T(8,128)(2,1)}), bf16[32,64,128]{2,1,0:T(8,128)(2,1)S(1)}, u32[]{:S(2)}, u32[]{:S(2)}) async-start(bf16[32,64,128]{2,1,0:T(8,128)(2,1)} %bitcast.55), calls=%async_computation.3 | async-start | bytes 1048576 | tf_op jit(solution)/shard_map/all_to_all | solution.py:123
  225.2 8.4 %all-to-all-done.3 = bf16[32,64,128]{2,1,0:T(8,128)(2,1)S(1)} async-done(((bf16[32,64,128]{2,1,0:T(8,128)(2,1)}), bf16[32,64,128]{2,1,0:T(8,128)(2,1)S(1)}, u32[]{:S(2)}, u32[]{:S(2)}) %all-to-all-start.3) | async-done | bytes 524320 | tf_op jit(solution)/shard_map/all_to_all | solution.py:123
  (208 shorter events, 91.5 us)
Async XLA Ops:
  6.4 44.9 %all-to-all-start = ((bf16[32,8,2048]{2,1,0:T(8,128)(2,1)}), bf16[32,8,2048]{2,1,0:T(8,128)(2,1)S(1)}, u32[]{:S(2)}, u32[]{:S(2)}) async-start(bf16[32,8,2048]{2,1,0:T(8,128)(2,1)} %pad_maximum_fusion), calls=%async_computation | async-start | bytes 2097152 | tf_op jit(solution)/shard_map/all_to_all | solution.py:67
  20.3 16.0 %collective-permute-start.4 = (bf16[2048,128]{1,0:T(8,128)(2,1)}, bf16[2048,128]{1,0:T(8,128)(2,1)}, u32[]{:S(2)}, u32[]{:S(2)}) collective-permute-start(bf16[2048,128]{1,0:T(8,128)(2,1)} %bitcast.10), channel_id=1, source_target_pairs={{0,2},{2,0},{4,6},{6,4},{8,10},{10,8},{12,14},{14,12},{1,3},{3,1},... | collective-permute-start | bytes 1572872 | tf_op jit(solution)/shard_map/ppermute | solution.py:17
  23.5 46.7 %collective-permute-start.1 = (bf16[2048,128]{1,0:T(8,128)(2,1)}, bf16[2048,128]{1,0:T(8,128)(2,1)}, u32[]{:S(2)}, u32[]{:S(2)}) collective-permute-start(bf16[2048,128]{1,0:T(8,128)(2,1)} %bitcast.10), channel_id=1, source_target_pairs={{0,1},{1,0},{2,3},{3,2},{4,5},{5,4},{6,7},{7,6},{8,9},{9,8},{10,11... | collective-permute-start | bytes 1572872 | tf_op jit(solution)/shard_map/ppermute | solution.py:21
  26.7 19.6 %collective-permute-start.5 = (bf16[2048,128]{1,0:T(8,128)(2,1)S(1)}, bf16[2048,128]{1,0:T(8,128)(2,1)}, u32[]{:S(2)}, u32[]{:S(2)}) collective-permute-start(bf16[2048,128]{1,0:T(8,128)(2,1)S(1)} %bitcast.183), channel_id=1, source_target_pairs={{0,2},{2,0},{4,6},{6,4},{8,10},{10,8},{12,14},{14,12},{1,3},{3,1},... | collective-permute-start | bytes 1572872 | tf_op jit(solution)/shard_map/ppermute | solution.py:17
  28.8 42.8 %collective-permute-start.2 = (bf16[2048,128]{1,0:T(8,128)(2,1)S(1)}, bf16[2048,128]{1,0:T(8,128)(2,1)}, u32[]{:S(2)}, u32[]{:S(2)}) collective-permute-start(bf16[2048,128]{1,0:T(8,128)(2,1)S(1)} %bitcast.184), channel_id=1, source_target_pairs={{0,1},{1,0},{2,3},{3,2},{4,5},{5,4},{6,7},{7,6},{8,9},{9,8},{10,11... | collective-permute-start | bytes 1572872 | tf_op jit(solution)/shard_map/ppermute | solution.py:21
  31.0 26.5 %collective-permute-start.3 = (bf16[128,2048]{1,0:T(8,128)(2,1)}, bf16[128,2048]{1,0:T(8,128)(2,1)}, u32[]{:S(2)}, u32[]{:S(2)}) collective-permute-start(bf16[128,2048]{1,0:T(8,128)(2,1)} %bitcast.9), channel_id=1, source_target_pairs={{0,2},{2,0},{4,6},{6,4},{8,10},{10,8},{12,14},{14,12},{1,3},{3,1},... | collective-permute-start | bytes 1572872 | tf_op jit(solution)/shard_map/ppermute | solution.py:17
  36.3 24.9 %collective-permute-start.7 = (bf16[2048,128]{1,0:T(8,128)(2,1)}, bf16[2048,128]{1,0:T(8,128)(2,1)}, u32[]{:S(2)}, u32[]{:S(2)}) collective-permute-start(bf16[2048,128]{1,0:T(8,128)(2,1)} %collective-permute-done.4), channel_id=1, source_target_pairs={{0,1},{1,0},{2,3},{3,2},{4,5},{5,4},{6,7},{7,6},{8,9},{9,8},{10,11... | collective-permute-start | bytes 1572872 | tf_op jit(solution)/shard_map/ppermute | solution.py:21
  46.3 18.2 %collective-permute-start.8 = (bf16[2048,128]{1,0:T(8,128)(2,1)}, bf16[2048,128]{1,0:T(8,128)(2,1)S(1)}, u32[]{:S(2)}, u32[]{:S(2)}) collective-permute-start(bf16[2048,128]{1,0:T(8,128)(2,1)} %collective-permute-done.5), channel_id=1, source_target_pairs={{0,1},{1,0},{2,3},{3,2},{4,5},{5,4},{6,7},{7,6},{8,9},{9,8},{10,11... | collective-permute-start | bytes 1572872 | tf_op jit(solution)/shard_map/ppermute | solution.py:21
  57.5 25.0 %collective-permute-start = (bf16[128,2048]{1,0:T(8,128)(2,1)}, bf16[128,2048]{1,0:T(8,128)(2,1)S(1)}, u32[]{:S(2)}, u32[]{:S(2)}) collective-permute-start(bf16[128,2048]{1,0:T(8,128)(2,1)} %bitcast.9), channel_id=1, source_target_pairs={{0,1},{1,0},{2,3},{3,2},{4,5},{5,4},{6,7},{7,6},{8,9},{9,8},{10,11... | collective-permute-start | bytes 1572872 | tf_op jit(solution)/shard_map/ppermute | solution.py:21
  61.2 17.1 %collective-permute-start.6 = (bf16[128,2048]{1,0:T(8,128)(2,1)}, bf16[128,2048]{1,0:T(8,128)(2,1)S(1)}, u32[]{:S(2)}, u32[]{:S(2)}) collective-permute-start(bf16[128,2048]{1,0:T(8,128)(2,1)} %collective-permute-done.3), channel_id=1, source_target_pairs={{0,1},{1,0},{2,3},{3,2},{4,5},{5,4},{6,7},{7,6},{8,9},{9,8},{10,11... | collective-permute-start | bytes 1572872 | tf_op jit(solution)/shard_map/ppermute | solution.py:21
  66.3 85.7 %collective-permute-start.23 = (bf16[128,2048]{1,0:T(8,128)(2,1)}, bf16[128,2048]{1,0:T(8,128)(2,1)}, u32[]{:S(2)}, u32[]{:S(2)}) collective-permute-start(bf16[128,2048]{1,0:T(8,128)(2,1)} %convolution_convert_fusion), channel_id=1, source_target_pairs={{0,1},{1,0},{2,3},{3,2},{4,5},{5,4},{6,7},{7,6},{8,9},{9,8},{10,11... | collective-permute-start | bytes 1572872 | tf_op jit(solution)/shard_map/ppermute | solution.py:21
  91.6 39.4 %all-to-all-start.1 = ((bf16[256,8,128]{2,1,0:T(8,128)(2,1)}), bf16[256,8,128]{2,1,0:T(8,128)(2,1)}, u32[]{:S(2)}, u32[]{:S(2)}) async-start(bf16[256,8,128]{2,1,0:T(8,128)(2,1)} %copy.42), calls=%async_computation.1 | async-start | bytes 1048576 | tf_op jit(solution)/shard_map/all_to_all | solution.py:93
  132.5 10.9 %collective-permute-start.9 = (bf16[128,128]{1,0:T(8,128)(2,1)S(1)}, bf16[128,128]{1,0:T(8,128)(2,1)S(1)}, u32[]{:S(2)}, u32[]{:S(2)}) collective-permute-start(bf16[128,128]{1,0:T(8,128)(2,1)S(1)} %slice.789), channel_id=1, source_target_pairs={{0,1},{1,0},{2,3},{3,2},{4,5},{5,4},{6,7},{7,6},{8,9},{9,8},{10,11... | collective-permute-start | bytes 98312 | tf_op jit(solution)/shard_map/ppermute | solution.py:21
  137.1 40.5 %collective-permute-start.22 = (bf16[128,2048]{1,0:T(8,128)(2,1)}, bf16[128,2048]{1,0:T(8,128)(2,1)}, u32[]{:S(2)}, u32[]{:S(2)}) collective-permute-start(bf16[128,2048]{1,0:T(8,128)(2,1)} %convolution_convert_fusion.1), channel_id=1, source_target_pairs={{0,1},{1,0},{2,3},{3,2},{4,5},{5,4},{6,7},{7,6},{8,9},{9,8},{10,11... | collective-permute-start | bytes 1572872 | tf_op jit(solution)/shard_map/ppermute | solution.py:21
  139.0 17.3 %collective-permute-start.20 = (bf16[2048,128]{1,0:T(8,128)(2,1)}, bf16[2048,128]{1,0:T(8,128)(2,1)}, u32[]{:S(2)}, u32[]{:S(2)}) collective-permute-start(bf16[2048,128]{1,0:T(8,128)(2,1)} %convolution_convert_fusion.2), channel_id=1, source_target_pairs={{0,1},{1,0},{2,3},{3,2},{4,5},{5,4},{6,7},{7,6},{8,9},{9,8},{10,11... | collective-permute-start | bytes 1572872 | tf_op jit(solution)/shard_map/ppermute | solution.py:21
  141.4 65.7 %collective-permute-start.19 = (bf16[2048,128]{1,0:T(8,128)(2,1)}, bf16[2048,128]{1,0:T(8,128)(2,1)}, u32[]{:S(2)}, u32[]{:S(2)}) collective-permute-start(bf16[2048,128]{1,0:T(8,128)(2,1)} %convolution_convert_fusion.3), channel_id=1, source_target_pairs={{0,1},{1,0},{2,3},{3,2},{4,5},{5,4},{6,7},{7,6},{8,9},{9,8},{10,11... | collective-permute-start | bytes 1572872 | tf_op jit(solution)/shard_map/ppermute | solution.py:21
  143.4 26.6 %collective-permute-start.17 = (bf16[2048,128]{1,0:T(8,128)(2,1)}, bf16[2048,128]{1,0:T(8,128)(2,1)}, u32[]{:S(2)}, u32[]{:S(2)}) collective-permute-start(bf16[2048,128]{1,0:T(8,128)(2,1)} %convolution_convert_fusion.4), channel_id=1, source_target_pairs={{0,1},{1,0},{2,3},{3,2},{4,5},{5,4},{6,7},{7,6},{8,9},{9,8},{10,11... | collective-permute-start | bytes 1572872 | tf_op jit(solution)/shard_map/ppermute | solution.py:21
  147.4 15.7 %all-to-all-start.2 = ((bf16[8,128,128]{1,2,0:T(8,128)(2,1)}), bf16[8,128,128]{1,2,0:T(8,128)(2,1)S(1)}, u32[]{:S(2)}, u32[]{:S(2)}) async-start(bf16[8,128,128]{1,2,0:T(8,128)(2,1)} %broadcast_in_dim.79), calls=%async_computation.2 | async-start | bytes 524288 | tf_op jit(solution)/shard_map/all_to_all | solution.py:111
  152.0 68.5 %collective-permute-start.16 = (bf16[2048,128]{1,0:T(8,128)(2,1)}, bf16[2048,128]{1,0:T(8,128)(2,1)S(1)}, u32[]{:S(2)}, u32[]{:S(2)}) collective-permute-start(bf16[2048,128]{1,0:T(8,128)(2,1)} %convolution_convert_fusion.5), channel_id=1, source_target_pairs={{0,1},{1,0},{2,3},{3,2},{4,5},{5,4},{6,7},{7,6},{8,9},{9,8},{10,11... | collective-permute-start | bytes 1572872 | tf_op jit(solution)/shard_map/ppermute | solution.py:21
  167.0 15.6 %collective-permute-start.24 = (bf16[128,2048]{1,0:T(8,128)(2,1)}, bf16[128,2048]{1,0:T(8,128)(2,1)S(1)}, u32[]{:S(2)}, u32[]{:S(2)}) collective-permute-start(bf16[128,2048]{1,0:T(8,128)(2,1)} %add_convert_fusion.1), channel_id=1, source_target_pairs={{0,2},{2,0},{4,6},{6,4},{8,10},{10,8},{12,14},{14,12},{1,3},{3,1},... | collective-permute-start | bytes 1572872 | tf_op jit(solution)/shard_map/ppermute | solution.py:17
  174.5 32.7 %collective-permute-start.21 = (bf16[2048,128]{1,0:T(8,128)(2,1)S(1)}, bf16[2048,128]{1,0:T(8,128)(2,1)S(1)}, u32[]{:S(2)}, u32[]{:S(2)}) collective-permute-start(bf16[2048,128]{1,0:T(8,128)(2,1)S(1)} %add_convert_fusion.3), channel_id=1, source_target_pairs={{0,2},{2,0},{4,6},{6,4},{8,10},{10,8},{12,14},{14,12},{1,3},{3,1},... | collective-permute-start | bytes 1572872 | tf_op jit(solution)/shard_map/ppermute | solution.py:17
  177.6 42.9 %collective-permute-start.18 = (bf16[2048,128]{1,0:T(8,128)(2,1)}, bf16[2048,128]{1,0:T(8,128)(2,1)}, u32[]{:S(2)}, u32[]{:S(2)}) collective-permute-start(bf16[2048,128]{1,0:T(8,128)(2,1)} %add_convert_fusion.5), channel_id=1, source_target_pairs={{0,2},{2,0},{4,6},{6,4},{8,10},{10,8},{12,14},{14,12},{1,3},{3,1},... | collective-permute-start | bytes 1572872 | tf_op jit(solution)/shard_map/ppermute | solution.py:17
  182.6 22.6 %collective-permute-start.12 = (f32[2,128]{1,0:T(2,128)S(1)}, f32[2,128]{1,0:T(2,128)S(1)}, u32[]{:S(2)}, u32[]{:S(2)}) collective-permute-start(f32[2,128]{1,0:T(2,128)S(1)} %fusion.158), channel_id=1, source_target_pairs={{0,2},{2,0},{4,6},{6,4},{8,10},{10,8},{12,14},{14,12},{1,3},{3,1},... | collective-permute-start | bytes 3080 | tf_op jit(solution)/shard_map/ppermute | solution.py:17
  214.5 19.1 %all-to-all-start.3 = ((bf16[32,64,128]{2,1,0:T(8,128)(2,1)}), bf16[32,64,128]{2,1,0:T(8,128)(2,1)S(1)}, u32[]{:S(2)}, u32[]{:S(2)}) async-start(bf16[32,64,128]{2,1,0:T(8,128)(2,1)} %bitcast.55), calls=%async_computation.3 | async-start | bytes 1048576 | tf_op jit(solution)/shard_map/all_to_all | solution.py:123
  (49 other events, 332.4 us)

commit v2 on v1

v2 whole, which is shorter than its diff:
```python
import jax
import jax.numpy as jnp
from jax import lax
from jax.experimental import pallas as pl
from jax.experimental.pallas import tpu as pltpu
from jax.sharding import Mesh, PartitionSpec as P

BF, F32, I32 = jnp.bfloat16, jnp.float32, jnp.int32
LAST = (((1,), (1,)), ((), ()))
FIRST = (((0,), (0,)), ((), ()))
SPAN = 4
VMEM = pl.BlockSpec(memory_space=pltpu.VMEM)


def mm(a, b, dims=(((1,), (0,)), ((), ()))):
    return lax.dot_general(a, b, dims, preferred_element_type=F32)


def iota(shape, dim):
    return lax.broadcasted_iota(I32, shape, dim)


def kernel(body, outs, flops, *args):
    return pl.pallas_call(
        body,
        out_shape=outs,
        in_specs=[VMEM] * len(args),
        out_specs=jax.tree.map(lambda _: VMEM, outs),
        cost_estimate=pl.CostEstimate(flops=flops, bytes_accessed=1 << 20, transcendentals=0),
    )(*args)


def shape(*dims, kind=BF):
    return jax.ShapeDtypeStruct(dims, kind)


def head_body(ids_ref, weight_ref, mix_ref, cot_ref, out_ref):
    tok = ids_ref.shape[0]
    experts = out_ref.shape[0] // (2 * SPAN)
    group = (lax.axis_index("y") % 2) * 2 + lax.axis_index("c")
    ids = [jnp.broadcast_to(ids_ref[:, k : k + 1], (tok, tok)).T[:1] for k in range(2)]
    wts = [jnp.broadcast_to(weight_ref[:, k : k + 1], (tok, tok)).T[:1] for k in range(2)]
    expert = iota((experts, tok), 0)
    hot = [(expert == i).astype(F32) for i in ids]
    after = (iota((tok, tok), 0) < iota((tok, tok), 1)).astype(BF)
    rank = mm((hot[0] + hot[1]).astype(BF), after)
    rows = out_ref.shape[0]
    row = iota((rows, tok), 0)
    row_e, row_j = row // (2 * SPAN), row % (2 * SPAN)
    target = group * SPAN + row_j % SPAN
    found = jnp.zeros((rows, tok), jnp.bool_)
    scale = jnp.zeros((rows, tok), F32)
    for i, w, h in zip(ids, wts, hot):
        place = jnp.sum(rank * h, axis=0, keepdims=True).astype(I32)
        match = (row_e == i) & (target == place)
        found = found | match
        scale = jnp.where(match, w, scale)
    scale = jnp.sum(scale, axis=1, keepdims=True)
    is_x = row_j < SPAN
    take_x = jnp.where(found & is_x, 1.0, 0.0).astype(BF)
    take_g = jnp.where(found & ~is_x, 1.0, 0.0).astype(BF)
    scale = jnp.where(iota((rows, 1), 0) % (2 * SPAN) < SPAN, 1.0, scale)
    step = 512
    for at in range(0, mix_ref.shape[1], step):
        picked = mm(take_x, mix_ref[:, at : at + step]) + mm(take_g, cot_ref[:, at : at + step])
        out_ref[:, at : at + step] = (picked * scale).astype(BF)


def table_body(ids_ref, out_ref):
    tok = ids_ref.shape[0]
    ci = lax.axis_index("c")
    cols = out_ref.shape[1]
    experts = cols // 64
    lane = iota((tok, experts), 1)
    hot = jnp.zeros((tok, experts), F32)
    for k in range(2):
        hot = hot + (lane == ids_ref[:, k : k + 1]).astype(F32)
    before = (iota((tok, tok), 0) > iota((tok, tok), 1)).astype(BF)
    slot = jnp.where(hot > 0, mm(before, hot.astype(BF)), -1.0)
    spread = (iota((experts, cols), 1) // 64 == iota((experts, cols), 0)).astype(BF)
    held = mm(slot.astype(BF), spread).astype(I32)
    col = iota((tok, cols), 1)
    place = ((col // 8) % 2 * 2 + ci) * SPAN + col % SPAN
    half = (col // SPAN) % 2
    hit = held == place
    out_ref[:tok, :] = jnp.where(hit & (half == ci), 1.0, 0.0).astype(BF)
    out_ref[tok:, :] = jnp.where(hit & (half != ci), 1.0, 0.0).astype(BF)


def pack_body(gate_ref, up_ref, down_ref, out_ref):
    out_ref[0] = gate_ref[...]
    out_ref[1] = up_ref[...]
    for j in range(down_ref.shape[1] // 128):
        out_ref[2, j * 128 : (j + 1) * 128, :] = down_ref[:, j * 128 : (j + 1) * 128]


def expert_body(got_ref, w0, w1, w2, w3, x_ref, g_ref, hid_ref, back_ref):
    rows, width = got_ref.shape
    slots = rows // 2
    out_row, in_row = iota((slots, rows), 0), iota((slots, rows), 1)
    want = (out_row // SPAN) * (2 * SPAN) + out_row % SPAN
    pick_x = (in_row == want).astype(BF)
    pick_g = (in_row == want + SPAN).astype(BF)
    for at in range(0, width, 512):
        part = got_ref[:, at : at + 512]
        x_ref[:, at : at + 512] = mm(pick_x, part).astype(BF)
        g_ref[:, at : at + 512] = mm(pick_g, part).astype(BF)
    for q, w in enumerate((w0, w1, w2, w3)):
        hg = mm(x_ref[...], w[0])
        hu = mm(x_ref[...], w[1])
        gact = jnp.zeros((slots, 128), F32)
        for j in range(width // 128):
            gact = gact + mm(
                g_ref[:, j * 128 : (j + 1) * 128], w[2, j * 128 : (j + 1) * 128, :], LAST
            )
        sigma = jax.nn.sigmoid(hg)
        swish = hg * sigma
        lanes = slice(q * 128, (q + 1) * 128)
        hid_ref[0, :, lanes] = (gact * hu * sigma * (1.0 + hg * (1.0 - sigma))).astype(BF)
        hid_ref[1, :, lanes] = (gact * swish).astype(BF)
        hid_ref[2, :, lanes] = (swish * hu).astype(BF)
    low = iota((slots, 128), 0) % (2 * SPAN) < SPAN
    for y in range(width // 256):
        pair = []
        for h in range(2):
            at = (y * 2 + h) * 128
            acc = jnp.zeros((slots, 128), F32)
            for q, w in enumerate((w0, w1, w2, w3)):
                lanes = slice(q * 128, (q + 1) * 128)
                acc = acc + mm(hid_ref[0, :, lanes], w[0, at : at + 128, :], LAST)
                acc = acc + mm(hid_ref[1, :, lanes], w[1, at : at + 128, :], LAST)
            pair.append(acc)
        even = jnp.where(low, pair[0], pltpu.roll(pair[1], SPAN, 0))
        odd = jnp.where(low, pltpu.roll(pair[0], slots - SPAN, 0), pair[1])
        back_ref[:, y * 8 : (y + 1) * 8, :] = even.reshape(-1, 8, 128).astype(BF)
        back_ref[:, 64 + y * 8 : 64 + (y + 1) * 8, :] = odd.reshape(-1, 8, 128).astype(BF)


def grads_body(x_ref, g_ref, hid_ref, keep_ref, give_ref):
    width = x_ref.shape[1]
    for j in range(width // 128):
        at = slice(j * 128, (j + 1) * 128)
        xt, gt = x_ref[:, at], g_ref[:, at]
        for m in range(3):
            h = hid_ref[m]
            both = mm(xt, h, FIRST) if m < 2 else mm(h, gt, FIRST)
            for q in range(4):
                ref, to = ((keep_ref, 0), (give_ref, 0), (keep_ref, 1), (give_ref, 1))[q]
                cut = slice(q * 128, (q + 1) * 128)
                piece = both[:, cut] if m < 2 else both[cut, :]
                ref[to, m, at, :] = piece.astype(BF)


def final_body(mine_ref, other_ref, proj_ref, act_ref, slope_ref, norm_ref, out_ref, grad_ref, sum_ref):
    ci = lax.axis_index("c")
    tok = act_ref.shape[0]
    acc = jnp.zeros((tok, tok), F32)
    for y in range(mine_ref.shape[0]):
        for ref, cc in ((mine_ref, ci), (other_ref, 1 - ci)):
            at = pl.ds(pl.multiple_of((2 * y + cc) * 128, 128), 128)
            part = ref[y]
            out_ref[at, :] = mm(part, act_ref[...], FIRST).astype(BF)
            acc = acc + mm(part, proj_ref[:, at], LAST)
    grad = acc * slope_ref[...]
    grad_ref[...] = grad
    sum_ref[0:1, :] = jnp.sum(grad.T, axis=0, keepdims=True)
    sum_ref[1:2, :] = jnp.sum((grad * norm_ref[...]).T, axis=0, keepdims=True)


def shards(
    cotangent,
    mixer_out,
    expert_ids,
    route_weight,
    saved_normalized,
    inverse_deviation,
    channel_norm_gain,
    taps,
    proj_weight,
    gate_weight,
    up_weight,
    down_weight,
):
    sp = ("z", "x")
    experts = lax.axis_size(sp)
    ny = lax.axis_size("y")
    yi, ci = lax.axis_index("y"), lax.axis_index("c")
    tok, width = cotangent.shape

    def flip_c(value):
        return lax.ppermute(value, "c", [(0, 1), (1, 0)])

    def hop(value, sign):
        pairs = []
        for y in range(ny):
            for c in range(2):
                pairs.append((2 * y + c, 2 * ((y + (sign if c == 0 else -sign)) % ny) + c))
        return lax.ppermute(value, ("y", "c"), pairs)

    own = kernel(pack_body, shape(3, width, 128), 1000000, gate_weight[0], up_weight[0], down_weight[0])
    by_y = hop(own, 1)
    by_c = flip_c(own)
    by_yc = flip_c(by_y)

    rows = experts * 2 * SPAN
    sent = kernel(
        head_body, shape(rows, width), 2000000000, expert_ids, route_weight, mixer_out, cotangent
    )
    got = lax.all_to_all(sent.reshape(experts, 2 * SPAN, width), sp, 0, 0, tiled=True)
    table = kernel(table_body, shape(2 * tok, experts * ny * 2 * SPAN), 2000000000, expert_ids)

    normalized = saved_normalized.astype(F32)
    values = normalized * channel_norm_gain[None, :]
    gate = jax.nn.sigmoid(values)
    act_conv = (values * gate).astype(BF)
    slope = gate * (1.0 + values * (1.0 - gate)) * channel_norm_gain[None, :]

    slots = experts * SPAN
    x, g, hidden, back = kernel(
        expert_body,
        (shape(slots, width), shape(slots, width), shape(3, slots, 512), shape(experts // 2, 128, 128)),
        4000000000,
        got.reshape(rows, width),
        own,
        by_c,
        by_y,
        by_yc,
    )
    home = lax.all_to_all(
        back.reshape(experts * ny, 2 * SPAN, 128), ("z", "x", "y"), 0, 0, tiled=True
    ).reshape(-1, 128)

    packed = shape(2, 3, width, 128)
    keep, give = kernel(grads_body, (packed, packed), 8000000000, x, g, hidden)
    given = flip_c(give)
    passed = hop((keep[1].astype(F32) + given[1].astype(F32)).astype(BF), -1)
    final = (keep[0].astype(F32) + given[0].astype(F32) + passed.astype(F32)).astype(BF)
    grad_down = final[2].reshape(-1, 128, 128).transpose(1, 0, 2).reshape(128, width)

    combined = mm(table, home)
    other = flip_c(combined[tok:].astype(BF))
    feat = (yi * 2 + ci) * 128
    cot = lax.dynamic_slice_in_dim(cotangent, feat, 128, axis=1)
    mix = (cot.astype(F32) + combined[:tok] + other.astype(F32)).astype(BF)
    mine_all = lax.all_to_all(jnp.broadcast_to(mix[None], (ny, *mix.shape)), "y", 0, 0, tiled=True)
    other_all = flip_c(mine_all)

    proj, grad_norm, sums = kernel(
        final_body,
        (shape(width, 128), shape(tok, 128, kind=F32), shape(2, 128, kind=F32)),
        2000000000,
        mine_all,
        other_all,
        proj_weight,
        act_conv,
        slope,
        normalized,
    )
    proj = lax.all_to_all(proj.reshape(experts, -1, 128), sp, 0, 0, tiled=True)
    grad_proj = jnp.sum(proj.astype(F32), axis=0)

    sums = sums + flip_c(sums)
    for bit in (1, 2, 4):
        sums = sums + lax.ppermute(sums, "y", [(i, i ^ bit) for i in range(ny)])
    mean = sums / (128 * 2 * ny)
    conv = inverse_deviation[:, None] * (
        grad_norm - mean[0][:, None] - normalized * mean[1][:, None]
    )
    reach = taps.shape[0] - 1
    beyond = lax.ppermute(conv[:reach], sp, [(i + 1, i) for i in range(experts - 1)])
    extended = jnp.concatenate([conv, beyond], axis=0)
    result = jnp.zeros_like(conv)
    for j in range(reach + 1):
        result = result + taps[j][None, :] * extended[j : j + tok]
    return (result.astype(BF), grad_proj, final[0][None], final[1][None], grad_down[None])


def solution(mesh):
    fine = Mesh(mesh.devices.reshape(8, 4, 8, 2), ("z", "x", "y", "c"))
    sp, tp = ("z", "x"), ("y", "c")
    return jax.shard_map(
        shards,
        mesh=fine,
        in_specs=(
            P(sp, None),
            P(sp, None),
            P(sp, None),
            P(sp, None),
            P(sp, tp),
            P(sp),
            P(tp),
            P(None, tp),
            P(tp, None),
            P(sp, None, tp),
            P(sp, None, tp),
            P(sp, tp, None),
        ),
        out_specs=(
            P(sp, tp),
            P(sp, tp),
            P(sp, None, tp),
            P(sp, None, tp),
            P(sp, tp, None),
        ),
        check_vma=False,
    )
```

time: 238 us -> 194 us (0.82)
  the two profiles are of different devices: /device:TPU:1 before, /device:TPU:8 now
where the time goes in v2:
time: 194 us; the launch traced here: 193 us
  waiting for transfers between devices  81.1 us (42%)
  starting transfers between devices  64.4 us (33%)
  Pallas kernels  26.5 us (14%)
  other arithmetic  11 us (6%)
  local copies, waits for them, and re-layouts  7.37 us (4%)
    pallas_call x6, Pallas kernels, kernel(): pl.pallas_call(body, out_shape=outs, in_specs=[VMEM] * len(args), out_spe...  26.5 us
    all_to_all x1, waiting for transfers between devices, shards(): lax.all_to_all(sent.reshape(experts, 2 * SPAN, width), sp, 0, 0, tiled=True)  19.8 us
    all_to_all x1, waiting for transfers between devices, shards(): lax.all_to_all(back.reshape(experts * ny, 2 * SPAN, 128), ('z', 'x', 'y')...  18.6 us
    ppermute x3, waiting for transfers between devices, shards(): sums = sums + lax.ppermute(sums, 'y', [(i, i ^ bit) for i in range(ny)])  15.2 us
    all_to_all x1, starting transfers between devices, shards(): lax.all_to_all(back.reshape(experts * ny, 2 * SPAN, 128), ('z', 'x', 'y')...  14.9 us
    all_to_all x1, starting transfers between devices, shards(): lax.all_to_all(sent.reshape(experts, 2 * SPAN, width), sp, 0, 0, tiled=True)  13.2 us
    ppermute x6, starting transfers between devices, flip_c(): return lax.ppermute(value, 'c', [(0, 1), (1, 0)])  11.5 us
    all_to_all x1, waiting for transfers between devices, shards(): lax.all_to_all(jnp.broadcast_to(mix[None], (ny, *mix.shape)), 'y', 0, 0,...  9.91 us
  transfers between devices with their start and end apart: 16, of which 11 were waited for; matrix products, arithmetic and copies ran while one was open for 7% of the time, Pallas kernels for 4%

profile of v2, /device:TPU:8, one launch (start us, length us, event | category | flops | bytes accessed | tf_op | source)
XLA Modules:
  0.0 193.2 jit_solution(11534571797644056424)
XLA Ops:
  0.7 2.7 %shard_map.156.w0 = bf16[3,2048,128]{2,1,0:T(8,128)(2,1)} custom-call(bf16[2048,128]{1,0:T(8,128)(2,1)} %bitcast.92, bf16[2048,128]{1,0:T(8,128)(2,1)} %bitcast.93, bf16[128,2048]{1,0:T(8,128)(2,1)} %bitcast.94), custom_call_target="tpu_custom_call" | custom-call | flops 1000000 | bytes 1048576 | tf_op jit(solution)/shard_map/pallas_call | solution.py:24
  3.4 3.5 %collective-permute-start.1 = (bf16[3,2048,128]{2,1,0:T(8,128)(2,1)}, bf16[3,2048,128]{2,1,0:T(8,128)(2,1)}, u32[]{:S(2)}, u32[]{:S(2)}) collective-permute-start(bf16[3,2048,128]{2,1,0:T(8,128)(2,1)} %shard_map.156.w0), channel_id=1, source_target_pairs={{0,2},{1,15},{2,4},{3,1},{4,6},{5,3},{6,8},{7,5},{8,10},{9,7},{10,... | collective-permute-start | bytes 4718600 | tf_op jit(solution)/shard_map/ppermute | solution.py:198
  8.3 3.3 %shard_map.155 = bf16[256,2048]{1,0:T(8,128)(2,1)} custom-call(s32[128,2]{1,0:T(8,128)} %copy.18.ids_ref, f32[128,2]{1,0:T(8,128)} %copy.19.weight_ref, bf16[128,2048]{1,0:T(8,128)(2,1)} %mix_ref.1, bf16[128,2048]{1,0:T(8,128)(2,1)} %cot_ref.1), custom_call_target="tpu_custom_call" | custom-call | flops 2000000000 | bytes 1048576 | tf_op jit(solution)/shard_map/pallas_call | solution.py:24
  11.7 13.2 %all-to-all-start = ((bf16[32,8,2048]{2,1,0:T(8,128)(2,1)}), bf16[32,8,2048]{2,1,0:T(8,128)(2,1)S(1)}, u32[]{:S(2)}, u32[]{:S(2)}) async-start(bf16[32,8,2048]{2,1,0:T(8,128)(2,1)} %bitcast.90), calls=%async_computation | async-start | bytes 2097152 | tf_op jit(solution)/shard_map/all_to_all | solution.py:209
  26.8 3.0 %collective-permute-done.1.w2 = bf16[3,2048,128]{2,1,0:T(8,128)(2,1)} collective-permute-done((bf16[3,2048,128]{2,1,0:T(8,128)(2,1)}, bf16[3,2048,128]{2,1,0:T(8,128)(2,1)}, u32[]{:S(2)}, u32[]{:S(2)}) %collective-permute-start.1) | collective-permute-done | bytes 1572896 | tf_op jit(solution)/shard_map/ppermute | solution.py:198
  31.7 19.8 %all-to-all-done = bf16[32,8,2048]{2,1,0:T(8,128)(2,1)S(1)} async-done(((bf16[32,8,2048]{2,1,0:T(8,128)(2,1)}), bf16[32,8,2048]{2,1,0:T(8,128)(2,1)S(1)}, u32[]{:S(2)}, u32[]{:S(2)}) %all-to-all-start) | async-done | bytes 1048608 | tf_op jit(solution)/shard_map/all_to_all | solution.py:209
  52.4 9.5 %shard_map.157 = (bf16[128,2048]{1,0:T(8,128)(2,1)}, bf16[128,2048]{1,0:T(8,128)(2,1)}, bf16[3,128,512]{2,1,0:T(8,128)(2,1)}, bf16[16,128,128]{2,1,0:T(8,128)(2,1)}) custom-call(bf16[256,2048]{1,0:T(8,128)(2,1)} %bitcast.89, bf16[3,2048,128]{2,1,0:T(8,128)(2,1)} %shard_map.156.w0, bf16[3,2048,128]{2,1,0:T(8,128)(2,1)} %collective-permute-done.w1, ...), custom_call_target="tpu_custom_call" | custom-call | flops 4000000000 | bytes 1048576 | tf_op jit(solution)/shard_map/pallas_call | solution.py:24
  62.0 5.8 %shard_map.160 = (bf16[2,3,2048,128]{3,2,1,0:T(8,128)(2,1)}, bf16[2,3,2048,128]{3,2,1,0:T(8,128)(2,1)}) custom-call(bf16[128,2048]{1,0:T(8,128)(2,1)} %get-tuple-element.18.x_ref, bf16[128,2048]{1,0:T(8,128)(2,1)} %get-tuple-element.19.g_ref, bf16[3,128,512]{2,1,0:T(8,128)(2,1)} %get-tuple-element.20.hid_ref), custom_call_target="tpu_custom_call" | custom-call | flops 8000000000 | bytes 1048576 | tf_op jit(solution)/shard_map/pallas_call | solution.py:24
  69.7 14.9 %all-to-all-start.1 = ((bf16[256,8,128]{2,1,0:T(8,128)(2,1)}), bf16[256,8,128]{2,1,0:T(8,128)(2,1)}, u32[]{:S(2)}, u32[]{:S(2)}) async-start(bf16[256,8,128]{2,1,0:T(8,128)(2,1)} %bitcast.6), calls=%async_computation.1 | async-start | bytes 1048576 | tf_op jit(solution)/shard_map/all_to_all | solution.py:229
  84.6 2.4 %shard_map.158 = bf16[256,2048]{1,0:T(8,128)(2,1)} custom-call(s32[128,2]{1,0:T(8,128)} %copy.18.ids_ref), custom_call_target="tpu_custom_call" | custom-call | flops 2000000000 | bytes 1048576 | tf_op jit(solution)/shard_map/pallas_call | solution.py:24
  87.1 18.6 %all-to-all-done.1 = bf16[256,8,128]{2,1,0:T(8,128)(2,1)} async-done(((bf16[256,8,128]{2,1,0:T(8,128)(2,1)}), bf16[256,8,128]{2,1,0:T(8,128)(2,1)}, u32[]{:S(2)}, u32[]{:S(2)}) %all-to-all-start.1) | async-done | bytes 524320 | tf_op jit(solution)/shard_map/all_to_all | solution.py:229
  111.6 5.4 %all-to-all-start.2 = ((bf16[8,128,128]{2,1,0:T(8,128)(2,1)}), bf16[8,128,128]{2,1,0:T(8,128)(2,1)}, u32[]{:S(2)}, u32[]{:S(2)}) async-start(bf16[8,128,128]{2,1,0:T(8,128)(2,1)} %broadcast_in_dim.2), calls=%async_computation.2 | async-start | bytes 524288 | tf_op jit(solution)/shard_map/all_to_all | solution.py:245
  118.3 9.9 %all-to-all-done.2.mine_ref = bf16[8,128,128]{2,1,0:T(8,128)(2,1)} async-done(((bf16[8,128,128]{2,1,0:T(8,128)(2,1)}), bf16[8,128,128]{2,1,0:T(8,128)(2,1)}, u32[]{:S(2)}, u32[]{:S(2)}) %all-to-all-start.2) | async-done | bytes 262176 | tf_op jit(solution)/shard_map/all_to_all | solution.py:245
  130.1 3.0 %fusion.1 = bf16[3,2048,128]{2,1,0:T(8,128)(2,1)} fusion(bf16[2,3,2048,128]{3,2,1,0:T(8,128)(2,1)} %collective-permute-done.10, bf16[2,3,2048,128]{3,2,1,0:T(8,128)(2,1)S(1)} %copy-done), kind=kLoop, calls=%fused_computation.3 | loop fusion | flops 3145728 | bytes 4718592 | tf_op jit(solution)/shard_map/convert_element_type | solution.py:236
  133.2 3.4 %collective-permute-start.11 = (bf16[3,2048,128]{2,1,0:T(8,128)(2,1)}, bf16[3,2048,128]{2,1,0:T(8,128)(2,1)}, u32[]{:S(2)}, u32[]{:S(2)}) collective-permute-start(bf16[3,2048,128]{2,1,0:T(8,128)(2,1)} %fusion.1), channel_id=1, source_target_pairs={{0,14},{1,3},{2,0},{3,5},{4,2},{5,7},{6,4},{7,9},{8,6},{9,11},{10,... | collective-permute-start | bytes 4718600 | tf_op jit(solution)/shard_map/ppermute | solution.py:198
  137.3 2.7 %shard_map.159 = (bf16[2048,128]{1,0:T(8,128)(2,1)}, f32[128,128]{1,0:T(8,128)}, f32[2,128]{1,0:T(2,128)}) custom-call(bf16[8,128,128]{2,1,0:T(8,128)(2,1)} %all-to-all-done.2.mine_ref, bf16[8,128,128]{2,1,0:T(8,128)(2,1)} %copy-done.9, bf16[128,2048]{1,0:T(8,128)(2,1)} %proj_ref.1, bf16[128,128]{1,0:T(8,128)(2,1)} %get-tuple-element.27.act_ref, ...), custom_call_target="tpu_custom_call" | custom-call | flops 2000000000 | bytes 1048576 | tf_op jit(solution)/shard_map/pallas_call | solution.py:24
  143.9 2.3 %collective-permute-start.6 = (f32[2,128]{1,0:T(2,128)S(1)}, f32[2,128]{1,0:T(2,128)S(1)}, u32[]{:S(2)}, u32[]{:S(2)}) collective-permute-start(f32[2,128]{1,0:T(2,128)S(1)} %add.139), channel_id=1, source_target_pairs={{0,2},{2,0},{4,6},{6,4},{8,10},{10,8},{12,14},{14,12},{1,3},{3,1},... | collective-permute-start | bytes 3080 | tf_op jit(solution)/shard_map/ppermute | solution.py:264
  146.2 8.5 %collective-permute-done.6 = f32[2,128]{1,0:T(2,128)S(1)} collective-permute-done((f32[2,128]{1,0:T(2,128)S(1)}, f32[2,128]{1,0:T(2,128)S(1)}, u32[]{:S(2)}, u32[]{:S(2)}) %collective-permute-start.6) | collective-permute-done | bytes 1056 | tf_op jit(solution)/shard_map/ppermute | solution.py:264
  156.7 4.4 %collective-permute-done.7 = f32[2,128]{1,0:T(2,128)S(1)} collective-permute-done((f32[2,128]{1,0:T(2,128)S(1)}, f32[2,128]{1,0:T(2,128)S(1)}, u32[]{:S(2)}, u32[]{:S(2)}) %collective-permute-start.7) | collective-permute-done | bytes 1056 | tf_op jit(solution)/shard_map/ppermute | solution.py:264
  161.1 2.4 %collective-permute-start.8 = (f32[2,128]{1,0:T(2,128)S(1)}, f32[2,128]{1,0:T(2,128)S(1)}, u32[]{:S(2)}, u32[]{:S(2)}) collective-permute-start(f32[2,128]{1,0:T(2,128)S(1)} %add.141), channel_id=1, source_target_pairs={{0,8},{2,10},{4,12},{6,14},{8,0},{10,2},{12,4},{14,6},{1,9},{3,11}... | collective-permute-start | bytes 3080 | tf_op jit(solution)/shard_map/ppermute | solution.py:264
  163.6 4.6 %all-to-all-start.3 = ((bf16[32,64,128]{2,1,0:T(8,128)(2,1)}), bf16[32,64,128]{2,1,0:T(8,128)(2,1)}, u32[]{:S(2)}, u32[]{:S(2)}) async-start(bf16[32,64,128]{2,1,0:T(8,128)(2,1)} %bitcast.91), calls=%async_computation.3 | async-start | bytes 1048576 | tf_op jit(solution)/shard_map/all_to_all | solution.py:259
  172.8 4.6 %collective-permute-done.9 = f32[30,128]{1,0:T(8,128)S(1)} collective-permute-done((f32[30,128]{1,0:T(8,128)S(1)}, f32[30,128]{1,0:T(8,128)S(1)}, u32[]{:S(2)}, u32[]{:S(2)}) %collective-permute-start.9) | collective-permute-done | bytes 15392 | tf_op jit(solution)/shard_map/ppermute | solution.py:270
  178.3 8.3 %all-to-all-done.3 = bf16[32,64,128]{2,1,0:T(8,128)(2,1)} async-done(((bf16[32,64,128]{2,1,0:T(8,128)(2,1)}), bf16[32,64,128]{2,1,0:T(8,128)(2,1)}, u32[]{:S(2)}, u32[]{:S(2)}) %all-to-all-start.3) | async-done | bytes 524320 | tf_op jit(solution)/shard_map/all_to_all | solution.py:259
  188.3 2.5 %fusion = bf16[3,2048,128]{2,1,0:T(8,128)(2,1)S(1)} fusion(bf16[3,2048,128]{2,1,0:T(8,128)(2,1)} %collective-permute-done.11, bf16[2,3,2048,128]{3,2,1,0:T(8,128)(2,1)} %collective-permute-done.10, bf16[2,3,2048,128]{3,2,1,0:T(8,128)(2,1)S(1)} %copy-done), kind=kLoop, calls=%fused_computation.1 | loop fusion | flops 4718592 | bytes 6291456 | tf_op jit(solution)/shard_map/convert_element_type | solution.py:237
  (61 shorter events, 33.3 us)
Async XLA Ops:
  0.6 6.2 %copy-start.5 = (s32[128,2]{0,1:T(2,128)S(1)}, s32[128,2]{0,1:T(2,128)}, u32[]{:S(2)}) copy-start(s32[128,2]{0,1:T(2,128)} %param.14) | copy-start | bytes 3076
  0.6 6.9 %copy-start.6 = (f32[128,2]{0,1:T(2,128)S(1)}, f32[128,2]{0,1:T(2,128)}, u32[]{:S(2)}) copy-start(f32[128,2]{0,1:T(2,128)} %param.15) | copy-start | bytes 3076
  3.4 26.4 %collective-permute-start.1 = (bf16[3,2048,128]{2,1,0:T(8,128)(2,1)}, bf16[3,2048,128]{2,1,0:T(8,128)(2,1)}, u32[]{:S(2)}, u32[]{:S(2)}) collective-permute-start(bf16[3,2048,128]{2,1,0:T(8,128)(2,1)} %shard_map.156.w0), channel_id=1, source_target_pairs={{0,2},{1,15},{2,4},{3,1},{4,6},{5,3},{6,8},{7,5},{8,10},{9,7},{10,... | collective-permute-start | bytes 4718600 | tf_op jit(solution)/shard_map/ppermute | solution.py:198
  8.3 16.5 %copy-start.1 = (bf16[3,2048,128]{2,1,0:T(8,128)(2,1)S(1)}, bf16[3,2048,128]{2,1,0:T(8,128)(2,1)}, u32[]{:S(2)}) copy-start(bf16[3,2048,128]{2,1,0:T(8,128)(2,1)} %shard_map.156.w0) | copy-start | bytes 4718596
  11.7 39.8 %all-to-all-start = ((bf16[32,8,2048]{2,1,0:T(8,128)(2,1)}), bf16[32,8,2048]{2,1,0:T(8,128)(2,1)S(1)}, u32[]{:S(2)}, u32[]{:S(2)}) async-start(bf16[32,8,2048]{2,1,0:T(8,128)(2,1)} %bitcast.90), calls=%async_computation | async-start | bytes 2097152 | tf_op jit(solution)/shard_map/all_to_all | solution.py:209
  24.9 6.8 %collective-permute-start = (bf16[3,2048,128]{2,1,0:T(8,128)(2,1)S(1)}, bf16[3,2048,128]{2,1,0:T(8,128)(2,1)}, u32[]{:S(2)}, u32[]{:S(2)}) collective-permute-start(bf16[3,2048,128]{2,1,0:T(8,128)(2,1)S(1)} %copy-done.1), channel_id=1, source_target_pairs={{0,1},{1,0},{2,3},{3,2},{4,5},{5,4},{6,7},{7,6},{8,9},{9,8},{10,11... | collective-permute-start | bytes 4718600 | tf_op jit(solution)/shard_map/ppermute | solution.py:191
  29.8 21.7 %collective-permute-start.2 = (bf16[3,2048,128]{2,1,0:T(8,128)(2,1)}, bf16[3,2048,128]{2,1,0:T(8,128)(2,1)}, u32[]{:S(2)}, u32[]{:S(2)}) collective-permute-start(bf16[3,2048,128]{2,1,0:T(8,128)(2,1)} %collective-permute-done.1.w2), channel_id=1, source_target_pairs={{0,1},{1,0},{2,3},{3,2},{4,5},{5,4},{6,7},{7,6},{8,9},{9,8},{10,11... | collective-permute-start | bytes 4718600 | tf_op jit(solution)/shard_map/ppermute | solution.py:191
  67.8 62.4 %collective-permute-start.10 = (bf16[2,3,2048,128]{3,2,1,0:T(8,128)(2,1)}, bf16[2,3,2048,128]{3,2,1,0:T(8,128)(2,1)}, u32[]{:S(2)}, u32[]{:S(2)}) collective-permute-start(bf16[2,3,2048,128]{3,2,1,0:T(8,128)(2,1)} %get-tuple-element.22), channel_id=1, source_target_pairs={{0,1},{1,0},{2,3},{3,2},{4,5},{5,4},{6,7},{7,6},{8,9},{9,8},{10,11... | collective-permute-start | bytes 9437192 | tf_op jit(solution)/shard_map/ppermute | solution.py:191
  69.7 36.0 %all-to-all-start.1 = ((bf16[256,8,128]{2,1,0:T(8,128)(2,1)}), bf16[256,8,128]{2,1,0:T(8,128)(2,1)}, u32[]{:S(2)}, u32[]{:S(2)}) async-start(bf16[256,8,128]{2,1,0:T(8,128)(2,1)} %bitcast.6), calls=%async_computation.1 | async-start | bytes 1048576 | tf_op jit(solution)/shard_map/all_to_all | solution.py:229
  84.6 32.4 %copy-start.3 = (bf16[128,128]{1,0:T(8,128)(2,1)S(1)}, bf16[128,128]{1,0:T(8,128)(2,1)}, u32[]{:S(2)}) copy-start(bf16[128,128]{1,0:T(8,128)(2,1)} %param.16) | copy-start | bytes 98308
  84.6 33.0 %copy-start.7 = (f32[128]{0:T(128)S(1)}, f32[128]{0:T(128)}, u32[]{:S(2)}) copy-start(f32[128]{0:T(128)} %param.18) | copy-start | bytes 1540
  87.1 43.1 %copy-start = (bf16[2,3,2048,128]{3,2,1,0:T(8,128)(2,1)S(1)}, bf16[2,3,2048,128]{3,2,1,0:T(8,128)(2,1)}, u32[]{:S(2)}) copy-start(bf16[2,3,2048,128]{3,2,1,0:T(8,128)(2,1)} %get-tuple-element.21) | copy-start | bytes 9437188
  107.6 3.1 %collective-permute-start.3 = (bf16[128,128]{0,1:T(8,128)(2,1)S(1)}, bf16[128,128]{0,1:T(8,128)(2,1)S(1)}, u32[]{:S(2)}, u32[]{:S(2)}) collective-permute-start(bf16[128,128]{0,1:T(8,128)(2,1)S(1)} %slice.796), channel_id=1, source_target_pairs={{0,1},{1,0},{2,3},{3,2},{4,5},{5,4},{6,7},{7,6},{8,9},{9,8},{10,11... | collective-permute-start | bytes 98312 | tf_op jit(solution)/shard_map/ppermute | solution.py:191
  111.6 16.6 %all-to-all-start.2 = ((bf16[8,128,128]{2,1,0:T(8,128)(2,1)}), bf16[8,128,128]{2,1,0:T(8,128)(2,1)}, u32[]{:S(2)}, u32[]{:S(2)}) async-start(bf16[8,128,128]{2,1,0:T(8,128)(2,1)} %broadcast_in_dim.2), calls=%async_computation.2 | async-start | bytes 524288 | tf_op jit(solution)/shard_map/all_to_all | solution.py:245
  128.2 8.3 %collective-permute-start.4 = (bf16[8,128,128]{2,1,0:T(8,128)(2,1)}, bf16[8,128,128]{2,1,0:T(8,128)(2,1)S(1)}, u32[]{:S(2)}, u32[]{:S(2)}) collective-permute-start(bf16[8,128,128]{2,1,0:T(8,128)(2,1)} %all-to-all-done.2.mine_ref), channel_id=1, source_target_pairs={{0,1},{1,0},{2,3},{3,2},{4,5},{5,4},{6,7},{7,6},{8,9},{9,8},{10,11... | collective-permute-start | bytes 786440 | tf_op jit(solution)/shard_map/ppermute | solution.py:191
  133.2 55.1 %collective-permute-start.11 = (bf16[3,2048,128]{2,1,0:T(8,128)(2,1)}, bf16[3,2048,128]{2,1,0:T(8,128)(2,1)}, u32[]{:S(2)}, u32[]{:S(2)}) collective-permute-start(bf16[3,2048,128]{2,1,0:T(8,128)(2,1)} %fusion.1), channel_id=1, source_target_pairs={{0,14},{1,3},{2,0},{3,5},{4,2},{5,7},{6,4},{7,9},{8,6},{9,11},{10,... | collective-permute-start | bytes 4718600 | tf_op jit(solution)/shard_map/ppermute | solution.py:198
  137.3 26.3 %copy-start.4 = (f32[31,128]{1,0:T(8,128)S(1)}, f32[31,128]{1,0:T(8,128)}, u32[]{:S(2)}) copy-start(f32[31,128]{1,0:T(8,128)} %param.19) | copy-start | bytes 47620
  137.3 33.3 %copy-start.8 = (f32[128]{0:T(128)S(1)}, f32[128]{0:T(128)}, u32[]{:S(2)}) copy-start(f32[128]{0:T(128)} %param.17) | copy-start | bytes 1540
  140.0 3.3 %collective-permute-start.5 = (f32[2,128]{1,0:T(2,128)}, f32[2,128]{1,0:T(2,128)S(1)}, u32[]{:S(2)}, u32[]{:S(2)}) collective-permute-start(f32[2,128]{1,0:T(2,128)} %get-tuple-element.16), channel_id=1, source_target_pairs={{0,1},{1,0},{2,3},{3,2},{4,5},{5,4},{6,7},{7,6},{8,9},{9,8},{10,11... | collective-permute-start | bytes 3080 | tf_op jit(solution)/shard_map/ppermute | solution.py:191
  143.9 10.9 %collective-permute-start.6 = (f32[2,128]{1,0:T(2,128)S(1)}, f32[2,128]{1,0:T(2,128)S(1)}, u32[]{:S(2)}, u32[]{:S(2)}) collective-permute-start(f32[2,128]{1,0:T(2,128)S(1)} %add.139), channel_id=1, source_target_pairs={{0,2},{2,0},{4,6},{6,4},{8,10},{10,8},{12,14},{14,12},{1,3},{3,1},... | collective-permute-start | bytes 3080 | tf_op jit(solution)/shard_map/ppermute | solution.py:264
  154.8 6.4 %collective-permute-start.7 = (f32[2,128]{1,0:T(2,128)S(1)}, f32[2,128]{1,0:T(2,128)S(1)}, u32[]{:S(2)}, u32[]{:S(2)}) collective-permute-start(f32[2,128]{1,0:T(2,128)S(1)} %add.140), channel_id=1, source_target_pairs={{0,4},{2,6},{4,0},{6,2},{8,12},{10,14},{12,8},{14,10},{1,5},{3,7},... | collective-permute-start | bytes 3080 | tf_op jit(solution)/shard_map/ppermute | solution.py:264
  161.1 9.4 %collective-permute-start.8 = (f32[2,128]{1,0:T(2,128)S(1)}, f32[2,128]{1,0:T(2,128)S(1)}, u32[]{:S(2)}, u32[]{:S(2)}) collective-permute-start(f32[2,128]{1,0:T(2,128)S(1)} %add.141), channel_id=1, source_target_pairs={{0,8},{2,10},{4,12},{6,14},{8,0},{10,2},{12,4},{14,6},{1,9},{3,11}... | collective-permute-start | bytes 3080 | tf_op jit(solution)/shard_map/ppermute | solution.py:264
  163.6 22.9 %all-to-all-start.3 = ((bf16[32,64,128]{2,1,0:T(8,128)(2,1)}), bf16[32,64,128]{2,1,0:T(8,128)(2,1)}, u32[]{:S(2)}, u32[]{:S(2)}) async-start(bf16[32,64,128]{2,1,0:T(8,128)(2,1)} %bitcast.91), calls=%async_computation.3 | async-start | bytes 1048576 | tf_op jit(solution)/shard_map/all_to_all | solution.py:259
  171.5 6.0 %collective-permute-start.9 = (f32[30,128]{1,0:T(8,128)S(1)}, f32[30,128]{1,0:T(8,128)S(1)}, u32[]{:S(2)}, u32[]{:S(2)}) collective-permute-start(f32[30,128]{1,0:T(8,128)S(1)} %slice.295), channel_id=1, source_target_pairs={{16,0},{32,16},{48,32},{64,48},{80,64},{96,80},{112,96},{128,112},... | collective-permute-start | bytes 46088 | tf_op jit(solution)/shard_map/ppermute | solution.py:270
  (2 other events, 1.7 us)

commit v3 on v2

--- a/solution.py
+++ b/solution.py
@@ -5,11 +5,13 @@
 from jax.experimental.pallas import tpu as pltpu
 from jax.sharding import Mesh, PartitionSpec as P
 
+
 BF, F32, I32 = jnp.bfloat16, jnp.float32, jnp.int32
 LAST = (((1,), (1,)), ((), ()))
 FIRST = (((0,), (0,)), ((), ()))
 SPAN = 4
 VMEM = pl.BlockSpec(memory_space=pltpu.VMEM)
+ANY = pl.BlockSpec(memory_space=pl.ANY)
 
 
 def mm(a, b, dims=(((1,), (0,)), ((), ()))):
@@ -20,11 +22,12 @@
     return lax.broadcasted_iota(I32, shape, dim)
 
 
-def kernel(body, outs, flops, *args):
+def kernel(body, outs, flops, *args, scratch=(), far=()):
     return pl.pallas_call(
         body,
         out_shape=outs,
-        in_specs=[VMEM] * len(args),
+        in_specs=[ANY if i in far else VMEM for i in range(len(args))],
+        scratch_shapes=list(scratch),
         out_specs=jax.tree.map(lambda _: VMEM, outs),
         cost_estimate=pl.CostEstimate(flops=flops, bytes_accessed=1 << 20, transcendentals=0),
     )(*args)
@@ -35,11 +38,11 @@
 
 
 def head_body(ids_ref, weight_ref, mix_ref, cot_ref, out_ref):
-    tok = ids_ref.shape[0]
+    tok = ids_ref.shape[1]
     experts = out_ref.shape[0] // (2 * SPAN)
     group = (lax.axis_index("y") % 2) * 2 + lax.axis_index("c")
-    ids = [jnp.broadcast_to(ids_ref[:, k : k + 1], (tok, tok)).T[:1] for k in range(2)]
-    wts = [jnp.broadcast_to(weight_ref[:, k : k + 1], (tok, tok)).T[:1] for k in range(2)]
+    ids = [ids_ref[k : k + 1, :] for k in range(2)]
+    wts = [weight_ref[k : k + 1, :] for k in range(2)]
     expert = iota((experts, tok), 0)
     hot = [(expert == i).astype(F32) for i in ids]
     after = (iota((tok, tok), 0) < iota((tok, tok), 1)).astype(BF)
@@ -67,14 +70,15 @@
 
 
 def table_body(ids_ref, out_ref):
-    tok = ids_ref.shape[0]
+    tok = ids_ref.shape[1]
     ci = lax.axis_index("c")
     cols = out_ref.shape[1]
     experts = cols // 64
     lane = iota((tok, experts), 1)
     hot = jnp.zeros((tok, experts), F32)
     for k in range(2):
-        hot = hot + (lane == ids_ref[:, k : k + 1]).astype(F32)
+        ids = jnp.broadcast_to(ids_ref[k : k + 1, :].astype(F32), (tok, tok)).T
+        hot = hot + (lane == ids[:, :experts].astype(I32)).astype(F32)
     before = (iota((tok, tok), 0) > iota((tok, tok), 1)).astype(BF)
     slot = jnp.where(hot > 0, mm(before, hot.astype(BF)), -1.0)
     spread = (iota((experts, cols), 1) // 64 == iota((experts, cols), 0)).astype(BF)
@@ -94,9 +98,22 @@
         out_ref[2, j * 128 : (j + 1) * 128, :] = down_ref[:, j * 128 : (j + 1) * 128]
 
 
-def expert_body(got_ref, w0, w1, w2, w3, x_ref, g_ref, hid_ref, back_ref):
+def expert_body(got_ref, w0, w1, w2, w3, x_ref, g_ref, hid_ref, back_ref, in_ref, down_ref, sem):
     rows, width = got_ref.shape
     slots = rows // 2
+    copies = []
+    for q, w in enumerate((w0, w1, w2, w3)):
+        three = []
+        for m in range(2):
+            at = (2 * q + m) * 128
+            three.append(pltpu.make_async_copy(w.at[m], in_ref.at[:, at : at + 128], sem.at[q, m]))
+        down = w.at[2].reshape(width // 128, 128, 128)
+        three.append(
+            pltpu.make_async_copy(down, down_ref.at[:, q * 128 : (q + 1) * 128, :], sem.at[q, 2])
+        )
+        for copy in three:
+            copy.start()
+        copies.append(three)
     out_row, in_row = iota((slots, rows), 0), iota((slots, rows), 1)
     want = (out_row // SPAN) * (2 * SPAN) + out_row % SPAN
     pick_x = (in_row == want).astype(BF)
@@ -105,31 +122,27 @@
         part = got_ref[:, at : at + 512]
         x_ref[:, at : at + 512] = mm(pick_x, part).astype(BF)
         g_ref[:, at : at + 512] = mm(pick_g, part).astype(BF)
-    for q, w in enumerate((w0, w1, w2, w3)):
-        hg = mm(x_ref[...], w[0])
-        hu = mm(x_ref[...], w[1])
+    for q in range(4):
+        for copy in copies[q]:
+            copy.wait()
+        both = mm(x_ref[...], in_ref[:, q * 256 : (q + 1) * 256])
+        hg, hu = both[:, :128], both[:, 128:]
         gact = jnp.zeros((slots, 128), F32)
-        for j in range(width // 128):
+        for j in range(0, width // 128, 2):
+            blocks = [down_ref[j + i, q * 128 : (q + 1) * 128, :] for i in range(2)]
             gact = gact + mm(
-                g_ref[:, j * 128 : (j + 1) * 128], w[2, j * 128 : (j + 1) * 128, :], LAST
+                g_ref[:, j * 128 : (j + 2) * 128], jnp.concatenate(blocks, axis=1), LAST
             )
         sigma = jax.nn.sigmoid(hg)
         swish = hg * sigma
-        lanes = slice(q * 128, (q + 1) * 128)
-        hid_ref[0, :, lanes] = (gact * hu * sigma * (1.0 + hg * (1.0 - sigma))).astype(BF)
-        hid_ref[1, :, lanes] = (gact * swish).astype(BF)
-        hid_ref[2, :, lanes] = (swish * hu).astype(BF)
+        at = q * 256
+        hid_ref[:, at : at + 128] = (gact * hu * sigma * (1.0 + hg * (1.0 - sigma))).astype(BF)
+        hid_ref[:, at + 128 : at + 256] = (gact * swish).astype(BF)
+        hid_ref[:, 1024 + q * 128 : 1152 + q * 128] = (swish * hu).astype(BF)
     low = iota((slots, 128), 0) % (2 * SPAN) < SPAN
     for y in range(width // 256):
-        pair = []
-        for h in range(2):
-            at = (y * 2 + h) * 128
-            acc = jnp.zeros((slots, 128), F32)
-            for q, w in enumerate((w0, w1, w2, w3)):
-                lanes = slice(q * 128, (q + 1) * 128)
-                acc = acc + mm(hid_ref[0, :, lanes], w[0, at : at + 128, :], LAST)
-                acc = acc + mm(hid_ref[1, :, lanes], w[1, at : at + 128, :], LAST)
-            pair.append(acc)
+        both = mm(hid_ref[:, :1024], in_ref[y * 256 : (y + 1) * 256, :], LAST)
+        pair = [both[:, :128], both[:, 128:]]
         even = jnp.where(low, pair[0], pltpu.roll(pair[1], SPAN, 0))
         odd = jnp.where(low, pltpu.roll(pair[0], slots - SPAN, 0), pair[1])
         back_ref[:, y * 8 : (y + 1) * 8, :] = even.reshape(-1, 8, 128).astype(BF)
@@ -138,17 +151,30 @@
 
 def grads_body(x_ref, g_ref, hid_ref, keep_ref, give_ref):
     width = x_ref.shape[1]
+    places = ((keep_ref, 0), (give_ref, 0), (keep_ref, 1), (give_ref, 1))
     for j in range(width // 128):
         at = slice(j * 128, (j + 1) * 128)
-        xt, gt = x_ref[:, at], g_ref[:, at]
-        for m in range(3):
-            h = hid_ref[m]
-            both = mm(xt, h, FIRST) if m < 2 else mm(h, gt, FIRST)
-            for q in range(4):
-                ref, to = ((keep_ref, 0), (give_ref, 0), (keep_ref, 1), (give_ref, 1))[q]
-                cut = slice(q * 128, (q + 1) * 128)
-                piece = both[:, cut] if m < 2 else both[cut, :]
-                ref[to, m, at, :] = piece.astype(BF)
+        both = mm(x_ref[:, at], hid_ref[:, :1024], FIRST)
+        down = mm(hid_ref[:, 1024:], g_ref[:, at], FIRST)
+        for q, (ref, to) in enumerate(places):
+            ref[to, 0, at, :] = both[:, q * 256 : q * 256 + 128].astype(BF)
+            ref[to, 1, at, :] = both[:, q * 256 + 128 : (q + 1) * 256].astype(BF)
+            ref[to, 2, at, :] = down[q * 128 : (q + 1) * 128, :].astype(BF)
+
+
+def combine_body(table_ref, home_ref, cot_ref, own_ref, other_ref):
+    tok = cot_ref.shape[0]
+    place = lax.axis_index("y") * 2 + lax.axis_index("c")
+    cot = cot_ref[:, pl.ds(pl.multiple_of(place * 128, 128), 128)].astype(F32)
+    both = mm(table_ref[...], home_ref[...])
+    own_ref[...] = both[:tok] + cot
+    other_ref[...] = both[tok:].astype(BF)
+
+
+def mix_body(own_ref, other_ref, out_ref):
+    mix = (own_ref[...] + other_ref[...].astype(F32)).astype(BF)
+    for y in range(out_ref.shape[0]):
+        out_ref[y] = mix
 
 
 def final_body(mine_ref, other_ref, proj_ref, act_ref, slope_ref, norm_ref, out_ref, grad_ref, sum_ref):
@@ -184,7 +210,6 @@
     sp = ("z", "x")
     experts = lax.axis_size(sp)
     ny = lax.axis_size("y")
-    yi, ci = lax.axis_index("y"), lax.axis_index("c")
     tok, width = cotangent.shape
 
     def flip_c(value):
@@ -197,17 +222,20 @@
                 pairs.append((2 * y + c, 2 * ((y + (sign if c == 0 else -sign)) % ny) + c))
         return lax.ppermute(value, ("y", "c"), pairs)
 
-    own = kernel(pack_body, shape(3, width, 128), 1000000, gate_weight[0], up_weight[0], down_weight[0])
+    own = kernel(
+        pack_body, shape(3, width, 128), 1000000, gate_weight[0], up_weight[0], down_weight[0]
+    )
     by_y = hop(own, 1)
     by_c = flip_c(own)
     by_yc = flip_c(by_y)
 
     rows = experts * 2 * SPAN
+    ids, weights = expert_ids.T, route_weight.T
     sent = kernel(
-        head_body, shape(rows, width), 2000000000, expert_ids, route_weight, mixer_out, cotangent
+        head_body, shape(rows, width), 2000000000, ids, weights, mixer_out, cotangent
     )
     got = lax.all_to_all(sent.reshape(experts, 2 * SPAN, width), sp, 0, 0, tiled=True)
-    table = kernel(table_body, shape(2 * tok, experts * ny * 2 * SPAN), 2000000000, expert_ids)
+    table = kernel(table_body, shape(2 * tok, experts * ny * 2 * SPAN), 2000000000, ids)
 
     normalized = saved_normalized.astype(F32)
     values = normalized * channel_norm_gain[None, :]
@@ -218,13 +246,19 @@
     slots = experts * SPAN
     x, g, hidden, back = kernel(
         expert_body,
-        (shape(slots, width), shape(slots, width), shape(3, slots, 512), shape(experts // 2, 128, 128)),
+        (shape(slots, width), shape(slots, width), shape(slots, 1536), shape(experts // 2, 128, 128)),
         4000000000,
         got.reshape(rows, width),
         own,
         by_c,
         by_y,
         by_yc,
+        far=(1, 2, 3, 4),
+        scratch=(
+            pltpu.VMEM((width, 1024), BF),
+            pltpu.VMEM((width // 128, 512, 128), BF),
+            pltpu.SemaphoreType.DMA((4, 3)),
+        ),
     )
     home = lax.all_to_all(
         back.reshape(experts * ny, 2 * SPAN, 128), ("z", "x", "y"), 0, 0, tiled=True
@@ -233,16 +267,22 @@
     packed = shape(2, 3, width, 128)
     keep, give = kernel(grads_body, (packed, packed), 8000000000, x, g, hidden)
     given = flip_c(give)
-    passed = hop((keep[1].astype(F32) + given[1].astype(F32)).astype(BF), -1)
+    passing = (keep[1].astype(F32) + given[1].astype(F32)).astype(BF)
+    passed = hop(passing, -1)
     final = (keep[0].astype(F32) + given[0].astype(F32) + passed.astype(F32)).astype(BF)
     grad_down = final[2].reshape(-1, 128, 128).transpose(1, 0, 2).reshape(128, width)
 
-    combined = mm(table, home)
-    other = flip_c(combined[tok:].astype(BF))
-    feat = (yi * 2 + ci) * 128
-    cot = lax.dynamic_slice_in_dim(cotangent, feat, 128, axis=1)
-    mix = (cot.astype(F32) + combined[:tok] + other.astype(F32)).astype(BF)
-    mine_all = lax.all_to_all(jnp.broadcast_to(mix[None], (ny, *mix.shape)), "y", 0, 0, tiled=True)
+    mine, other = kernel(
+        combine_body,
+        (shape(tok, 128, kind=F32), shape(tok, 128)),
+        200000000,
+        table,
+        home,
+        cotangent,
+    )
+    other = flip_c(other)
+    mix = kernel(mix_body, shape(ny, tok, 128), 1000000, mine, other)
+    mine_all = lax.all_to_all(mix, "y", 0, 0, tiled=True)
     other_all = flip_c(mine_all)
 
     proj, grad_norm, sums = kernel(
@@ -261,7 +301,7 @@
 
     sums = sums + flip_c(sums)
     for bit in (1, 2, 4):
-        sums = sums + lax.ppermute(sums, "y", [(i, i ^ bit) for i in range(ny)])
+        sums = sums + hop(sums, bit)
     mean = sums / (128 * 2 * ny)
     conv = inverse_deviation[:, None] * (
         grad_norm - mean[0][:, None] - normalized * mean[1][:, None]

time: 194 us -> 188 us (0.969)
  the two profiles are of different devices: /device:TPU:8 before, /device:TPU:29 now
where the time goes in v3:
time: 188 us; the launch traced here: 187 us
  starting transfers between devices  82.9 us (44%)
  waiting for transfers between devices  59.6 us (32%)
  Pallas kernels  27.4 us (15%)
  other arithmetic  11 us (6%)
  local copies, waits for them, and re-layouts  4.76 us (3%)
    pallas_call x8, Pallas kernels, kernel(): pl.pallas_call(body, out_shape=outs, in_specs=[ANY if i in far else VMEM...  27.4 us
    ppermute x6, starting transfers between devices, flip_c(): return lax.ppermute(value, 'c', [(0, 1), (1, 0)])  23.4 us
    ppermute x5, starting transfers between devices, hop(): return lax.ppermute(value, ('y', 'c'), pairs)  18.7 us
    all_to_all x1, waiting for transfers between devices, shards(): lax.all_to_all(back.reshape(experts * ny, 2 * SPAN, 128), ('z', 'x', 'y')...  15.4 us
    all_to_all x1, waiting for transfers between devices, shards(): lax.all_to_all(sent.reshape(experts, 2 * SPAN, width), sp, 0, 0, tiled=True)  15.2 us
    all_to_all x1, starting transfers between devices, shards(): lax.all_to_all(back.reshape(experts * ny, 2 * SPAN, 128), ('z', 'x', 'y')...  13.7 us
    all_to_all x1, starting transfers between devices, shards(): lax.all_to_all(sent.reshape(experts, 2 * SPAN, width), sp, 0, 0, tiled=True)  12.9 us
    all_to_all x1, waiting for transfers between devices, shards(): proj = lax.all_to_all(proj.reshape(experts, -1, 128), sp, 0, 0, tiled=True)  10.2 us
  transfers between devices with their start and end apart: 16, of which 10 were waited for; matrix products, arithmetic and copies ran while one was open for 5% of the time, Pallas kernels for 7%

profile of v3, /device:TPU:29, one launch (start us, length us, event | category | flops | bytes accessed | tf_op | source)
XLA Modules:
  0.0 186.6 jit_solution(18109408632386586351)
XLA Ops:
  0.6 2.7 %shard_map.157.w0 = bf16[3,2048,128]{2,1,0:T(8,128)(2,1)} custom-call(bf16[2048,128]{1,0:T(8,128)(2,1)} %bitcast.89, bf16[2048,128]{1,0:T(8,128)(2,1)} %bitcast.90, bf16[128,2048]{1,0:T(8,128)(2,1)} %bitcast.91), custom_call_target="tpu_custom_call" | custom-call | flops 1000000 | bytes 1048576 | tf_op jit(solution)/shard_map/pallas_call | solution.py:26
  5.4 3.2 %shard_map.156 = bf16[256,2048]{1,0:T(8,128)(2,1)} custom-call(s32[2,128]{1,0:T(2,128)} %bitcast.93, f32[2,128]{1,0:T(2,128)} %bitcast.92, bf16[128,2048]{1,0:T(8,128)(2,1)} %mix_ref.1, bf16[128,2048]{1,0:T(8,128)(2,1)} %cot_ref.3), custom_call_target="tpu_custom_call" | custom-call | flops 2000000000 | bytes 1048576 | tf_op jit(solution)/shard_map/pallas_call | solution.py:26
  8.6 12.9 %all-to-all-start = ((bf16[32,8,2048]{2,1,0:T(8,128)(2,1)}), bf16[32,8,2048]{2,1,0:T(8,128)(2,1)S(1)}, u32[]{:S(2)}, u32[]{:S(2)}) async-start(bf16[32,8,2048]{2,1,0:T(8,128)(2,1)} %bitcast.87), calls=%async_computation | async-start | bytes 2097152 | tf_op jit(solution)/shard_map/all_to_all | solution.py:237
  21.5 5.8 %collective-permute-start = (bf16[3,2048,128]{2,1,0:T(8,128)(2,1)S(1)}, bf16[3,2048,128]{2,1,0:T(8,128)(2,1)}, u32[]{:S(2)}, u32[]{:S(2)}) collective-permute-start(bf16[3,2048,128]{2,1,0:T(8,128)(2,1)S(1)} %copy-done.1), channel_id=1, source_target_pairs={{0,1},{1,0},{2,3},{3,2},{4,5},{5,4},{6,7},{7,6},{8,9},{9,8},{10,11... | collective-permute-start | bytes 4718600 | tf_op jit(solution)/shard_map/ppermute | solution.py:216
  30.4 15.2 %all-to-all-done = bf16[32,8,2048]{2,1,0:T(8,128)(2,1)S(1)} async-done(((bf16[32,8,2048]{2,1,0:T(8,128)(2,1)}), bf16[32,8,2048]{2,1,0:T(8,128)(2,1)S(1)}, u32[]{:S(2)}, u32[]{:S(2)}) %all-to-all-start) | async-done | bytes 1048608 | tf_op jit(solution)/shard_map/all_to_all | solution.py:237
  46.5 6.7 %shard_map.158 = (bf16[128,2048]{1,0:T(8,128)(2,1)}, bf16[128,2048]{1,0:T(8,128)(2,1)}, bf16[128,1536]{1,0:T(8,128)(2,1)}, bf16[16,128,128]{2,1,0:T(8,128)(2,1)}) custom-call(bf16[256,2048]{1,0:T(8,128)(2,1)} %bitcast.86, bf16[3,2048,128]{2,1,0:T(8,128)(2,1)} %shard_map.157.w0, bf16[3,2048,128]{2,1,0:T(8,128)(2,1)} %collective-permute-done.w1, ...), custom_call_target="tpu_custom_call" | custom-call | flops 4000000000 | bytes 1048576 | tf_op jit(solution)/shard_map/pallas_call | solution.py:26
  53.2 5.8 %shard_map.162 = (bf16[2,3,2048,128]{3,2,1,0:T(8,128)(2,1)}, bf16[2,3,2048,128]{3,2,1,0:T(8,128)(2,1)}) custom-call(bf16[128,2048]{1,0:T(8,128)(2,1)} %get-tuple-element.22.x_ref, bf16[128,2048]{1,0:T(8,128)(2,1)} %get-tuple-element.23.g_ref, bf16[128,1536]{1,0:T(8,128)(2,1)} %get-tuple-element.24.hid_ref), custom_call_target="tpu_custom_call" | custom-call | flops 8000000000 | bytes 1048576 | tf_op jit(solution)/shard_map/pallas_call | solution.py:26
  59.0 7.1 %collective-permute-start.10 = (bf16[2,3,2048,128]{3,2,1,0:T(8,128)(2,1)}, bf16[2,3,2048,128]{3,2,1,0:T(8,128)(2,1)}, u32[]{:S(2)}, u32[]{:S(2)}) collective-permute-start(bf16[2,3,2048,128]{3,2,1,0:T(8,128)(2,1)} %get-tuple-element.26), channel_id=1, source_target_pairs={{0,1},{1,0},{2,3},{3,2},{4,5},{5,4},{6,7},{7,6},{8,9},{9,8},{10,11... | collective-permute-start | bytes 9437192 | tf_op jit(solution)/shard_map/ppermute | solution.py:216
  66.1 13.7 %all-to-all-start.1 = ((bf16[256,8,128]{2,1,0:T(8,128)(2,1)}), bf16[256,8,128]{2,1,0:T(8,128)(2,1)}, u32[]{:S(2)}, u32[]{:S(2)}) async-start(bf16[256,8,128]{2,1,0:T(8,128)(2,1)} %bitcast.8), calls=%async_computation.1 | async-start | bytes 1048576 | tf_op jit(solution)/shard_map/all_to_all | solution.py:263
  82.1 15.4 %all-to-all-done.1 = bf16[256,8,128]{2,1,0:T(8,128)(2,1)} async-done(((bf16[256,8,128]{2,1,0:T(8,128)(2,1)}), bf16[256,8,128]{2,1,0:T(8,128)(2,1)}, u32[]{:S(2)}, u32[]{:S(2)}) %all-to-all-start.1) | async-done | bytes 524320 | tf_op jit(solution)/shard_map/all_to_all | solution.py:263
  100.1 3.0 %collective-permute-start.3 = (bf16[128,128]{1,0:T(8,128)(2,1)}, bf16[128,128]{1,0:T(8,128)(2,1)S(1)}, u32[]{:S(2)}, u32[]{:S(2)}) collective-permute-start(bf16[128,128]{1,0:T(8,128)(2,1)} %get-tuple-element.18), channel_id=1, source_target_pairs={{0,1},{1,0},{2,3},{3,2},{4,5},{5,4},{6,7},{7,6},{8,9},{9,8},{10,11... | collective-permute-start | bytes 98312 | tf_op jit(solution)/shard_map/ppermute | solution.py:216
  106.3 6.5 %all-to-all-start.2 = ((bf16[8,128,128]{2,1,0:T(8,128)(2,1)}), bf16[8,128,128]{2,1,0:T(8,128)(2,1)S(1)}, u32[]{:S(2)}, u32[]{:S(2)}) async-start(bf16[8,128,128]{2,1,0:T(8,128)(2,1)} %shard_map.160), calls=%async_computation.2 | async-start | bytes 524288 | tf_op jit(solution)/shard_map/all_to_all | solution.py:285
  114.1 7.0 %all-to-all-done.2.mine_ref = bf16[8,128,128]{2,1,0:T(8,128)(2,1)S(1)} async-done(((bf16[8,128,128]{2,1,0:T(8,128)(2,1)}), bf16[8,128,128]{2,1,0:T(8,128)(2,1)S(1)}, u32[]{:S(2)}, u32[]{:S(2)}) %all-to-all-start.2) | async-done | bytes 262176 | tf_op jit(solution)/shard_map/all_to_all | solution.py:285
  121.1 3.2 %collective-permute-start.4 = (bf16[8,128,128]{2,1,0:T(8,128)(2,1)S(1)}, bf16[8,128,128]{2,1,0:T(8,128)(2,1)S(1)}, u32[]{:S(2)}, u32[]{:S(2)}) collective-permute-start(bf16[8,128,128]{2,1,0:T(8,128)(2,1)S(1)} %all-to-all-done.2.mine_ref), channel_id=1, source_target_pairs={{0,1},{1,0},{2,3},{3,2},{4,5},{5,4},{6,7},{7,6},{8,9},{9,8},{10,11... | collective-permute-start | bytes 786440 | tf_op jit(solution)/shard_map/ppermute | solution.py:216
  124.3 3.0 %fusion.1 = bf16[3,2048,128]{2,1,0:T(8,128)(2,1)} fusion(bf16[2,3,2048,128]{3,2,1,0:T(8,128)(2,1)} %collective-permute-done.10, bf16[2,3,2048,128]{3,2,1,0:T(8,128)(2,1)S(1)} %copy-done), kind=kLoop, calls=%fused_computation.3 | loop fusion | flops 3145728 | bytes 4718592 | tf_op jit(solution)/shard_map/convert_element_type | solution.py:270
  127.4 2.6 %collective-permute-start.11 = (bf16[3,2048,128]{2,1,0:T(8,128)(2,1)}, bf16[3,2048,128]{2,1,0:T(8,128)(2,1)}, u32[]{:S(2)}, u32[]{:S(2)}) collective-permute-start(bf16[3,2048,128]{2,1,0:T(8,128)(2,1)} %fusion.1), channel_id=1, source_target_pairs={{0,14},{1,3},{2,0},{3,5},{4,2},{5,7},{6,4},{7,9},{8,6},{9,11},{10,... | collective-permute-start | bytes 4718600 | tf_op jit(solution)/shard_map/ppermute | solution.py:223
  130.7 2.7 %shard_map.161 = (bf16[2048,128]{1,0:T(8,128)(2,1)}, f32[128,128]{1,0:T(8,128)}, f32[2,128]{1,0:T(2,128)}) custom-call(bf16[8,128,128]{2,1,0:T(8,128)(2,1)} %copy-done.4, bf16[8,128,128]{2,1,0:T(8,128)(2,1)} %copy-done.9, bf16[128,2048]{1,0:T(8,128)(2,1)} %proj_ref.1, bf16[128,128]{1,0:T(8,128)(2,1)} %get-tuple-element.31.act_ref, ...), custom_call_target="tpu_custom_call" | custom-call | flops 2000000000 | bytes 1048576 | tf_op jit(solution)/shard_map/pallas_call | solution.py:26
  137.5 3.8 %collective-permute-start.6 = (f32[2,128]{1,0:T(2,128)S(1)}, f32[2,128]{1,0:T(2,128)S(1)}, u32[]{:S(2)}, u32[]{:S(2)}) collective-permute-start(f32[2,128]{1,0:T(2,128)S(1)} %add.123), channel_id=1, source_target_pairs={{0,2},{1,15},{2,4},{3,1},{4,6},{5,3},{6,8},{7,5},{8,10},{9,7},{10,... | collective-permute-start | bytes 3080 | tf_op jit(solution)/shard_map/ppermute | solution.py:223
  143.5 3.5 %collective-permute-start.7 = (f32[2,128]{1,0:T(2,128)S(1)}, f32[2,128]{1,0:T(2,128)S(1)}, u32[]{:S(2)}, u32[]{:S(2)}) collective-permute-start(f32[2,128]{1,0:T(2,128)S(1)} %add.124), channel_id=1, source_target_pairs={{0,4},{1,13},{2,6},{3,15},{4,8},{5,1},{6,10},{7,3},{8,12},{9,5},{1... | collective-permute-start | bytes 3080 | tf_op jit(solution)/shard_map/ppermute | solution.py:223
  146.9 2.9 %collective-permute-done.7 = f32[2,128]{1,0:T(2,128)S(1)} collective-permute-done((f32[2,128]{1,0:T(2,128)S(1)}, f32[2,128]{1,0:T(2,128)S(1)}, u32[]{:S(2)}, u32[]{:S(2)}) %collective-permute-start.7) | collective-permute-done | bytes 1056 | tf_op jit(solution)/shard_map/ppermute | solution.py:223
  149.9 6.8 %collective-permute-start.8 = (f32[2,128]{1,0:T(2,128)S(1)}, f32[2,128]{1,0:T(2,128)S(1)}, u32[]{:S(2)}, u32[]{:S(2)}) collective-permute-start(f32[2,128]{1,0:T(2,128)S(1)} %add.125), channel_id=1, source_target_pairs={{0,8},{1,9},{2,10},{3,11},{4,12},{5,13},{6,14},{7,15},{8,0},{9,1},... | collective-permute-start | bytes 3080 | tf_op jit(solution)/shard_map/ppermute | solution.py:223
  156.7 5.5 %all-to-all-start.3 = ((bf16[32,64,128]{2,1,0:T(8,128)(2,1)}), bf16[32,64,128]{2,1,0:T(8,128)(2,1)}, u32[]{:S(2)}, u32[]{:S(2)}) async-start(bf16[32,64,128]{2,1,0:T(8,128)(2,1)} %bitcast.88), calls=%async_computation.3 | async-start | bytes 1048576 | tf_op jit(solution)/shard_map/all_to_all | solution.py:299
  165.4 3.5 %collective-permute-done.9 = f32[30,128]{1,0:T(8,128)S(1)} collective-permute-done((f32[30,128]{1,0:T(8,128)S(1)}, f32[30,128]{1,0:T(8,128)S(1)}, u32[]{:S(2)}, u32[]{:S(2)}) %collective-permute-start.9) | collective-permute-done | bytes 15392 | tf_op jit(solution)/shard_map/ppermute | solution.py:310
  169.7 10.2 %all-to-all-done.3 = bf16[32,64,128]{2,1,0:T(8,128)(2,1)} async-done(((bf16[32,64,128]{2,1,0:T(8,128)(2,1)}), bf16[32,64,128]{2,1,0:T(8,128)(2,1)}, u32[]{:S(2)}, u32[]{:S(2)}) %all-to-all-start.3) | async-done | bytes 524320 | tf_op jit(solution)/shard_map/all_to_all | solution.py:299
  (54 shorter events, 33.1 us)
Async XLA Ops:
  3.3 23.9 %collective-permute-start.1 = (bf16[3,2048,128]{2,1,0:T(8,128)(2,1)}, bf16[3,2048,128]{2,1,0:T(8,128)(2,1)}, u32[]{:S(2)}, u32[]{:S(2)}) collective-permute-start(bf16[3,2048,128]{2,1,0:T(8,128)(2,1)} %shard_map.157.w0), channel_id=1, source_target_pairs={{0,2},{1,15},{2,4},{3,1},{4,6},{5,3},{6,8},{7,5},{8,10},{9,7},{10,... | collective-permute-start | bytes 4718600 | tf_op jit(solution)/shard_map/ppermute | solution.py:223
  5.4 16.1 %copy-start.1 = (bf16[3,2048,128]{2,1,0:T(8,128)(2,1)S(1)}, bf16[3,2048,128]{2,1,0:T(8,128)(2,1)}, u32[]{:S(2)}) copy-start(bf16[3,2048,128]{2,1,0:T(8,128)(2,1)} %shard_map.157.w0) | copy-start | bytes 4718596
  8.6 37.0 %all-to-all-start = ((bf16[32,8,2048]{2,1,0:T(8,128)(2,1)}), bf16[32,8,2048]{2,1,0:T(8,128)(2,1)S(1)}, u32[]{:S(2)}, u32[]{:S(2)}) async-start(bf16[32,8,2048]{2,1,0:T(8,128)(2,1)} %bitcast.87), calls=%async_computation | async-start | bytes 2097152 | tf_op jit(solution)/shard_map/all_to_all | solution.py:237
  21.5 8.9 %collective-permute-start = (bf16[3,2048,128]{2,1,0:T(8,128)(2,1)S(1)}, bf16[3,2048,128]{2,1,0:T(8,128)(2,1)}, u32[]{:S(2)}, u32[]{:S(2)}) collective-permute-start(bf16[3,2048,128]{2,1,0:T(8,128)(2,1)S(1)} %copy-done.1), channel_id=1, source_target_pairs={{0,1},{1,0},{2,3},{3,2},{4,5},{5,4},{6,7},{7,6},{8,9},{9,8},{10,11... | collective-permute-start | bytes 4718600 | tf_op jit(solution)/shard_map/ppermute | solution.py:216
  27.2 18.3 %collective-permute-start.2 = (bf16[3,2048,128]{2,1,0:T(8,128)(2,1)}, bf16[3,2048,128]{2,1,0:T(8,128)(2,1)}, u32[]{:S(2)}, u32[]{:S(2)}) collective-permute-start(bf16[3,2048,128]{2,1,0:T(8,128)(2,1)} %collective-permute-done.1.w2), channel_id=1, source_target_pairs={{0,1},{1,0},{2,3},{3,2},{4,5},{5,4},{6,7},{7,6},{8,9},{9,8},{10,11... | collective-permute-start | bytes 4718600 | tf_op jit(solution)/shard_map/ppermute | solution.py:216
  45.6 1.0 copy-start.2
  59.0 65.3 %collective-permute-start.10 = (bf16[2,3,2048,128]{3,2,1,0:T(8,128)(2,1)}, bf16[2,3,2048,128]{3,2,1,0:T(8,128)(2,1)}, u32[]{:S(2)}, u32[]{:S(2)}) collective-permute-start(bf16[2,3,2048,128]{3,2,1,0:T(8,128)(2,1)} %get-tuple-element.26), channel_id=1, source_target_pairs={{0,1},{1,0},{2,3},{3,2},{4,5},{5,4},{6,7},{7,6},{8,9},{9,8},{10,11... | collective-permute-start | bytes 9437192 | tf_op jit(solution)/shard_map/ppermute | solution.py:216
  66.1 31.4 %all-to-all-start.1 = ((bf16[256,8,128]{2,1,0:T(8,128)(2,1)}), bf16[256,8,128]{2,1,0:T(8,128)(2,1)}, u32[]{:S(2)}, u32[]{:S(2)}) async-start(bf16[256,8,128]{2,1,0:T(8,128)(2,1)} %bitcast.8), calls=%async_computation.1 | async-start | bytes 1048576 | tf_op jit(solution)/shard_map/all_to_all | solution.py:263
  79.9 33.0 %copy-start.3 = (bf16[128,128]{1,0:T(8,128)(2,1)S(1)}, bf16[128,128]{1,0:T(8,128)(2,1)}, u32[]{:S(2)}) copy-start(bf16[128,128]{1,0:T(8,128)(2,1)} %param.16) | copy-start | bytes 98308
  79.9 33.6 %copy-start.7 = (f32[128]{0:T(128)S(1)}, f32[128]{0:T(128)}, u32[]{:S(2)}) copy-start(f32[128]{0:T(128)} %param.18) | copy-start | bytes 1540
  82.1 42.2 %copy-start = (bf16[2,3,2048,128]{3,2,1,0:T(8,128)(2,1)S(1)}, bf16[2,3,2048,128]{3,2,1,0:T(8,128)(2,1)}, u32[]{:S(2)}) copy-start(bf16[2,3,2048,128]{3,2,1,0:T(8,128)(2,1)} %get-tuple-element.25) | copy-start | bytes 9437188
  100.1 4.1 %collective-permute-start.3 = (bf16[128,128]{1,0:T(8,128)(2,1)}, bf16[128,128]{1,0:T(8,128)(2,1)S(1)}, u32[]{:S(2)}, u32[]{:S(2)}) collective-permute-start(bf16[128,128]{1,0:T(8,128)(2,1)} %get-tuple-element.18), channel_id=1, source_target_pairs={{0,1},{1,0},{2,3},{3,2},{4,5},{5,4},{6,7},{7,6},{8,9},{9,8},{10,11... | collective-permute-start | bytes 98312 | tf_op jit(solution)/shard_map/ppermute | solution.py:216
  106.3 14.8 %all-to-all-start.2 = ((bf16[8,128,128]{2,1,0:T(8,128)(2,1)}), bf16[8,128,128]{2,1,0:T(8,128)(2,1)S(1)}, u32[]{:S(2)}, u32[]{:S(2)}) async-start(bf16[8,128,128]{2,1,0:T(8,128)(2,1)} %shard_map.160), calls=%async_computation.2 | async-start | bytes 524288 | tf_op jit(solution)/shard_map/all_to_all | solution.py:285
  121.1 9.6 %copy-start.4 = (bf16[8,128,128]{2,1,0:T(8,128)(2,1)}, bf16[8,128,128]{2,1,0:T(8,128)(2,1)S(1)}, u32[]{:S(2)}) copy-start(bf16[8,128,128]{2,1,0:T(8,128)(2,1)S(1)} %all-to-all-done.2.mine_ref) | copy-start | bytes 786436
  121.1 8.9 %collective-permute-start.4 = (bf16[8,128,128]{2,1,0:T(8,128)(2,1)S(1)}, bf16[8,128,128]{2,1,0:T(8,128)(2,1)S(1)}, u32[]{:S(2)}, u32[]{:S(2)}) collective-permute-start(bf16[8,128,128]{2,1,0:T(8,128)(2,1)S(1)} %all-to-all-done.2.mine_ref), channel_id=1, source_target_pairs={{0,1},{1,0},{2,3},{3,2},{4,5},{5,4},{6,7},{7,6},{8,9},{9,8},{10,11... | collective-permute-start | bytes 786440 | tf_op jit(solution)/shard_map/ppermute | solution.py:216
  127.4 54.3 %collective-permute-start.11 = (bf16[3,2048,128]{2,1,0:T(8,128)(2,1)}, bf16[3,2048,128]{2,1,0:T(8,128)(2,1)}, u32[]{:S(2)}, u32[]{:S(2)}) collective-permute-start(bf16[3,2048,128]{2,1,0:T(8,128)(2,1)} %fusion.1), channel_id=1, source_target_pairs={{0,14},{1,3},{2,0},{3,5},{4,2},{5,7},{6,4},{7,9},{8,6},{9,11},{10,... | collective-permute-start | bytes 4718600 | tf_op jit(solution)/shard_map/ppermute | solution.py:223
  130.7 26.0 %copy-start.6 = (f32[31,128]{1,0:T(8,128)S(1)}, f32[31,128]{1,0:T(8,128)}, u32[]{:S(2)}) copy-start(f32[31,128]{1,0:T(8,128)} %param.19) | copy-start | bytes 47620
  130.7 31.5 %copy-start.8 = (f32[128]{0:T(128)S(1)}, f32[128]{0:T(128)}, u32[]{:S(2)}) copy-start(f32[128]{0:T(128)} %param.17) | copy-start | bytes 1540
  133.4 3.4 %collective-permute-start.5 = (f32[2,128]{1,0:T(2,128)}, f32[2,128]{1,0:T(2,128)S(1)}, u32[]{:S(2)}, u32[]{:S(2)}) collective-permute-start(f32[2,128]{1,0:T(2,128)} %get-tuple-element.20), channel_id=1, source_target_pairs={{0,1},{1,0},{2,3},{3,2},{4,5},{5,4},{6,7},{7,6},{8,9},{9,8},{10,11... | collective-permute-start | bytes 3080 | tf_op jit(solution)/shard_map/ppermute | solution.py:216
  137.5 5.9 %collective-permute-start.6 = (f32[2,128]{1,0:T(2,128)S(1)}, f32[2,128]{1,0:T(2,128)S(1)}, u32[]{:S(2)}, u32[]{:S(2)}) collective-permute-start(f32[2,128]{1,0:T(2,128)S(1)} %add.123), channel_id=1, source_target_pairs={{0,2},{1,15},{2,4},{3,1},{4,6},{5,3},{6,8},{7,5},{8,10},{9,7},{10,... | collective-permute-start | bytes 3080 | tf_op jit(solution)/shard_map/ppermute | solution.py:223
  143.5 6.4 %collective-permute-start.7 = (f32[2,128]{1,0:T(2,128)S(1)}, f32[2,128]{1,0:T(2,128)S(1)}, u32[]{:S(2)}, u32[]{:S(2)}) collective-permute-start(f32[2,128]{1,0:T(2,128)S(1)} %add.124), channel_id=1, source_target_pairs={{0,4},{1,13},{2,6},{3,15},{4,8},{5,1},{6,10},{7,3},{8,12},{9,5},{1... | collective-permute-start | bytes 3080 | tf_op jit(solution)/shard_map/ppermute | solution.py:223
  149.9 12.3 %collective-permute-start.8 = (f32[2,128]{1,0:T(2,128)S(1)}, f32[2,128]{1,0:T(2,128)S(1)}, u32[]{:S(2)}, u32[]{:S(2)}) collective-permute-start(f32[2,128]{1,0:T(2,128)S(1)} %add.125), channel_id=1, source_target_pairs={{0,8},{1,9},{2,10},{3,11},{4,12},{5,13},{6,14},{7,15},{8,0},{9,1},... | collective-permute-start | bytes 3080 | tf_op jit(solution)/shard_map/ppermute | solution.py:223
  156.7 23.2 %all-to-all-start.3 = ((bf16[32,64,128]{2,1,0:T(8,128)(2,1)}), bf16[32,64,128]{2,1,0:T(8,128)(2,1)}, u32[]{:S(2)}, u32[]{:S(2)}) async-start(bf16[32,64,128]{2,1,0:T(8,128)(2,1)} %bitcast.88), calls=%async_computation.3 | async-start | bytes 1048576 | tf_op jit(solution)/shard_map/all_to_all | solution.py:299
  163.2 5.7 %collective-permute-start.9 = (f32[30,128]{1,0:T(8,128)S(1)}, f32[30,128]{1,0:T(8,128)S(1)}, u32[]{:S(2)}, u32[]{:S(2)}) collective-permute-start(f32[30,128]{1,0:T(8,128)S(1)} %slice.284), channel_id=1, source_target_pairs={{16,0},{32,16},{48,32},{64,48},{80,64},{96,80},{112,96},{128,112},... | collective-permute-start | bytes 46088 | tf_op jit(solution)/shard_map/ppermute | solution.py:310
  (2 other events, 1.3 us)

commit v4 on v3

--- a/solution.py
+++ b/solution.py
@@ -22,13 +22,13 @@
     return lax.broadcasted_iota(I32, shape, dim)
 
 
-def kernel(body, outs, flops, *args, scratch=(), far=()):
+def kernel(body, outs, flops, *args, scratch=(), far=(), near=True):
     return pl.pallas_call(
         body,
         out_shape=outs,
         in_specs=[ANY if i in far else VMEM for i in range(len(args))],
         scratch_shapes=list(scratch),
-        out_specs=jax.tree.map(lambda _: VMEM, outs),
+        out_specs=jax.tree.map(lambda _: VMEM if near else ANY, outs),
         cost_estimate=pl.CostEstimate(flops=flops, bytes_accessed=1 << 20, transcendentals=0),
     )(*args)
 
@@ -91,11 +91,64 @@
     out_ref[tok:, :] = jnp.where(hit & (half != ci), 1.0, 0.0).astype(BF)
 
 
-def pack_body(gate_ref, up_ref, down_ref, out_ref):
-    out_ref[0] = gate_ref[...]
-    out_ref[1] = up_ref[...]
-    for j in range(down_ref.shape[1] // 128):
-        out_ref[2, j * 128 : (j + 1) * 128, :] = down_ref[:, j * 128 : (j + 1) * 128]
+def pack_body(gate_ref, up_ref, down_ref, out_ref, buf_ref, sem):
+    blocks = down_ref.shape[1] // 128
+    load, store = [], []
+    for m, ref in enumerate((gate_ref, up_ref)):
+        load.append(pltpu.make_async_copy(ref, buf_ref.at[m], sem.at[m, 0]))
+    down = [
+        pltpu.make_async_copy(
+            down_ref.at[:, j * 128 : (j + 1) * 128],
+            buf_ref.at[2, j * 128 : (j + 1) * 128],
+            sem.at[2 + j, 0],
+        )
+        for j in range(blocks)
+    ]
+    for copy in (*load, *down):
+        copy.start()
+    for m in range(3):
+        for copy in load[m : m + 1] if m < 2 else down:
+            copy.wait()
+        copy = pltpu.make_async_copy(buf_ref.at[m], out_ref.at[m], sem.at[m, 1])
+        copy.start()
+        store.append(copy)
+    for copy in store:
+        copy.wait()
+
+
+def slope_body(saved_ref, gain_ref, proj_ref, act_ref, slope_ref, keep_ref, give_ref):
+    ci = lax.axis_index("c")
+    saved = saved_ref[...].astype(F32)
+    values = saved * gain_ref[...]
+    gate = jax.nn.sigmoid(values)
+    act_ref[...] = (values * gate).astype(BF)
+    slope = gate * (1.0 + values * (1.0 - gate)) * gain_ref[...]
+    slope_ref[...] = slope
+    high, low = [], []
+    for u in (slope, slope * saved):
+        high.append(u.astype(BF))
+        low.append((u - high[-1].astype(F32)).astype(BF))
+    high, low = jnp.concatenate(high, axis=0), jnp.concatenate(low, axis=0)
+    for y in range(keep_ref.shape[0]):
+        for ref, cc in ((keep_ref, ci), (give_ref, 1 - ci)):
+            part = proj_ref[:, pl.ds(pl.multiple_of((2 * y + cc) * 128, 128), 128)]
+            ref[y] = (mm(high, part) + mm(low, part)).astype(ref.dtype)
+
+
+def share_body(keep_ref, given_ref, own_ref, *out_refs):
+    yi = lax.axis_index("y")
+    ny = keep_ref.shape[0]
+    own_ref[...] = keep_ref[yi] + given_ref[yi].astype(F32)
+    for k, ref in enumerate(out_refs, 1):
+        to = lax.rem(yi + k, ny)
+        ref[...] = (keep_ref[to] + given_ref[to].astype(F32)).astype(BF)
+
+
+def total_body(own_ref, *refs):
+    total = own_ref[...]
+    for ref in refs[:-1]:
+        total = total + ref[...].astype(F32)
+    refs[-1][...] = total
 
 
 def expert_body(got_ref, w0, w1, w2, w3, x_ref, g_ref, hid_ref, back_ref, in_ref, down_ref, sem):
@@ -171,26 +224,56 @@
     other_ref[...] = both[tok:].astype(BF)
 
 
-def mix_body(own_ref, other_ref, out_ref):
+def mix_body(own_ref, other_ref, total_ref, out_ref):
+    tok = own_ref.shape[0]
     mix = (own_ref[...] + other_ref[...].astype(F32)).astype(BF)
+    wide = mix.astype(F32)
+    parts = []
+    for k in range(2):
+        rest = jnp.sum((wide * total_ref[k * tok : (k + 1) * tok, :]).T, axis=0, keepdims=True)
+        for _ in range(3):
+            parts.append(rest.astype(BF).astype(F32))
+            rest = rest - parts[-1]
+    parts.append(jnp.zeros((2, tok), F32))
+    sums = jnp.concatenate(parts, axis=0).astype(BF)
     for y in range(out_ref.shape[0]):
-        out_ref[y] = mix
-
-
-def final_body(mine_ref, other_ref, proj_ref, act_ref, slope_ref, norm_ref, out_ref, grad_ref, sum_ref):
+        out_ref[y, :tok, :] = mix
+        out_ref[y, tok:, :] = sums
+
+
+def final_body(mine_ref, other_ref, proj_ref, act_ref, slope_ref, saved_ref, dev_ref, out_ref, conv_ref):
     ci = lax.axis_index("c")
     tok = act_ref.shape[0]
     acc = jnp.zeros((tok, tok), F32)
+    sums = jnp.zeros((8, tok), F32)
     for y in range(mine_ref.shape[0]):
         for ref, cc in ((mine_ref, ci), (other_ref, 1 - ci)):
             at = pl.ds(pl.multiple_of((2 * y + cc) * 128, 128), 128)
-            part = ref[y]
+            part = ref[y, :tok, :]
+            sums = sums + ref[y, tok:, :].astype(F32)
             out_ref[at, :] = mm(part, act_ref[...], FIRST).astype(BF)
             acc = acc + mm(part, proj_ref[:, at], LAST)
     grad = acc * slope_ref[...]
-    grad_ref[...] = grad
-    sum_ref[0:1, :] = jnp.sum(grad.T, axis=0, keepdims=True)
-    sum_ref[1:2, :] = jnp.sum((grad * norm_ref[...]).T, axis=0, keepdims=True)
+    count = 2 * mine_ref.shape[0] * 128
+    means = []
+    for k in range(2):
+        total = jnp.sum(sums[3 * k : 3 * k + 3], axis=0, keepdims=True) / count
+        means.append(jnp.broadcast_to(total, (tok, tok)).T)
+    dev = jnp.broadcast_to(dev_ref[...], (tok, tok)).T
+    conv_ref[...] = dev * (grad - means[0] - saved_ref[...].astype(F32) * means[1])
+
+
+def sumout_body(keep_ref, given_ref, pre_ref, pass_ref):
+    pre_ref[0] = (keep_ref[0, 0].astype(F32) + given_ref[0, 0].astype(F32)).astype(BF)
+    pass_ref[0] = (keep_ref[1, 0].astype(F32) + given_ref[1, 0].astype(F32)).astype(BF)
+
+
+def addup_body(pre_ref, passed_ref, gate_ref, up_ref, down_ref):
+    for m, ref in ((0, gate_ref), (1, up_ref)):
+        ref[...] = (pre_ref[m].astype(F32) + passed_ref[m].astype(F32)).astype(BF)
+    for j in range(down_ref.shape[1] // 128):
+        at = slice(j * 128, (j + 1) * 128)
+        down_ref[:, at] = (pre_ref[2, at].astype(F32) + passed_ref[2, at].astype(F32)).astype(BF)
 
 
 def shards(
@@ -215,6 +298,9 @@
     def flip_c(value):
         return lax.ppermute(value, "c", [(0, 1), (1, 0)])
 
+    def shift(value, k):
+        return lax.ppermute(value, "y", [(i, (i + k) % ny) for i in range(ny)])
+
     def hop(value, sign):
         pairs = []
         for y in range(ny):
@@ -223,7 +309,15 @@
         return lax.ppermute(value, ("y", "c"), pairs)
 
     own = kernel(
-        pack_body, shape(3, width, 128), 1000000, gate_weight[0], up_weight[0], down_weight[0]
+        pack_body,
+        shape(3, width, 128),
+        1000000,
+        gate_weight[0],
+        up_weight[0],
+        down_weight[0],
+        far=(0, 1, 2),
+        near=False,
+        scratch=(pltpu.VMEM((3, width, 128), BF), pltpu.SemaphoreType.DMA((2 + width // 128, 2))),
     )
     by_y = hop(own, 1)
     by_c = flip_c(own)
@@ -237,11 +331,31 @@
     got = lax.all_to_all(sent.reshape(experts, 2 * SPAN, width), sp, 0, 0, tiled=True)
     table = kernel(table_body, shape(2 * tok, experts * ny * 2 * SPAN), 2000000000, ids)
 
-    normalized = saved_normalized.astype(F32)
-    values = normalized * channel_norm_gain[None, :]
-    gate = jax.nn.sigmoid(values)
-    act_conv = (values * gate).astype(BF)
-    slope = gate * (1.0 + values * (1.0 - gate)) * channel_norm_gain[None, :]
+    act_conv, slope, vkeep, vgive = kernel(
+        slope_body,
+        (
+            shape(tok, 128),
+            shape(tok, 128, kind=F32),
+            shape(ny, 2 * tok, 128, kind=F32),
+            shape(ny, 2 * tok, 128),
+        ),
+        500000000,
+        saved_normalized,
+        channel_norm_gain[None, :],
+        proj_weight,
+    )
+    vgiven = flip_c(vgive)
+    vown, *vsent = kernel(
+        share_body,
+        (shape(2 * tok, 128, kind=F32), *[shape(2 * tok, 128)] * (ny - 1)),
+        1000000,
+        vkeep,
+        vgiven,
+    )
+    vgot = []
+    for k, value in enumerate(vsent, 1):
+        vgot.append(shift(value, k))
+    vtotal = kernel(total_body, shape(2 * tok, 128, kind=F32), 1000000, vown, *vgot)
 
     slots = experts * SPAN
     x, g, hidden, back = kernel(
@@ -267,10 +381,24 @@
     packed = shape(2, 3, width, 128)
     keep, give = kernel(grads_body, (packed, packed), 8000000000, x, g, hidden)
     given = flip_c(give)
-    passing = (keep[1].astype(F32) + given[1].astype(F32)).astype(BF)
+    block = pl.BlockSpec((2, 1, width, 128), lambda m: (0, m, 0, 0))
+    piece = pl.BlockSpec((1, width, 128), lambda m: (m, 0, 0))
+    before, passing = pl.pallas_call(
+        sumout_body,
+        grid=(3,),
+        out_shape=(shape(3, width, 128), shape(3, width, 128)),
+        in_specs=[block, block],
+        out_specs=[piece, piece],
+        cost_estimate=pl.CostEstimate(flops=1000000, bytes_accessed=9 << 20, transcendentals=0),
+    )(keep, given)
     passed = hop(passing, -1)
-    final = (keep[0].astype(F32) + given[0].astype(F32) + passed.astype(F32)).astype(BF)
-    grad_down = final[2].reshape(-1, 128, 128).transpose(1, 0, 2).reshape(128, width)
+    grad_gate, grad_up, grad_down = kernel(
+        addup_body,
+        (shape(width, 128), shape(width, 128), shape(128, width)),
+        1000000,
+        before,
+        passed,
+    )
 
     mine, other = kernel(
         combine_body,
@@ -281,38 +409,32 @@
         cotangent,
     )
     other = flip_c(other)
-    mix = kernel(mix_body, shape(ny, tok, 128), 1000000, mine, other)
+    mix = kernel(mix_body, shape(ny, tok + 8, 128), 1000000, mine, other, vtotal)
     mine_all = lax.all_to_all(mix, "y", 0, 0, tiled=True)
     other_all = flip_c(mine_all)
 
-    proj, grad_norm, sums = kernel(
+    proj, conv = kernel(
         final_body,
-        (shape(width, 128), shape(tok, 128, kind=F32), shape(2, 128, kind=F32)),
+        (shape(width, 128), shape(tok, 128, kind=F32)),
         2000000000,
         mine_all,
         other_all,
         proj_weight,
         act_conv,
         slope,
-        normalized,
+        saved_normalized,
+        inverse_deviation[None, :],
     )
     proj = lax.all_to_all(proj.reshape(experts, -1, 128), sp, 0, 0, tiled=True)
     grad_proj = jnp.sum(proj.astype(F32), axis=0)
 
-    sums = sums + flip_c(sums)
-    for bit in (1, 2, 4):
-        sums = sums + hop(sums, bit)
-    mean = sums / (128 * 2 * ny)
-    conv = inverse_deviation[:, None] * (
-        grad_norm - mean[0][:, None] - normalized * mean[1][:, None]
-    )
     reach = taps.shape[0] - 1
     beyond = lax.ppermute(conv[:reach], sp, [(i + 1, i) for i in range(experts - 1)])
     extended = jnp.concatenate([conv, beyond], axis=0)
     result = jnp.zeros_like(conv)
     for j in range(reach + 1):
         result = result + taps[j][None, :] * extended[j : j + tok]
-    return (result.astype(BF), grad_proj, final[0][None], final[1][None], grad_down[None])
+    return (result.astype(BF), grad_proj, grad_gate[None], grad_up[None], grad_down[None])
 
 
 def solution(mesh):

time: 188 us -> 195 us (1.037)
  the two profiles are of different devices: /device:TPU:29 before, /device:TPU:1 now
where the time goes in v4:
time: 195 us; the launch traced here: 194 us
  starting transfers between devices  93.3 us (48%)
  Pallas kernels  42.8 us (22%)
  waiting for transfers between devices  31.5 us (16%)
  blocking collectives  15.9 us (8%)
  local copies, waits for them, and re-layouts  6.69 us (3%)
  other arithmetic  2.33 us (1%)
    pallas_call x12, Pallas kernels, kernel(): pl.pallas_call(body, out_shape=outs, in_specs=[ANY if i in far else VMEM...  37.5 us
    ppermute x7, starting transfers between devices, shift(): return lax.ppermute(value, 'y', [(i, (i + k) % ny) for i in range(ny)])  25.6 us
    ppermute x6, starting transfers between devices, flip_c(): return lax.ppermute(value, 'c', [(0, 1), (1, 0)])  21.7 us
    all_to_all x1, waiting for transfers between devices, shards(): lax.all_to_all(sent.reshape(experts, 2 * SPAN, width), sp, 0, 0, tiled=True)  17.4 us
    all_to_all x1, blocking collectives, shards(): mine_all = lax.all_to_all(mix, 'y', 0, 0, tiled=True)  15.9 us
    all_to_all x1, starting transfers between devices, shards(): lax.all_to_all(back.reshape(experts * ny, 2 * SPAN, 128), ('z', 'x', 'y')...  13.6 us
    all_to_all x1, starting transfers between devices, shards(): lax.all_to_all(sent.reshape(experts, 2 * SPAN, width), sp, 0, 0, tiled=True)  13 us
    all_to_all x1, starting transfers between devices, shards(): proj = lax.all_to_all(proj.reshape(experts, -1, 128), sp, 0, 0, tiled=True)  10.1 us
  transfers between devices with their start and end apart: 19, of which 4 were waited for; matrix products, arithmetic and copies ran while one was open for 2% of the time, Pallas kernels for 13%

profile of v4, /device:TPU:1, one launch (start us, length us, event | category | flops | bytes accessed | tf_op | source)
XLA Modules:
  0.0 193.6 jit_solution(14149451039261960443)
XLA Ops:
  0.6 2.5 %shard_map.157.w0 = bf16[3,2048,128]{2,1,0:T(8,128)(2,1)} custom-call(bf16[2048,128]{1,0:T(8,128)(2,1)} %bitcast.81, bf16[2048,128]{1,0:T(8,128)(2,1)} %bitcast.82, bf16[128,2048]{1,0:T(8,128)(2,1)} %bitcast.83), custom_call_target="tpu_custom_call" | custom-call | flops 1000000 | bytes 1048576 | tf_op jit(solution)/shard_map/pallas_call | solution.py:26
  3.2 5.9 %collective-permute-start.1 = (bf16[3,2048,128]{2,1,0:T(8,128)(2,1)}, bf16[3,2048,128]{2,1,0:T(8,128)(2,1)}, u32[]{:S(2)}, u32[]{:S(2)}) collective-permute-start(bf16[3,2048,128]{2,1,0:T(8,128)(2,1)} %shard_map.157.w0), channel_id=1, source_target_pairs={{0,2},{1,15},{2,4},{3,1},{4,6},{5,3},{6,8},{7,5},{8,10},{9,7},{10,... | collective-permute-start | bytes 4718600 | tf_op jit(solution)/shard_map/ppermute | solution.py:309
  9.1 3.1 %shard_map.156 = bf16[256,2048]{1,0:T(8,128)(2,1)} custom-call(s32[2,128]{1,0:T(2,128)} %bitcast.88, f32[2,128]{1,0:T(2,128)} %bitcast.87, bf16[128,2048]{1,0:T(8,128)(2,1)} %mix_ref.1, bf16[128,2048]{1,0:T(8,128)(2,1)} %cot_ref.3), custom_call_target="tpu_custom_call" | custom-call | flops 2000000000 | bytes 1048576 | tf_op jit(solution)/shard_map/pallas_call | solution.py:26
  12.2 13.0 %all-to-all-start = ((bf16[32,8,2048]{2,1,0:T(8,128)(2,1)}), bf16[32,8,2048]{2,1,0:T(8,128)(2,1)S(1)}, u32[]{:S(2)}, u32[]{:S(2)}) async-start(bf16[32,8,2048]{2,1,0:T(8,128)(2,1)} %bitcast.78), calls=%async_computation | async-start | bytes 2097152 | tf_op jit(solution)/shard_map/all_to_all | solution.py:331
  27.2 8.6 %collective-permute-start.2 = (bf16[3,2048,128]{2,1,0:T(8,128)(2,1)}, bf16[3,2048,128]{2,1,0:T(8,128)(2,1)}, u32[]{:S(2)}, u32[]{:S(2)}) collective-permute-start(bf16[3,2048,128]{2,1,0:T(8,128)(2,1)} %collective-permute-done.1.w2), channel_id=1, source_target_pairs={{0,1},{1,0},{2,3},{3,2},{4,5},{5,4},{6,7},{7,6},{8,9},{9,8},{10,11... | collective-permute-start | bytes 4718600 | tf_op jit(solution)/shard_map/ppermute | solution.py:299
  35.8 17.4 %all-to-all-done = bf16[32,8,2048]{2,1,0:T(8,128)(2,1)S(1)} async-done(((bf16[32,8,2048]{2,1,0:T(8,128)(2,1)}), bf16[32,8,2048]{2,1,0:T(8,128)(2,1)S(1)}, u32[]{:S(2)}, u32[]{:S(2)}) %all-to-all-start) | async-done | bytes 1048608 | tf_op jit(solution)/shard_map/all_to_all | solution.py:331
  54.2 6.7 %shard_map.158 = (bf16[128,2048]{1,0:T(8,128)(2,1)}, bf16[128,2048]{1,0:T(8,128)(2,1)}, bf16[128,1536]{1,0:T(8,128)(2,1)}, bf16[16,128,128]{2,1,0:T(8,128)(2,1)}) custom-call(bf16[256,2048]{1,0:T(8,128)(2,1)} %bitcast.77, bf16[3,2048,128]{2,1,0:T(8,128)(2,1)} %shard_map.157.w0, bf16[3,2048,128]{2,1,0:T(8,128)(2,1)} %collective-permute-done.w1, ...), custom_call_target="tpu_custom_call" | custom-call | flops 4000000000 | bytes 1048576 | tf_op jit(solution)/shard_map/pallas_call | solution.py:26
  60.8 5.8 %shard_map.165 = (bf16[2,3,2048,128]{3,2,1,0:T(8,128)(2,1)}, bf16[2,3,2048,128]{3,2,1,0:T(8,128)(2,1)}) custom-call(bf16[128,2048]{1,0:T(8,128)(2,1)} %get-tuple-element.49.x_ref, bf16[128,2048]{1,0:T(8,128)(2,1)} %get-tuple-element.50.g_ref, bf16[128,1536]{1,0:T(8,128)(2,1)} %get-tuple-element.51.hid_ref), custom_call_target="tpu_custom_call" | custom-call | flops 8000000000 | bytes 1048576 | tf_op jit(solution)/shard_map/pallas_call | solution.py:26
  68.9 13.6 %all-to-all-start.1 = ((bf16[256,8,128]{2,1,0:T(8,128)(2,1)}), bf16[256,8,128]{2,1,0:T(8,128)(2,1)}, u32[]{:S(2)}, u32[]{:S(2)}) async-start(bf16[256,8,128]{2,1,0:T(8,128)(2,1)} %bitcast.80), calls=%async_computation.1 | async-start | bytes 1048576 | tf_op jit(solution)/shard_map/all_to_all | solution.py:377
  82.5 2.9 %shard_map.160 = (bf16[128,128]{1,0:T(8,128)(2,1)}, f32[128,128]{1,0:T(8,128)}, f32[8,256,128]{2,1,0:T(8,128)}, bf16[8,256,128]{2,1,0:T(8,128)(2,1)}) custom-call(bf16[128,128]{1,0:T(8,128)(2,1)} %saved_ref.3, f32[1,128]{1,0:T(1,128)} %bitcast.90, bf16[128,2048]{1,0:T(8,128)(2,1)} %proj_ref.3), custom_call_target="tpu_custom_call" | custom-call | flops 500000000 | bytes 1048576 | tf_op jit(solution)/shard_map/pallas_call | solution.py:26
  91.8 3.8 %collective-permute-start.10 = (bf16[256,128]{1,0:T(8,128)(2,1)}, bf16[256,128]{1,0:T(8,128)(2,1)S(1)}, u32[]{:S(2)}, u32[]{:S(2)}) collective-permute-start(bf16[256,128]{1,0:T(8,128)(2,1)} %get-tuple-element.43), channel_id=1, source_target_pairs={{0,12},{2,14},{4,0},{6,2},{8,4},{10,6},{12,8},{14,10},{1,13},{3,15... | collective-permute-start | bytes 196616 | tf_op jit(solution)/shard_map/ppermute | solution.py:302
  95.7 3.1 %collective-permute-start.11 = (bf16[256,128]{1,0:T(8,128)(2,1)}, bf16[256,128]{1,0:T(8,128)(2,1)S(1)}, u32[]{:S(2)}, u32[]{:S(2)}) collective-permute-start(bf16[256,128]{1,0:T(8,128)(2,1)} %get-tuple-element.44), channel_id=1, source_target_pairs={{0,14},{2,0},{4,2},{6,4},{8,6},{10,8},{12,10},{14,12},{1,15},{3,1}... | collective-permute-start | bytes 196616 | tf_op jit(solution)/shard_map/ppermute | solution.py:302
  103.3 4.7 %collective-permute-start.7 = (bf16[256,128]{1,0:T(8,128)(2,1)}, bf16[256,128]{1,0:T(8,128)(2,1)S(1)}, u32[]{:S(2)}, u32[]{:S(2)}) collective-permute-start(bf16[256,128]{1,0:T(8,128)(2,1)} %get-tuple-element.40), channel_id=1, source_target_pairs={{0,6},{2,8},{4,10},{6,12},{8,14},{10,0},{12,2},{14,4},{1,7},{3,9},... | collective-permute-start | bytes 196616 | tf_op jit(solution)/shard_map/ppermute | solution.py:302
  108.1 4.3 %collective-permute-start.8 = (bf16[256,128]{1,0:T(8,128)(2,1)}, bf16[256,128]{1,0:T(8,128)(2,1)S(1)}, u32[]{:S(2)}, u32[]{:S(2)}) collective-permute-start(bf16[256,128]{1,0:T(8,128)(2,1)} %get-tuple-element.41), channel_id=1, source_target_pairs={{0,8},{2,10},{4,12},{6,14},{8,0},{10,2},{12,4},{14,6},{1,9},{3,11}... | collective-permute-start | bytes 196616 | tf_op jit(solution)/shard_map/ppermute | solution.py:302
  112.4 5.1 %collective-permute-start.9 = (bf16[256,128]{1,0:T(8,128)(2,1)}, bf16[256,128]{1,0:T(8,128)(2,1)}, u32[]{:S(2)}, u32[]{:S(2)}) collective-permute-start(bf16[256,128]{1,0:T(8,128)(2,1)} %get-tuple-element.42), channel_id=1, source_target_pairs={{0,10},{2,12},{4,14},{6,0},{8,2},{10,4},{12,6},{14,8},{1,11},{3,13... | collective-permute-start | bytes 196616 | tf_op jit(solution)/shard_map/ppermute | solution.py:302
  119.8 2.6 %shard_map.159 = (f32[128,128]{1,0:T(8,128)}, bf16[128,128]{1,0:T(8,128)(2,1)}) custom-call(bf16[256,2048]{1,0:T(8,128)(2,1)} %shard_map.155.table_ref, bf16[2048,128]{1,0:T(8,128)(2,1)} %bitcast.9.home_ref, bf16[128,2048]{1,0:T(8,128)(2,1)} %cot_ref.3), custom_call_target="tpu_custom_call" | custom-call | flops 200000000 | bytes 1048576 | tf_op jit(solution)/shard_map/pallas_call | solution.py:26
  122.3 4.2 %collective-permute-start.3 = (bf16[128,128]{1,0:T(8,128)(2,1)}, bf16[128,128]{1,0:T(8,128)(2,1)S(1)}, u32[]{:S(2)}, u32[]{:S(2)}) collective-permute-start(bf16[128,128]{1,0:T(8,128)(2,1)} %get-tuple-element.34), channel_id=1, source_target_pairs={{0,1},{1,0},{2,3},{3,2},{4,5},{5,4},{6,7},{7,6},{8,9},{9,8},{10,11... | collective-permute-start | bytes 98312 | tf_op jit(solution)/shard_map/ppermute | solution.py:299
  131.5 15.9 %all_to_all.20.mine_ref = bf16[8,136,128]{2,1,0:T(8,128)(2,1)S(1)} all-to-all(bf16[8,136,128]{2,1,0:T(8,128)(2,1)} %shard_map.163), channel_id=1, replica_groups=mesh['z'=8,'x'=4,'y'=8,'c'=2] {'y'}, dimensions={0} | all-to-all | bytes 557056 | tf_op jit(solution)/shard_map/all_to_all | solution.py:413
  151.6 5.3 %shard_map.166 = (bf16[3,2048,128]{2,1,0:T(8,128)(2,1)}, bf16[3,2048,128]{2,1,0:T(8,128)(2,1)}) custom-call(bf16[2,3,2048,128]{3,2,1,0:T(8,128)(2,1)} %get-tuple-element.52.keep_ref, bf16[2,3,2048,128]{3,2,1,0:T(8,128)(2,1)} %copy-done), custom_call_target="tpu_custom_call" | custom-call | flops 1000000 | bytes 9437184 | tf_op jit(solution)/shard_map/pallas_call | solution.py:386
  159.1 2.7 %shard_map.164 = (bf16[2048,128]{1,0:T(8,128)(2,1)}, f32[128,128]{1,0:T(8,128)}) custom-call(bf16[8,136,128]{2,1,0:T(8,128)(2,1)} %copy-done.4, bf16[8,136,128]{2,1,0:T(8,128)(2,1)} %collective-permute-done.12.other_ref, bf16[128,2048]{1,0:T(8,128)(2,1)} %proj_ref.3, bf16[128,128]{1,0:T(8,128)(2,1)} %get-tuple-element.45.act_ref, ...), custom_call_target="tpu_custom_call" | custom-call | flops 2000000000 | bytes 1048576 | tf_op jit(solution)/shard_map/pallas_call | solution.py:26
  161.9 10.1 %all-to-all-start.3 = ((bf16[32,64,128]{2,1,0:T(8,128)(2,1)}), bf16[32,64,128]{2,1,0:T(8,128)(2,1)S(1)}, u32[]{:S(2)}, u32[]{:S(2)}) async-start(bf16[32,64,128]{2,1,0:T(8,128)(2,1)} %bitcast.79), calls=%async_computation.3 | async-start | bytes 1048576 | tf_op jit(solution)/shard_map/all_to_all | solution.py:428
  174.8 2.7 %collective-permute-done.13 = f32[30,128]{1,0:T(8,128)S(1)} collective-permute-done((f32[30,128]{1,0:T(8,128)S(1)}, f32[30,128]{1,0:T(8,128)S(1)}, u32[]{:S(2)}, u32[]{:S(2)}) %collective-permute-start.13) | collective-permute-done | bytes 15392 | tf_op jit(solution)/shard_map/ppermute | solution.py:432
  179.2 9.4 %all-to-all-done.3 = bf16[32,64,128]{2,1,0:T(8,128)(2,1)S(1)} async-done(((bf16[32,64,128]{2,1,0:T(8,128)(2,1)}), bf16[32,64,128]{2,1,0:T(8,128)(2,1)S(1)}, u32[]{:S(2)}, u32[]{:S(2)}) %all-to-all-start.3) | async-done | bytes 524320 | tf_op jit(solution)/shard_map/all_to_all | solution.py:428
  190.5 3.1 %shard_map.167 = (bf16[2048,128]{1,0:T(8,128)(2,1)}, bf16[2048,128]{1,0:T(8,128)(2,1)}, bf16[128,2048]{1,0:T(8,128)(2,1)}) custom-call(bf16[3,2048,128]{2,1,0:T(8,128)(2,1)} %get-tuple-element.54.pre_ref, bf16[3,2048,128]{2,1,0:T(8,128)(2,1)} %copy-done.1), custom_call_target="tpu_custom_call" | custom-call | flops 1000000 | bytes 1048576 | tf_op jit(solution)/shard_map/pallas_call | solution.py:26
  (61 shorter events, 36.0 us)
Async XLA Ops:
  3.2 24.0 %collective-permute-start.1 = (bf16[3,2048,128]{2,1,0:T(8,128)(2,1)}, bf16[3,2048,128]{2,1,0:T(8,128)(2,1)}, u32[]{:S(2)}, u32[]{:S(2)}) collective-permute-start(bf16[3,2048,128]{2,1,0:T(8,128)(2,1)} %shard_map.157.w0), channel_id=1, source_target_pairs={{0,2},{1,15},{2,4},{3,1},{4,6},{5,3},{6,8},{7,5},{8,10},{9,7},{10,... | collective-permute-start | bytes 4718600 | tf_op jit(solution)/shard_map/ppermute | solution.py:309
  12.2 13.0 %copy-start.2 = (bf16[3,2048,128]{2,1,0:T(8,128)(2,1)S(1)}, bf16[3,2048,128]{2,1,0:T(8,128)(2,1)}, u32[]{:S(2)}) copy-start(bf16[3,2048,128]{2,1,0:T(8,128)(2,1)} %shard_map.157.w0) | copy-start | bytes 4718596
  12.2 41.0 %all-to-all-start = ((bf16[32,8,2048]{2,1,0:T(8,128)(2,1)}), bf16[32,8,2048]{2,1,0:T(8,128)(2,1)S(1)}, u32[]{:S(2)}, u32[]{:S(2)}) async-start(bf16[32,8,2048]{2,1,0:T(8,128)(2,1)} %bitcast.78), calls=%async_computation | async-start | bytes 2097152 | tf_op jit(solution)/shard_map/all_to_all | solution.py:331
  25.2 10.6 %collective-permute-start = (bf16[3,2048,128]{2,1,0:T(8,128)(2,1)S(1)}, bf16[3,2048,128]{2,1,0:T(8,128)(2,1)}, u32[]{:S(2)}, u32[]{:S(2)}) collective-permute-start(bf16[3,2048,128]{2,1,0:T(8,128)(2,1)S(1)} %copy-done.2), channel_id=1, source_target_pairs={{0,1},{1,0},{2,3},{3,2},{4,5},{5,4},{6,7},{7,6},{8,9},{9,8},{10,11... | collective-permute-start | bytes 4718600 | tf_op jit(solution)/shard_map/ppermute | solution.py:299
  27.2 26.0 %collective-permute-start.2 = (bf16[3,2048,128]{2,1,0:T(8,128)(2,1)}, bf16[3,2048,128]{2,1,0:T(8,128)(2,1)}, u32[]{:S(2)}, u32[]{:S(2)}) collective-permute-start(bf16[3,2048,128]{2,1,0:T(8,128)(2,1)} %collective-permute-done.1.w2), channel_id=1, source_target_pairs={{0,1},{1,0},{2,3},{3,2},{4,5},{5,4},{6,7},{7,6},{8,9},{9,8},{10,11... | collective-permute-start | bytes 4718600 | tf_op jit(solution)/shard_map/ppermute | solution.py:299
  66.6 83.3 %collective-permute-start.14 = (bf16[2,3,2048,128]{3,2,1,0:T(8,128)(2,1)}, bf16[2,3,2048,128]{3,2,1,0:T(8,128)(2,1)S(1)}, u32[]{:S(2)}, u32[]{:S(2)}) collective-permute-start(bf16[2,3,2048,128]{3,2,1,0:T(8,128)(2,1)} %get-tuple-element.53), channel_id=1, source_target_pairs={{0,1},{1,0},{2,3},{3,2},{4,5},{5,4},{6,7},{7,6},{8,9},{9,8},{10,11... | collective-permute-start | bytes 9437192 | tf_op jit(solution)/shard_map/ppermute | solution.py:299
  68.9 50.9 %all-to-all-start.1 = ((bf16[256,8,128]{2,1,0:T(8,128)(2,1)}), bf16[256,8,128]{2,1,0:T(8,128)(2,1)}, u32[]{:S(2)}, u32[]{:S(2)}) async-start(bf16[256,8,128]{2,1,0:T(8,128)(2,1)} %bitcast.80), calls=%async_computation.1 | async-start | bytes 1048576 | tf_op jit(solution)/shard_map/all_to_all | solution.py:377
  85.5 4.1 %collective-permute-start.4 = (bf16[8,256,128]{2,1,0:T(8,128)(2,1)}, bf16[8,256,128]{2,1,0:T(8,128)(2,1)}, u32[]{:S(2)}, u32[]{:S(2)}) collective-permute-start(bf16[8,256,128]{2,1,0:T(8,128)(2,1)} %get-tuple-element.36), channel_id=1, source_target_pairs={{0,1},{1,0},{2,3},{3,2},{4,5},{5,4},{6,7},{7,6},{8,9},{9,8},{10,11... | collective-permute-start | bytes 1572872 | tf_op jit(solution)/shard_map/ppermute | solution.py:299
  91.8 11.5 %collective-permute-start.10 = (bf16[256,128]{1,0:T(8,128)(2,1)}, bf16[256,128]{1,0:T(8,128)(2,1)S(1)}, u32[]{:S(2)}, u32[]{:S(2)}) collective-permute-start(bf16[256,128]{1,0:T(8,128)(2,1)} %get-tuple-element.43), channel_id=1, source_target_pairs={{0,12},{2,14},{4,0},{6,2},{8,4},{10,6},{12,8},{14,10},{1,13},{3,15... | collective-permute-start | bytes 196616 | tf_op jit(solution)/shard_map/ppermute | solution.py:302
  95.7 12.4 %collective-permute-start.11 = (bf16[256,128]{1,0:T(8,128)(2,1)}, bf16[256,128]{1,0:T(8,128)(2,1)S(1)}, u32[]{:S(2)}, u32[]{:S(2)}) collective-permute-start(bf16[256,128]{1,0:T(8,128)(2,1)} %get-tuple-element.44), channel_id=1, source_target_pairs={{0,14},{2,0},{4,2},{6,4},{8,6},{10,8},{12,10},{14,12},{1,15},{3,1}... | collective-permute-start | bytes 196616 | tf_op jit(solution)/shard_map/ppermute | solution.py:302
  98.8 13.6 %collective-permute-start.5 = (bf16[256,128]{1,0:T(8,128)(2,1)}, bf16[256,128]{1,0:T(8,128)(2,1)S(1)}, u32[]{:S(2)}, u32[]{:S(2)}) collective-permute-start(bf16[256,128]{1,0:T(8,128)(2,1)} %get-tuple-element.38), channel_id=1, source_target_pairs={{0,2},{2,4},{4,6},{6,8},{8,10},{10,12},{12,14},{14,0},{1,3},{3,5},... | collective-permute-start | bytes 196616 | tf_op jit(solution)/shard_map/ppermute | solution.py:302
  101.0 21.4 %collective-permute-start.6 = (bf16[256,128]{1,0:T(8,128)(2,1)}, bf16[256,128]{1,0:T(8,128)(2,1)S(1)}, u32[]{:S(2)}, u32[]{:S(2)}) collective-permute-start(bf16[256,128]{1,0:T(8,128)(2,1)} %get-tuple-element.39), channel_id=1, source_target_pairs={{0,4},{2,6},{4,8},{6,10},{8,12},{10,14},{12,0},{14,2},{1,5},{3,7},... | collective-permute-start | bytes 196616 | tf_op jit(solution)/shard_map/ppermute | solution.py:302
  103.3 16.4 %copy-start.5 = (bf16[256,128]{1,0:T(8,128)(2,1)}, bf16[256,128]{1,0:T(8,128)(2,1)S(1)}, u32[]{:S(2)}) copy-start(bf16[256,128]{1,0:T(8,128)(2,1)S(1)} %collective-permute-done.10.refs_5_) | copy-start | bytes 196612
  103.3 23.2 %collective-permute-start.7 = (bf16[256,128]{1,0:T(8,128)(2,1)}, bf16[256,128]{1,0:T(8,128)(2,1)S(1)}, u32[]{:S(2)}, u32[]{:S(2)}) collective-permute-start(bf16[256,128]{1,0:T(8,128)(2,1)} %get-tuple-element.40), channel_id=1, source_target_pairs={{0,6},{2,8},{4,10},{6,12},{8,14},{10,0},{12,2},{14,4},{1,7},{3,9},... | collective-permute-start | bytes 196616 | tf_op jit(solution)/shard_map/ppermute | solution.py:302
  108.1 11.7 %copy-start.6 = (bf16[256,128]{1,0:T(8,128)(2,1)}, bf16[256,128]{1,0:T(8,128)(2,1)S(1)}, u32[]{:S(2)}) copy-start(bf16[256,128]{1,0:T(8,128)(2,1)S(1)} %collective-permute-done.11.refs_6_) | copy-start | bytes 196612
  108.1 18.5 %collective-permute-start.8 = (bf16[256,128]{1,0:T(8,128)(2,1)}, bf16[256,128]{1,0:T(8,128)(2,1)S(1)}, u32[]{:S(2)}, u32[]{:S(2)}) collective-permute-start(bf16[256,128]{1,0:T(8,128)(2,1)} %get-tuple-element.41), channel_id=1, source_target_pairs={{0,8},{2,10},{4,12},{6,14},{8,0},{10,2},{12,4},{14,6},{1,9},{3,11}... | collective-permute-start | bytes 196616 | tf_op jit(solution)/shard_map/ppermute | solution.py:302
  112.4 14.2 %collective-permute-start.9 = (bf16[256,128]{1,0:T(8,128)(2,1)}, bf16[256,128]{1,0:T(8,128)(2,1)}, u32[]{:S(2)}, u32[]{:S(2)}) collective-permute-start(bf16[256,128]{1,0:T(8,128)(2,1)} %get-tuple-element.42), channel_id=1, source_target_pairs={{0,10},{2,12},{4,14},{6,0},{8,2},{10,4},{12,6},{14,8},{1,11},{3,13... | collective-permute-start | bytes 196616 | tf_op jit(solution)/shard_map/ppermute | solution.py:302
  122.3 6.7 %collective-permute-start.3 = (bf16[128,128]{1,0:T(8,128)(2,1)}, bf16[128,128]{1,0:T(8,128)(2,1)S(1)}, u32[]{:S(2)}, u32[]{:S(2)}) collective-permute-start(bf16[128,128]{1,0:T(8,128)(2,1)} %get-tuple-element.34), channel_id=1, source_target_pairs={{0,1},{1,0},{2,3},{3,2},{4,5},{5,4},{6,7},{7,6},{8,9},{9,8},{10,11... | collective-permute-start | bytes 98312 | tf_op jit(solution)/shard_map/ppermute | solution.py:299
  147.4 11.7 %copy-start.4 = (bf16[8,136,128]{2,1,0:T(8,128)(2,1)}, bf16[8,136,128]{2,1,0:T(8,128)(2,1)S(1)}, u32[]{:S(2)}) copy-start(bf16[8,136,128]{2,1,0:T(8,128)(2,1)S(1)} %all_to_all.20.mine_ref) | copy-start | bytes 835588
  147.4 11.7 %collective-permute-start.12 = (bf16[8,136,128]{2,1,0:T(8,128)(2,1)S(1)}, bf16[8,136,128]{2,1,0:T(8,128)(2,1)}, u32[]{:S(2)}, u32[]{:S(2)}) collective-permute-start(bf16[8,136,128]{2,1,0:T(8,128)(2,1)S(1)} %all_to_all.20.mine_ref), channel_id=1, source_target_pairs={{0,1},{1,0},{2,3},{3,2},{4,5},{5,4},{6,7},{7,6},{8,9},{9,8},{10,11... | collective-permute-start | bytes 835592 | tf_op jit(solution)/shard_map/ppermute | solution.py:299
  156.9 32.4 %collective-permute-start.15 = (bf16[3,2048,128]{2,1,0:T(8,128)(2,1)}, bf16[3,2048,128]{2,1,0:T(8,128)(2,1)S(1)}, u32[]{:S(2)}, u32[]{:S(2)}) collective-permute-start(bf16[3,2048,128]{2,1,0:T(8,128)(2,1)} %get-tuple-element.55), channel_id=1, source_target_pairs={{0,14},{1,3},{2,0},{3,5},{4,2},{5,7},{6,4},{7,9},{8,6},{9,11},{10,... | collective-permute-start | bytes 4718600 | tf_op jit(solution)/shard_map/ppermute | solution.py:309
  159.1 12.8 %copy-start.12 = (f32[31,128]{1,0:T(8,128)S(1)}, f32[31,128]{1,0:T(8,128)}, u32[]{:S(2)}) copy-start(f32[31,128]{1,0:T(8,128)} %param.19) | copy-start | bytes 47620
  161.9 26.8 %all-to-all-start.3 = ((bf16[32,64,128]{2,1,0:T(8,128)(2,1)}), bf16[32,64,128]{2,1,0:T(8,128)(2,1)S(1)}, u32[]{:S(2)}, u32[]{:S(2)}) async-start(bf16[32,64,128]{2,1,0:T(8,128)(2,1)} %bitcast.79), calls=%async_computation.3 | async-start | bytes 1048576 | tf_op jit(solution)/shard_map/all_to_all | solution.py:428
  172.7 4.9 %collective-permute-start.13 = (f32[30,128]{1,0:T(8,128)S(1)}, f32[30,128]{1,0:T(8,128)S(1)}, u32[]{:S(2)}, u32[]{:S(2)}) collective-permute-start(f32[30,128]{1,0:T(8,128)S(1)} %slice.188), channel_id=1, source_target_pairs={{16,0},{32,16},{48,32},{64,48},{80,64},{96,80},{112,96},{128,112},... | collective-permute-start | bytes 46088 | tf_op jit(solution)/shard_map/ppermute | solution.py:432
  (8 other events, 17.4 us)

commit v5 on v4

--- a/solution.py
+++ b/solution.py
@@ -1,3 +1,5 @@
+import functools
+
 import jax
 import jax.numpy as jnp
 from jax import lax
@@ -22,13 +24,15 @@
     return lax.broadcasted_iota(I32, shape, dim)
 
 
-def kernel(body, outs, flops, *args, scratch=(), far=(), near=True):
+def kernel(body, outs, flops, *args, scratch=(), far=(), far_out=()):
+    many = outs if isinstance(outs, tuple) else (outs,)
+    specs = [ANY if i in far_out else VMEM for i in range(len(many))]
     return pl.pallas_call(
         body,
         out_shape=outs,
         in_specs=[ANY if i in far else VMEM for i in range(len(args))],
+        out_specs=specs if isinstance(outs, tuple) else specs[0],
         scratch_shapes=list(scratch),
-        out_specs=jax.tree.map(lambda _: VMEM if near else ANY, outs),
         cost_estimate=pl.CostEstimate(flops=flops, bytes_accessed=1 << 20, transcendentals=0),
     )(*args)
 
@@ -37,7 +41,22 @@
     return jax.ShapeDtypeStruct(dims, kind)
 
 
-def head_body(ids_ref, weight_ref, mix_ref, cot_ref, out_ref):
+def head_body(
+    ids_ref, weight_ref, mix_ref, cot_ref, gate_ref, up_ref, down_ref, out_ref, pack_ref, buf_ref, sem
+):
+    load = []
+    for m, ref in enumerate((gate_ref, up_ref)):
+        load.append([pltpu.make_async_copy(ref, buf_ref.at[m], sem.at[m, 0])])
+    down = []
+    for j in range(down_ref.shape[1] // 128):
+        at = slice(j * 128, (j + 1) * 128)
+        down.append(
+            pltpu.make_async_copy(down_ref.at[:, at], buf_ref.at[2, at], sem.at[2 + j, 0])
+        )
+    load.append(down)
+    for copies in load:
+        for copy in copies:
+            copy.start()
     tok = ids_ref.shape[1]
     experts = out_ref.shape[0] // (2 * SPAN)
     group = (lax.axis_index("y") % 2) * 2 + lax.axis_index("c")
@@ -63,10 +82,18 @@
     take_x = jnp.where(found & is_x, 1.0, 0.0).astype(BF)
     take_g = jnp.where(found & ~is_x, 1.0, 0.0).astype(BF)
     scale = jnp.where(iota((rows, 1), 0) % (2 * SPAN) < SPAN, 1.0, scale)
+    store = []
+    for m, copies in enumerate(load):
+        for copy in copies:
+            copy.wait()
+        store.append(pltpu.make_async_copy(buf_ref.at[m], pack_ref.at[m], sem.at[m, 1]))
+        store[-1].start()
     step = 512
     for at in range(0, mix_ref.shape[1], step):
         picked = mm(take_x, mix_ref[:, at : at + step]) + mm(take_g, cot_ref[:, at : at + step])
         out_ref[:, at : at + step] = (picked * scale).astype(BF)
+    for copy in store:
+        copy.wait()
 
 
 def table_body(ids_ref, out_ref):
@@ -91,31 +118,6 @@
     out_ref[tok:, :] = jnp.where(hit & (half != ci), 1.0, 0.0).astype(BF)
 
 
-def pack_body(gate_ref, up_ref, down_ref, out_ref, buf_ref, sem):
-    blocks = down_ref.shape[1] // 128
-    load, store = [], []
-    for m, ref in enumerate((gate_ref, up_ref)):
-        load.append(pltpu.make_async_copy(ref, buf_ref.at[m], sem.at[m, 0]))
-    down = [
-        pltpu.make_async_copy(
-            down_ref.at[:, j * 128 : (j + 1) * 128],
-            buf_ref.at[2, j * 128 : (j + 1) * 128],
-            sem.at[2 + j, 0],
-        )
-        for j in range(blocks)
-    ]
-    for copy in (*load, *down):
-        copy.start()
-    for m in range(3):
-        for copy in load[m : m + 1] if m < 2 else down:
-            copy.wait()
-        copy = pltpu.make_async_copy(buf_ref.at[m], out_ref.at[m], sem.at[m, 1])
-        copy.start()
-        store.append(copy)
-    for copy in store:
-        copy.wait()
-
-
 def slope_body(saved_ref, gain_ref, proj_ref, act_ref, slope_ref, keep_ref, give_ref):
     ci = lax.axis_index("c")
     saved = saved_ref[...].astype(F32)
@@ -135,20 +137,11 @@
             ref[y] = (mm(high, part) + mm(low, part)).astype(ref.dtype)
 
 
-def share_body(keep_ref, given_ref, own_ref, *out_refs):
-    yi = lax.axis_index("y")
-    ny = keep_ref.shape[0]
-    own_ref[...] = keep_ref[yi] + given_ref[yi].astype(F32)
-    for k, ref in enumerate(out_refs, 1):
-        to = lax.rem(yi + k, ny)
-        ref[...] = (keep_ref[to] + given_ref[to].astype(F32)).astype(BF)
-
-
-def total_body(own_ref, *refs):
-    total = own_ref[...]
-    for ref in refs[:-1]:
-        total = total + ref[...].astype(F32)
-    refs[-1][...] = total
+def share_body(bit, keep_ref, given_ref, own_ref, send_ref):
+    side = lax.rem(lax.axis_index("y") // (1 << bit), 2)
+    for i in range(keep_ref.shape[0] // 2):
+        for ref, at in ((own_ref, 2 * i + side), (send_ref, 2 * i + 1 - side)):
+            ref[i] = (keep_ref[at] + given_ref[at].astype(F32)).astype(ref.dtype)
 
 
 def expert_body(got_ref, w0, w1, w2, w3, x_ref, g_ref, hid_ref, back_ref, in_ref, down_ref, sem):
@@ -224,13 +217,14 @@
     other_ref[...] = both[tok:].astype(BF)
 
 
-def mix_body(own_ref, other_ref, total_ref, out_ref):
+def mix_body(own_ref, other_ref, vown_ref, vgot_ref, out_ref):
     tok = own_ref.shape[0]
+    total = vown_ref[0] + vgot_ref[0].astype(F32)
     mix = (own_ref[...] + other_ref[...].astype(F32)).astype(BF)
     wide = mix.astype(F32)
     parts = []
     for k in range(2):
-        rest = jnp.sum((wide * total_ref[k * tok : (k + 1) * tok, :]).T, axis=0, keepdims=True)
+        rest = jnp.sum((wide * total[k * tok : (k + 1) * tok, :]).T, axis=0, keepdims=True)
         for _ in range(3):
             parts.append(rest.astype(BF).astype(F32))
             rest = rest - parts[-1]
@@ -241,20 +235,18 @@
         out_ref[y, tok:, :] = sums
 
 
-def final_body(mine_ref, other_ref, proj_ref, act_ref, slope_ref, saved_ref, dev_ref, out_ref, conv_ref):
-    ci = lax.axis_index("c")
+def final_body(all_ref, proj_ref, act_ref, slope_ref, saved_ref, dev_ref, out_ref, conv_ref):
     tok = act_ref.shape[0]
     acc = jnp.zeros((tok, tok), F32)
     sums = jnp.zeros((8, tok), F32)
-    for y in range(mine_ref.shape[0]):
-        for ref, cc in ((mine_ref, ci), (other_ref, 1 - ci)):
-            at = pl.ds(pl.multiple_of((2 * y + cc) * 128, 128), 128)
-            part = ref[y, :tok, :]
-            sums = sums + ref[y, tok:, :].astype(F32)
-            out_ref[at, :] = mm(part, act_ref[...], FIRST).astype(BF)
-            acc = acc + mm(part, proj_ref[:, at], LAST)
+    for t in range(all_ref.shape[0]):
+        at = slice(t * 128, (t + 1) * 128)
+        part = all_ref[t, :tok, :]
+        sums = sums + all_ref[t, tok:, :].astype(F32)
+        out_ref[at, :] = mm(part, act_ref[...], FIRST).astype(BF)
+        acc = acc + mm(part, proj_ref[:, at], LAST)
     grad = acc * slope_ref[...]
-    count = 2 * mine_ref.shape[0] * 128
+    count = all_ref.shape[0] * 128
     means = []
     for k in range(2):
         total = jnp.sum(sums[3 * k : 3 * k + 3], axis=0, keepdims=True) / count
@@ -298,8 +290,8 @@
     def flip_c(value):
         return lax.ppermute(value, "c", [(0, 1), (1, 0)])
 
-    def shift(value, k):
-        return lax.ppermute(value, "y", [(i, (i + k) % ny) for i in range(ny)])
+    def flip_y(value, bit):
+        return lax.ppermute(value, "y", [(i, i ^ (1 << bit)) for i in range(ny)])
 
     def hop(value, sign):
         pairs = []
@@ -308,26 +300,27 @@
                 pairs.append((2 * y + c, 2 * ((y + (sign if c == 0 else -sign)) % ny) + c))
         return lax.ppermute(value, ("y", "c"), pairs)
 
-    own = kernel(
-        pack_body,
-        shape(3, width, 128),
-        1000000,
+    rows = experts * 2 * SPAN
+    ids, weights = expert_ids.T, route_weight.T
+    sent, own = kernel(
+        head_body,
+        (shape(rows, width), shape(3, width, 128)),
+        2000000000,
+        ids,
+        weights,
+        mixer_out,
+        cotangent,
         gate_weight[0],
         up_weight[0],
         down_weight[0],
-        far=(0, 1, 2),
-        near=False,
+        far=(4, 5, 6),
+        far_out=(1,),
         scratch=(pltpu.VMEM((3, width, 128), BF), pltpu.SemaphoreType.DMA((2 + width // 128, 2))),
     )
     by_y = hop(own, 1)
     by_c = flip_c(own)
     by_yc = flip_c(by_y)
 
-    rows = experts * 2 * SPAN
-    ids, weights = expert_ids.T, route_weight.T
-    sent = kernel(
-        head_body, shape(rows, width), 2000000000, ids, weights, mixer_out, cotangent
-    )
     got = lax.all_to_all(sent.reshape(experts, 2 * SPAN, width), sp, 0, 0, tiled=True)
     table = kernel(table_body, shape(2 * tok, experts * ny * 2 * SPAN), 2000000000, ids)
 
@@ -345,17 +338,16 @@
         proj_weight,
     )
     vgiven = flip_c(vgive)
-    vown, *vsent = kernel(
-        share_body,
-        (shape(2 * tok, 128, kind=F32), *[shape(2 * tok, 128)] * (ny - 1)),
-        1000000,
-        vkeep,
-        vgiven,
-    )
-    vgot = []
-    for k, value in enumerate(vsent, 1):
-        vgot.append(shift(value, k))
-    vtotal = kernel(total_body, shape(2 * tok, 128, kind=F32), 1000000, vown, *vgot)
+    for bit in range(3):
+        half = ny >> (bit + 1)
+        vkeep, vgive = kernel(
+            functools.partial(share_body, bit),
+            (shape(half, 2 * tok, 128, kind=F32), shape(half, 2 * tok, 128)),
+            1000000,
+            vkeep,
+            vgiven,
+        )
+        vgiven = flip_y(vgive, bit)
 
     slots = experts * SPAN
     x, g, hidden, back = kernel(
@@ -409,16 +401,16 @@
         cotangent,
     )
     other = flip_c(other)
-    mix = kernel(mix_body, shape(ny, tok + 8, 128), 1000000, mine, other, vtotal)
-    mine_all = lax.all_to_all(mix, "y", 0, 0, tiled=True)
-    other_all = flip_c(mine_all)
+    mix = kernel(
+        mix_body, shape(2 * ny, tok + 8, 128), 1000000, mine, other, vkeep, vgiven
+    )
+    mix_all = lax.all_to_all(mix, ("y", "c"), 0, 0, tiled=True)
 
     proj, conv = kernel(
         final_body,
         (shape(width, 128), shape(tok, 128, kind=F32)),
         2000000000,
-        mine_all,
-        other_all,
+        mix_all,
         proj_weight,
         act_conv,
         slope,

time: 195 us -> 193 us (0.990)
  waiting for transfers between devices: 31.5 us -> 51.1 us
  blocking collectives: 15.9 us -> 0 us
  starting transfers between devices: 93.3 us -> 86.3 us
    all_to_all x1 -> x0, blocking collectives: 15.9 us -> none  [shards(): mine_all = lax.all_to_all(mix, 'y', 0, 0, tiled=True)]
    ppermute x7 -> x3, waiting for transfers between devices: 0.02 us -> 12.5 us  [flip_y(): return lax.ppermute(value, 'y', [(i, i ^ 1 << bit) for i in range(ny)])]
    ppermute x7 -> x3, starting transfers between devices: 25.6 us -> 16.7 us  [flip_y(): return lax.ppermute(value, 'y', [(i, i ^ 1 << bit) for i in range(ny)])]
    all_to_all x0 -> x1, waiting for transfers between devices: none -> 7.84 us  [shards(): mix_all = lax.all_to_all(mix, ('y', 'c'), 0, 0, tiled=True)]
    all_to_all x0 -> x1, starting transfers between devices: none -> 4.32 us  [shards(): mix_all = lax.all_to_all(mix, ('y', 'c'), 0, 0, tiled=True)]
    all_to_all x1, waiting for transfers between devices: 17.4 us -> 14.2 us  [shards(): lax.all_to_all(sent.reshape(experts, 2 * SPAN, width), sp, 0, 0, tiled=True)]
    ppermute x6 -> x5, starting transfers between devices: 21.7 us -> 18.6 us  [flip_c(): return lax.ppermute(value, 'c', [(0, 1), (1, 0)])]
    ppermute x2, waiting for transfers between devices: 0.01 us -> 2.81 us  [hop(): return lax.ppermute(value, ('y', 'c'), pairs)]
  transfers between devices with their start and end apart: 19 -> 15, of which waited for: 4 -> 8; matrix products, arithmetic and copies ran while one was open for 2% -> 2% of each run, Pallas kernels for 13% -> 12%
where the time goes in v5:
time: 193 us; the launch traced here: 192 us
  starting transfers between devices  86.3 us (45%)
  waiting for transfers between devices  51.1 us (26%)
  Pallas kernels  43.9 us (23%)
  local copies, waits for them, and re-layouts  7.41 us (4%)
  other arithmetic  2.33 us (1%)
    pallas_call x12, Pallas kernels, kernel(): pl.pallas_call(body, out_shape=outs, in_specs=[ANY if i in far else VMEM...  38.6 us
    ppermute x5, starting transfers between devices, flip_c(): return lax.ppermute(value, 'c', [(0, 1), (1, 0)])  18.6 us
    ppermute x3, starting transfers between devices, flip_y(): return lax.ppermute(value, 'y', [(i, i ^ 1 << bit) for i in range(ny)])  16.7 us
    all_to_all x1, waiting for transfers between devices, shards(): lax.all_to_all(sent.reshape(experts, 2 * SPAN, width), sp, 0, 0, tiled=True)  14.2 us
    all_to_all x1, starting transfers between devices, shards(): lax.all_to_all(back.reshape(experts * ny, 2 * SPAN, 128), ('z', 'x', 'y')...  13.5 us
    all_to_all x1, starting transfers between devices, shards(): lax.all_to_all(sent.reshape(experts, 2 * SPAN, width), sp, 0, 0, tiled=True)  12.9 us
    ppermute x3, waiting for transfers between devices, flip_y(): return lax.ppermute(value, 'y', [(i, i ^ 1 << bit) for i in range(ny)])  12.5 us
    all_to_all x1, starting transfers between devices, shards(): proj = lax.all_to_all(proj.reshape(experts, -1, 128), sp, 0, 0, tiled=True)  9.75 us
  transfers between devices with their start and end apart: 15, of which 8 were waited for; matrix products, arithmetic and copies ran while one was open for 2% of the time, Pallas kernels for 12%

profile of v5, /device:TPU:1, one launch (start us, length us, event | category | flops | bytes accessed | tf_op | source)
XLA Modules:
  0.0 191.9 jit_solution(15997051691940485248)
XLA Ops:
  0.6 4.8 %shard_map.156 = (bf16[256,2048]{1,0:T(8,128)(2,1)}, bf16[3,2048,128]{2,1,0:T(8,128)(2,1)}) custom-call(s32[2,128]{1,0:T(2,128)} %bitcast.88, f32[2,128]{1,0:T(2,128)} %bitcast.87, bf16[128,2048]{1,0:T(8,128)(2,1)} %mix_ref.1, bf16[128,2048]{1,0:T(8,128)(2,1)} %cot_ref.3, bf16[2048,128]{1,0:T(8,128)(2,1)} %bitcast.81, bf16[2048,128]{1,0:T(8,128)(2,1)} %bitcast.82, ...), custom_call_target="tpu_custom_call" | custom-call | flops 2000000000 | bytes 1048576 | tf_op jit(solution)/shard_map/pallas_call | solution.py:30
  5.4 6.0 %collective-permute-start.1 = (bf16[3,2048,128]{2,1,0:T(8,128)(2,1)}, bf16[3,2048,128]{2,1,0:T(8,128)(2,1)}, u32[]{:S(2)}, u32[]{:S(2)}) collective-permute-start(bf16[3,2048,128]{2,1,0:T(8,128)(2,1)} %get-tuple-element.33.w0), channel_id=1, source_target_pairs={{0,2},{1,15},{2,4},{3,1},{4,6},{5,3},{6,8},{7,5},{8,10},{9,7},{10,... | collective-permute-start | bytes 4718600 | tf_op jit(solution)/shard_map/ppermute | solution.py:301
  11.5 12.9 %all-to-all-start = ((bf16[32,8,2048]{2,1,0:T(8,128)(2,1)}), bf16[32,8,2048]{2,1,0:T(8,128)(2,1)S(1)}, u32[]{:S(2)}, u32[]{:S(2)}) async-start(bf16[32,8,2048]{2,1,0:T(8,128)(2,1)} %bitcast.78), calls=%async_computation | async-start | bytes 2097152 | tf_op jit(solution)/shard_map/all_to_all | solution.py:324
  26.3 2.8 %collective-permute-done.1.w2 = bf16[3,2048,128]{2,1,0:T(8,128)(2,1)} collective-permute-done((bf16[3,2048,128]{2,1,0:T(8,128)(2,1)}, bf16[3,2048,128]{2,1,0:T(8,128)(2,1)}, u32[]{:S(2)}, u32[]{:S(2)}) %collective-permute-start.1) | collective-permute-done | bytes 1572896 | tf_op jit(solution)/shard_map/ppermute | solution.py:301
  29.1 9.0 %collective-permute-start.2 = (bf16[3,2048,128]{2,1,0:T(8,128)(2,1)}, bf16[3,2048,128]{2,1,0:T(8,128)(2,1)}, u32[]{:S(2)}, u32[]{:S(2)}) collective-permute-start(bf16[3,2048,128]{2,1,0:T(8,128)(2,1)} %collective-permute-done.1.w2), channel_id=1, source_target_pairs={{0,1},{1,0},{2,3},{3,2},{4,5},{5,4},{6,7},{7,6},{8,9},{9,8},{10,11... | collective-permute-start | bytes 4718600 | tf_op jit(solution)/shard_map/ppermute | solution.py:291
  38.1 14.2 %all-to-all-done = bf16[32,8,2048]{2,1,0:T(8,128)(2,1)S(1)} async-done(((bf16[32,8,2048]{2,1,0:T(8,128)(2,1)}), bf16[32,8,2048]{2,1,0:T(8,128)(2,1)S(1)}, u32[]{:S(2)}, u32[]{:S(2)}) %all-to-all-start) | async-done | bytes 1048608 | tf_op jit(solution)/shard_map/all_to_all | solution.py:324
  53.3 6.7 %shard_map.157 = (bf16[128,2048]{1,0:T(8,128)(2,1)}, bf16[128,2048]{1,0:T(8,128)(2,1)}, bf16[128,1536]{1,0:T(8,128)(2,1)}, bf16[16,128,128]{2,1,0:T(8,128)(2,1)}) custom-call(bf16[256,2048]{1,0:T(8,128)(2,1)} %bitcast.77, bf16[3,2048,128]{2,1,0:T(8,128)(2,1)} %get-tuple-element.33.w0, bf16[3,2048,128]{2,1,0:T(8,128)(2,1)} %collective-permute-done.w1, ...), custom_call_target="tpu_custom_call" | custom-call | flops 4000000000 | bytes 1048576 | tf_op jit(solution)/shard_map/pallas_call | solution.py:30
  60.0 5.8 %shard_map.165 = (bf16[2,3,2048,128]{3,2,1,0:T(8,128)(2,1)}, bf16[2,3,2048,128]{3,2,1,0:T(8,128)(2,1)}) custom-call(bf16[128,2048]{1,0:T(8,128)(2,1)} %get-tuple-element.49.x_ref, bf16[128,2048]{1,0:T(8,128)(2,1)} %get-tuple-element.50.g_ref, bf16[128,1536]{1,0:T(8,128)(2,1)} %get-tuple-element.51.hid_ref), custom_call_target="tpu_custom_call" | custom-call | flops 8000000000 | bytes 1048576 | tf_op jit(solution)/shard_map/pallas_call | solution.py:30
  68.0 2.9 %shard_map.159 = (bf16[128,128]{1,0:T(8,128)(2,1)}, f32[128,128]{1,0:T(8,128)}, f32[8,256,128]{2,1,0:T(8,128)}, bf16[8,256,128]{2,1,0:T(8,128)(2,1)}) custom-call(bf16[128,128]{1,0:T(8,128)(2,1)} %saved_ref.3, f32[1,128]{1,0:T(1,128)} %bitcast.90, bf16[128,2048]{1,0:T(8,128)(2,1)} %proj_ref.3), custom_call_target="tpu_custom_call" | custom-call | flops 500000000 | bytes 1048576 | tf_op jit(solution)/shard_map/pallas_call | solution.py:30
  73.0 13.5 %all-to-all-start.1 = ((bf16[256,8,128]{2,1,0:T(8,128)(2,1)}), bf16[256,8,128]{2,1,0:T(8,128)(2,1)}, u32[]{:S(2)}, u32[]{:S(2)}) async-start(bf16[256,8,128]{2,1,0:T(8,128)(2,1)} %bitcast.80), calls=%async_computation.1 | async-start | bytes 1048576 | tf_op jit(solution)/shard_map/all_to_all | solution.py:369
  90.8 9.9 %collective-permute-done.5.given_ref = bf16[4,256,128]{2,1,0:T(8,128)(2,1)S(1)} collective-permute-done((bf16[4,256,128]{2,1,0:T(8,128)(2,1)}, bf16[4,256,128]{2,1,0:T(8,128)(2,1)S(1)}, u32[]{:S(2)}, u32[]{:S(2)}) %collective-permute-start.5) | collective-permute-done | bytes 262176 | tf_op jit(solution)/shard_map/ppermute | solution.py:294
  103.3 4.3 %collective-permute-start.6 = (bf16[2,256,128]{2,1,0:T(8,128)(2,1)}, bf16[2,256,128]{2,1,0:T(8,128)(2,1)S(1)}, u32[]{:S(2)}, u32[]{:S(2)}) collective-permute-start(bf16[2,256,128]{2,1,0:T(8,128)(2,1)} %get-tuple-element.42), channel_id=1, source_target_pairs={{0,4},{2,6},{4,0},{6,2},{8,12},{10,14},{12,8},{14,10},{1,5},{3,7},... | collective-permute-start | bytes 393224 | tf_op jit(solution)/shard_map/ppermute | solution.py:294
  112.4 10.5 %collective-permute-start.7 = (bf16[1,256,128]{2,1,0:T(8,128)(2,1)}, bf16[1,256,128]{2,1,0:T(8,128)(2,1)S(1)}, u32[]{:S(2)}, u32[]{:S(2)}) collective-permute-start(bf16[1,256,128]{2,1,0:T(8,128)(2,1)} %get-tuple-element.44), channel_id=1, source_target_pairs={{0,8},{2,10},{4,12},{6,14},{8,0},{10,2},{12,4},{14,6},{1,9},{3,11}... | collective-permute-start | bytes 196616 | tf_op jit(solution)/shard_map/ppermute | solution.py:294
  125.1 2.6 %shard_map.158 = (f32[128,128]{1,0:T(8,128)}, bf16[128,128]{1,0:T(8,128)(2,1)}) custom-call(bf16[256,2048]{1,0:T(8,128)(2,1)} %shard_map.155.table_ref, bf16[2048,128]{1,0:T(8,128)(2,1)} %bitcast.9.home_ref, bf16[128,2048]{1,0:T(8,128)(2,1)} %cot_ref.3), custom_call_target="tpu_custom_call" | custom-call | flops 200000000 | bytes 1048576 | tf_op jit(solution)/shard_map/pallas_call | solution.py:30
  127.7 3.4 %collective-permute-start.3 = (bf16[128,128]{1,0:T(8,128)(2,1)}, bf16[128,128]{1,0:T(8,128)(2,1)S(1)}, u32[]{:S(2)}, u32[]{:S(2)}) collective-permute-start(bf16[128,128]{1,0:T(8,128)(2,1)} %get-tuple-element.36), channel_id=1, source_target_pairs={{0,1},{1,0},{2,3},{3,2},{4,5},{5,4},{6,7},{7,6},{8,9},{9,8},{10,11... | collective-permute-start | bytes 98312 | tf_op jit(solution)/shard_map/ppermute | solution.py:291
  134.7 4.3 %all-to-all-start.2 = ((bf16[16,136,128]{2,1,0:T(8,128)(2,1)}), bf16[16,136,128]{2,1,0:T(8,128)(2,1)}, u32[]{:S(2)}, u32[]{:S(2)}) async-start(bf16[16,136,128]{2,1,0:T(8,128)(2,1)} %shard_map.163), calls=%async_computation.2 | async-start | bytes 1114112 | tf_op jit(solution)/shard_map/all_to_all | solution.py:407
  140.7 5.3 %shard_map.166 = (bf16[3,2048,128]{2,1,0:T(8,128)(2,1)}, bf16[3,2048,128]{2,1,0:T(8,128)(2,1)}) custom-call(bf16[2,3,2048,128]{3,2,1,0:T(8,128)(2,1)} %get-tuple-element.52.keep_ref, bf16[2,3,2048,128]{3,2,1,0:T(8,128)(2,1)} %copy-done), custom_call_target="tpu_custom_call" | custom-call | flops 1000000 | bytes 9437184 | tf_op jit(solution)/shard_map/pallas_call | solution.py:378
  146.0 3.3 %collective-permute-start.10 = (bf16[3,2048,128]{2,1,0:T(8,128)(2,1)}, bf16[3,2048,128]{2,1,0:T(8,128)(2,1)S(1)}, u32[]{:S(2)}, u32[]{:S(2)}) collective-permute-start(bf16[3,2048,128]{2,1,0:T(8,128)(2,1)} %get-tuple-element.55), channel_id=1, source_target_pairs={{0,14},{1,3},{2,0},{3,5},{4,2},{5,7},{6,4},{7,9},{8,6},{9,11},{10,... | collective-permute-start | bytes 4718600 | tf_op jit(solution)/shard_map/ppermute | solution.py:301
  149.3 7.8 %all-to-all-done.2.all_ref = bf16[16,136,128]{2,1,0:T(8,128)(2,1)} async-done(((bf16[16,136,128]{2,1,0:T(8,128)(2,1)}), bf16[16,136,128]{2,1,0:T(8,128)(2,1)}, u32[]{:S(2)}, u32[]{:S(2)}) %all-to-all-start.2) | async-done | bytes 557088 | tf_op jit(solution)/shard_map/all_to_all | solution.py:407
  157.1 2.7 %shard_map.164 = (bf16[2048,128]{1,0:T(8,128)(2,1)}, f32[128,128]{1,0:T(8,128)}) custom-call(bf16[16,136,128]{2,1,0:T(8,128)(2,1)} %all-to-all-done.2.all_ref, bf16[128,2048]{1,0:T(8,128)(2,1)} %proj_ref.3, bf16[128,128]{1,0:T(8,128)(2,1)} %get-tuple-element.45.act_ref, f32[128,128]{1,0:T(8,128)} %get-tuple-element.46.slope_ref, bf16[128,128]{1,0:T(8,128)(2,1)} %saved_ref.3, ...), custom_call_target="tpu_custom_call" | custom-call | flops 2000000000 | bytes 1048576 | tf_op jit(solution)/shard_map/pallas_call | solution.py:30
  159.8 9.7 %all-to-all-start.3 = ((bf16[32,64,128]{2,1,0:T(8,128)(2,1)}), bf16[32,64,128]{2,1,0:T(8,128)(2,1)S(1)}, u32[]{:S(2)}, u32[]{:S(2)}) async-start(bf16[32,64,128]{2,1,0:T(8,128)(2,1)} %bitcast.79), calls=%async_computation.3 | async-start | bytes 1048576 | tf_op jit(solution)/shard_map/all_to_all | solution.py:420
  172.5 4.1 %collective-permute-done.8 = f32[30,128]{1,0:T(8,128)S(1)} collective-permute-done((f32[30,128]{1,0:T(8,128)S(1)}, f32[30,128]{1,0:T(8,128)S(1)}, u32[]{:S(2)}, u32[]{:S(2)}) %collective-permute-start.8) | collective-permute-done | bytes 15392 | tf_op jit(solution)/shard_map/ppermute | solution.py:424
  178.3 8.6 %all-to-all-done.3 = bf16[32,64,128]{2,1,0:T(8,128)(2,1)S(1)} async-done(((bf16[32,64,128]{2,1,0:T(8,128)(2,1)}), bf16[32,64,128]{2,1,0:T(8,128)(2,1)S(1)}, u32[]{:S(2)}, u32[]{:S(2)}) %all-to-all-start.3) | async-done | bytes 524320 | tf_op jit(solution)/shard_map/all_to_all | solution.py:420
  188.8 3.1 %shard_map.167 = (bf16[2048,128]{1,0:T(8,128)(2,1)}, bf16[2048,128]{1,0:T(8,128)(2,1)}, bf16[128,2048]{1,0:T(8,128)(2,1)}) custom-call(bf16[3,2048,128]{2,1,0:T(8,128)(2,1)} %get-tuple-element.54.pre_ref, bf16[3,2048,128]{2,1,0:T(8,128)(2,1)} %copy-done.1), custom_call_target="tpu_custom_call" | custom-call | flops 1000000 | bytes 1048576 | tf_op jit(solution)/shard_map/pallas_call | solution.py:30
  (44 shorter events, 32.8 us)
Async XLA Ops:
  5.4 19.0 %copy-start.8 = (bf16[3,2048,128]{2,1,0:T(8,128)(2,1)S(1)}, bf16[3,2048,128]{2,1,0:T(8,128)(2,1)}, u32[]{:S(2)}) copy-start(bf16[3,2048,128]{2,1,0:T(8,128)(2,1)} %get-tuple-element.33.w0) | copy-start | bytes 4718596
  5.4 23.7 %collective-permute-start.1 = (bf16[3,2048,128]{2,1,0:T(8,128)(2,1)}, bf16[3,2048,128]{2,1,0:T(8,128)(2,1)}, u32[]{:S(2)}, u32[]{:S(2)}) collective-permute-start(bf16[3,2048,128]{2,1,0:T(8,128)(2,1)} %get-tuple-element.33.w0), channel_id=1, source_target_pairs={{0,2},{1,15},{2,4},{3,1},{4,6},{5,3},{6,8},{7,5},{8,10},{9,7},{10,... | collective-permute-start | bytes 4718600 | tf_op jit(solution)/shard_map/ppermute | solution.py:301
  11.5 40.9 %all-to-all-start = ((bf16[32,8,2048]{2,1,0:T(8,128)(2,1)}), bf16[32,8,2048]{2,1,0:T(8,128)(2,1)S(1)}, u32[]{:S(2)}, u32[]{:S(2)}) async-start(bf16[32,8,2048]{2,1,0:T(8,128)(2,1)} %bitcast.78), calls=%async_computation | async-start | bytes 2097152 | tf_op jit(solution)/shard_map/all_to_all | solution.py:324
  24.4 13.7 %collective-permute-start = (bf16[3,2048,128]{2,1,0:T(8,128)(2,1)S(1)}, bf16[3,2048,128]{2,1,0:T(8,128)(2,1)}, u32[]{:S(2)}, u32[]{:S(2)}) collective-permute-start(bf16[3,2048,128]{2,1,0:T(8,128)(2,1)S(1)} %copy-done.8), channel_id=1, source_target_pairs={{0,1},{1,0},{2,3},{3,2},{4,5},{5,4},{6,7},{7,6},{8,9},{9,8},{10,11... | collective-permute-start | bytes 4718600 | tf_op jit(solution)/shard_map/ppermute | solution.py:291
  29.1 23.2 %collective-permute-start.2 = (bf16[3,2048,128]{2,1,0:T(8,128)(2,1)}, bf16[3,2048,128]{2,1,0:T(8,128)(2,1)}, u32[]{:S(2)}, u32[]{:S(2)}) collective-permute-start(bf16[3,2048,128]{2,1,0:T(8,128)(2,1)} %collective-permute-done.1.w2), channel_id=1, source_target_pairs={{0,1},{1,0},{2,3},{3,2},{4,5},{5,4},{6,7},{7,6},{8,9},{9,8},{10,11... | collective-permute-start | bytes 4718600 | tf_op jit(solution)/shard_map/ppermute | solution.py:291
  52.3 1.0 copy-start.2
  65.7 73.3 %collective-permute-start.9 = (bf16[2,3,2048,128]{3,2,1,0:T(8,128)(2,1)}, bf16[2,3,2048,128]{3,2,1,0:T(8,128)(2,1)S(1)}, u32[]{:S(2)}, u32[]{:S(2)}) collective-permute-start(bf16[2,3,2048,128]{3,2,1,0:T(8,128)(2,1)} %get-tuple-element.53), channel_id=1, source_target_pairs={{0,1},{1,0},{2,3},{3,2},{4,5},{5,4},{6,7},{7,6},{8,9},{9,8},{10,11... | collective-permute-start | bytes 9437192 | tf_op jit(solution)/shard_map/ppermute | solution.py:291
  71.0 15.5 %collective-permute-start.4 = (bf16[8,256,128]{2,1,0:T(8,128)(2,1)}, bf16[8,256,128]{2,1,0:T(8,128)(2,1)}, u32[]{:S(2)}, u32[]{:S(2)}) collective-permute-start(bf16[8,256,128]{2,1,0:T(8,128)(2,1)} %get-tuple-element.38), channel_id=1, source_target_pairs={{0,1},{1,0},{2,3},{3,2},{4,5},{5,4},{6,7},{7,6},{8,9},{9,8},{10,11... | collective-permute-start | bytes 1572872 | tf_op jit(solution)/shard_map/ppermute | solution.py:291
  73.0 52.1 %all-to-all-start.1 = ((bf16[256,8,128]{2,1,0:T(8,128)(2,1)}), bf16[256,8,128]{2,1,0:T(8,128)(2,1)}, u32[]{:S(2)}, u32[]{:S(2)}) async-start(bf16[256,8,128]{2,1,0:T(8,128)(2,1)} %bitcast.80), calls=%async_computation.1 | async-start | bytes 1048576 | tf_op jit(solution)/shard_map/all_to_all | solution.py:369
  88.8 11.8 %collective-permute-start.5 = (bf16[4,256,128]{2,1,0:T(8,128)(2,1)}, bf16[4,256,128]{2,1,0:T(8,128)(2,1)S(1)}, u32[]{:S(2)}, u32[]{:S(2)}) collective-permute-start(bf16[4,256,128]{2,1,0:T(8,128)(2,1)} %get-tuple-element.40), channel_id=1, source_target_pairs={{0,2},{2,0},{4,6},{6,4},{8,10},{10,8},{12,14},{14,12},{1,3},{3,1},... | collective-permute-start | bytes 786440 | tf_op jit(solution)/shard_map/ppermute | solution.py:294
  100.7 0.7 copy-start.3
  103.3 6.8 %collective-permute-start.6 = (bf16[2,256,128]{2,1,0:T(8,128)(2,1)}, bf16[2,256,128]{2,1,0:T(8,128)(2,1)S(1)}, u32[]{:S(2)}, u32[]{:S(2)}) collective-permute-start(bf16[2,256,128]{2,1,0:T(8,128)(2,1)} %get-tuple-element.42), channel_id=1, source_target_pairs={{0,4},{2,6},{4,0},{6,2},{8,12},{10,14},{12,8},{14,10},{1,5},{3,7},... | collective-permute-start | bytes 393224 | tf_op jit(solution)/shard_map/ppermute | solution.py:294
  110.1 0.7 copy-start.4
  112.4 18.7 %collective-permute-start.7 = (bf16[1,256,128]{2,1,0:T(8,128)(2,1)}, bf16[1,256,128]{2,1,0:T(8,128)(2,1)S(1)}, u32[]{:S(2)}, u32[]{:S(2)}) collective-permute-start(bf16[1,256,128]{2,1,0:T(8,128)(2,1)} %get-tuple-element.44), channel_id=1, source_target_pairs={{0,8},{2,10},{4,12},{6,14},{8,0},{10,2},{12,4},{14,6},{1,9},{3,11}... | collective-permute-start | bytes 196616 | tf_op jit(solution)/shard_map/ppermute | solution.py:294
  127.7 4.5 %collective-permute-start.3 = (bf16[128,128]{1,0:T(8,128)(2,1)}, bf16[128,128]{1,0:T(8,128)(2,1)S(1)}, u32[]{:S(2)}, u32[]{:S(2)}) collective-permute-start(bf16[128,128]{1,0:T(8,128)(2,1)} %get-tuple-element.36), channel_id=1, source_target_pairs={{0,1},{1,0},{2,3},{3,2},{4,5},{5,4},{6,7},{7,6},{8,9},{9,8},{10,11... | collective-permute-start | bytes 98312 | tf_op jit(solution)/shard_map/ppermute | solution.py:291
  131.1 1.0 copy-start.5
  132.2 0.6 copy-start.6
  134.7 22.4 %all-to-all-start.2 = ((bf16[16,136,128]{2,1,0:T(8,128)(2,1)}), bf16[16,136,128]{2,1,0:T(8,128)(2,1)}, u32[]{:S(2)}, u32[]{:S(2)}) async-start(bf16[16,136,128]{2,1,0:T(8,128)(2,1)} %shard_map.163), calls=%async_computation.2 | async-start | bytes 1114112 | tf_op jit(solution)/shard_map/all_to_all | solution.py:407
  139.0 1.7 copy-start
  146.0 41.6 %collective-permute-start.10 = (bf16[3,2048,128]{2,1,0:T(8,128)(2,1)}, bf16[3,2048,128]{2,1,0:T(8,128)(2,1)S(1)}, u32[]{:S(2)}, u32[]{:S(2)}) collective-permute-start(bf16[3,2048,128]{2,1,0:T(8,128)(2,1)} %get-tuple-element.55), channel_id=1, source_target_pairs={{0,14},{1,3},{2,0},{3,5},{4,2},{5,7},{6,4},{7,9},{8,6},{9,11},{10,... | collective-permute-start | bytes 4718600 | tf_op jit(solution)/shard_map/ppermute | solution.py:301
  157.1 12.5 %copy-start.7 = (f32[31,128]{1,0:T(8,128)S(1)}, f32[31,128]{1,0:T(8,128)}, u32[]{:S(2)}) copy-start(f32[31,128]{1,0:T(8,128)} %param.19) | copy-start | bytes 47620
  159.8 27.1 %all-to-all-start.3 = ((bf16[32,64,128]{2,1,0:T(8,128)(2,1)}), bf16[32,64,128]{2,1,0:T(8,128)(2,1)S(1)}, u32[]{:S(2)}, u32[]{:S(2)}) async-start(bf16[32,64,128]{2,1,0:T(8,128)(2,1)} %bitcast.79), calls=%async_computation.3 | async-start | bytes 1048576 | tf_op jit(solution)/shard_map/all_to_all | solution.py:420
  170.3 6.3 %collective-permute-start.8 = (f32[30,128]{1,0:T(8,128)S(1)}, f32[30,128]{1,0:T(8,128)S(1)}, u32[]{:S(2)}, u32[]{:S(2)}) collective-permute-start(f32[30,128]{1,0:T(8,128)S(1)} %slice.188), channel_id=1, source_target_pairs={{16,0},{32,16},{48,32},{64,48},{80,64},{96,80},{112,96},{128,112},... | collective-permute-start | bytes 46088 | tf_op jit(solution)/shard_map/ppermute | solution.py:424
  187.6 1.2 copy-start.1

commit v6 on v5

--- a/solution.py
+++ b/solution.py
@@ -14,6 +14,7 @@
 SPAN = 4
 VMEM = pl.BlockSpec(memory_space=pltpu.VMEM)
 ANY = pl.BlockSpec(memory_space=pl.ANY)
+HBM = pl.BlockSpec(memory_space=pltpu.HBM)
 
 
 def mm(a, b, dims=(((1,), (0,)), ((), ()))):
@@ -24,15 +25,18 @@
     return lax.broadcasted_iota(I32, shape, dim)
 
 
-def kernel(body, outs, flops, *args, scratch=(), far=(), far_out=()):
+def kernel(body, outs, flops, *args, scratch=(), any_in=(), far=(), far_out=(), limit=60 * 1024):
     many = outs if isinstance(outs, tuple) else (outs,)
-    specs = [ANY if i in far_out else VMEM for i in range(len(many))]
+    specs = [HBM if i in far_out else VMEM for i in range(len(many))]
     return pl.pallas_call(
         body,
         out_shape=outs,
-        in_specs=[ANY if i in far else VMEM for i in range(len(args))],
+        in_specs=[
+            HBM if i in far else ANY if i in any_in else VMEM for i in range(len(args))
+        ],
         out_specs=specs if isinstance(outs, tuple) else specs[0],
         scratch_shapes=list(scratch),
+        compiler_params=pltpu.CompilerParams(vmem_limit_bytes=limit << 10),
         cost_estimate=pl.CostEstimate(flops=flops, bytes_accessed=1 << 20, transcendentals=0),
     )(*args)
 
@@ -42,23 +46,40 @@
 
 
 def head_body(
-    ids_ref, weight_ref, mix_ref, cot_ref, gate_ref, up_ref, down_ref, out_ref, pack_ref, buf_ref, sem
+    ids_ref,
+    weight_ref,
+    mix_any,
+    cot_any,
+    gate_ref,
+    up_ref,
+    down_ref,
+    out_any,
+    pack_ref,
+    mix_ref,
+    cot_ref,
+    out_ref,
+    buf_ref,
+    in_sem,
+    out_sem,
 ):
+    tokens = [
+        pltpu.make_async_copy(mix_any, mix_ref, in_sem.at[0]),
+        pltpu.make_async_copy(cot_any, cot_ref, in_sem.at[1]),
+    ]
     load = []
     for m, ref in enumerate((gate_ref, up_ref)):
-        load.append([pltpu.make_async_copy(ref, buf_ref.at[m], sem.at[m, 0])])
+        load.append([pltpu.make_async_copy(ref, buf_ref.at[m], in_sem.at[2 + m])])
     down = []
     for j in range(down_ref.shape[1] // 128):
         at = slice(j * 128, (j + 1) * 128)
-        down.append(
-            pltpu.make_async_copy(down_ref.at[:, at], buf_ref.at[2, at], sem.at[2 + j, 0])
-        )
+        down.append(pltpu.make_async_copy(down_ref.at[:, at], buf_ref.at[2, at], in_sem.at[4 + j]))
     load.append(down)
-    for copies in load:
+    for copies in (tokens, *load):
         for copy in copies:
             copy.start()
     tok = ids_ref.shape[1]
-    experts = out_ref.shape[0] // (2 * SPAN)
+    rows = out_ref.shape[0]
+    experts = rows // (2 * SPAN)
     group = (lax.axis_index("y") % 2) * 2 + lax.axis_index("c")
     ids = [ids_ref[k : k + 1, :] for k in range(2)]
     wts = [weight_ref[k : k + 1, :] for k in range(2)]
@@ -66,7 +87,6 @@
     hot = [(expert == i).astype(F32) for i in ids]
     after = (iota((tok, tok), 0) < iota((tok, tok), 1)).astype(BF)
     rank = mm((hot[0] + hot[1]).astype(BF), after)
-    rows = out_ref.shape[0]
     row = iota((rows, tok), 0)
     row_e, row_j = row // (2 * SPAN), row % (2 * SPAN)
     target = group * SPAN + row_j % SPAN
@@ -82,16 +102,23 @@
     take_x = jnp.where(found & is_x, 1.0, 0.0).astype(BF)
     take_g = jnp.where(found & ~is_x, 1.0, 0.0).astype(BF)
     scale = jnp.where(iota((rows, 1), 0) % (2 * SPAN) < SPAN, 1.0, scale)
+    for copy in tokens:
+        copy.wait()
     store = []
     for m, copies in enumerate(load):
         for copy in copies:
             copy.wait()
-        store.append(pltpu.make_async_copy(buf_ref.at[m], pack_ref.at[m], sem.at[m, 1]))
+        store.append(pltpu.make_async_copy(buf_ref.at[m], pack_ref.at[m], out_sem.at[m]))
         store[-1].start()
     step = 512
-    for at in range(0, mix_ref.shape[1], step):
-        picked = mm(take_x, mix_ref[:, at : at + step]) + mm(take_g, cot_ref[:, at : at + step])
-        out_ref[:, at : at + step] = (picked * scale).astype(BF)
+    for k, at in enumerate(range(0, mix_ref.shape[1], step)):
+        cut = slice(at, at + step)
+        picked = mm(take_x, mix_ref[:, cut]) + mm(take_g, cot_ref[:, cut])
+        out_ref[:, cut] = (picked * scale).astype(BF)
+        store.append(
+            pltpu.make_async_copy(out_ref.at[:, cut], out_any.at[:, cut], out_sem.at[3 + k])
+        )
+        store[-1].start()
     for copy in store:
         copy.wait()
 
@@ -100,7 +127,7 @@
     tok = ids_ref.shape[1]
     ci = lax.axis_index("c")
     cols = out_ref.shape[1]
-    experts = cols // 64
+    experts = cols // 16
     lane = iota((tok, experts), 1)
     hot = jnp.zeros((tok, experts), F32)
     for k in range(2):
@@ -108,7 +135,7 @@
         hot = hot + (lane == ids[:, :experts].astype(I32)).astype(F32)
     before = (iota((tok, tok), 0) > iota((tok, tok), 1)).astype(BF)
     slot = jnp.where(hot > 0, mm(before, hot.astype(BF)), -1.0)
-    spread = (iota((experts, cols), 1) // 64 == iota((experts, cols), 0)).astype(BF)
+    spread = (iota((experts, cols), 1) // 16 == iota((experts, cols), 0)).astype(BF)
     held = mm(slot.astype(BF), spread).astype(I32)
     col = iota((tok, cols), 1)
     place = ((col // 8) % 2 * 2 + ci) * SPAN + col % SPAN
@@ -144,7 +171,13 @@
             ref[i] = (keep_ref[at] + given_ref[at].astype(F32)).astype(ref.dtype)
 
 
-def expert_body(got_ref, w0, w1, w2, w3, x_ref, g_ref, hid_ref, back_ref, in_ref, down_ref, sem):
+def pickers(slots):
+    out_row, in_row = iota((slots, 2 * slots), 0), iota((slots, 2 * slots), 1)
+    want = (out_row // SPAN) * (2 * SPAN) + out_row % SPAN
+    return (in_row == want).astype(BF), (in_row == want + SPAN).astype(BF)
+
+
+def expert_body(got_ref, w0, w1, w2, w3, hid_ref, back_ref, x_ref, g_ref, in_ref, down_ref, sem):
     rows, width = got_ref.shape
     slots = rows // 2
     copies = []
@@ -160,10 +193,7 @@
         for copy in three:
             copy.start()
         copies.append(three)
-    out_row, in_row = iota((slots, rows), 0), iota((slots, rows), 1)
-    want = (out_row // SPAN) * (2 * SPAN) + out_row % SPAN
-    pick_x = (in_row == want).astype(BF)
-    pick_g = (in_row == want + SPAN).astype(BF)
+    pick_x, pick_g = pickers(slots)
     for at in range(0, width, 512):
         part = got_ref[:, at : at + 512]
         x_ref[:, at : at + 512] = mm(pick_x, part).astype(BF)
@@ -195,29 +225,37 @@
         back_ref[:, 64 + y * 8 : 64 + (y + 1) * 8, :] = odd.reshape(-1, 8, 128).astype(BF)
 
 
-def grads_body(x_ref, g_ref, hid_ref, keep_ref, give_ref):
-    width = x_ref.shape[1]
+def grads_body(got_ref, hid_ref, keep_ref, give_ref):
+    pick_x, pick_g = pickers(got_ref.shape[0] // 2)
     places = ((keep_ref, 0), (give_ref, 0), (keep_ref, 1), (give_ref, 1))
-    for j in range(width // 128):
+    for j in range(got_ref.shape[1] // 128):
         at = slice(j * 128, (j + 1) * 128)
-        both = mm(x_ref[:, at], hid_ref[:, :1024], FIRST)
-        down = mm(hid_ref[:, 1024:], g_ref[:, at], FIRST)
+        both = mm(mm(pick_x, got_ref[:, at]).astype(BF), hid_ref[:, :1024], FIRST)
+        down = mm(hid_ref[:, 1024:], mm(pick_g, got_ref[:, at]).astype(BF), FIRST)
         for q, (ref, to) in enumerate(places):
             ref[to, 0, at, :] = both[:, q * 256 : q * 256 + 128].astype(BF)
             ref[to, 1, at, :] = both[:, q * 256 + 128 : (q + 1) * 256].astype(BF)
             ref[to, 2, at, :] = down[q * 128 : (q + 1) * 128, :].astype(BF)
 
 
-def combine_body(table_ref, home_ref, cot_ref, own_ref, other_ref):
+def combine_body(table_ref, home_ref, cot_any, own_ref, other_ref, cot_ref, sem):
     tok = cot_ref.shape[0]
     place = lax.axis_index("y") * 2 + lax.axis_index("c")
-    cot = cot_ref[:, pl.ds(pl.multiple_of(place * 128, 128), 128)].astype(F32)
-    both = mm(table_ref[...], home_ref[...])
-    own_ref[...] = both[:tok] + cot
+    cut = pl.ds(pl.multiple_of(place * 128, 128), 128)
+    copy = pltpu.make_async_copy(cot_any.at[:, cut], cot_ref, sem)
+    copy.start()
+    cols = table_ref.shape[1]
+    part = home_ref[...].astype(F32).reshape(cols // 16, -1, 16, 128)
+    total = part[:, 0]
+    for j in range(1, part.shape[1]):
+        total = total + part[:, j]
+    both = mm(table_ref[...], total.reshape(cols, 128).astype(BF))
     other_ref[...] = both[tok:].astype(BF)
-
-
-def mix_body(own_ref, other_ref, vown_ref, vgot_ref, out_ref):
+    copy.wait()
+    own_ref[...] = both[:tok] + cot_ref[...].astype(F32)
+
+
+def mix_body(own_ref, other_ref, vown_ref, vgot_ref, out_ref, buf_ref, sem):
     tok = own_ref.shape[0]
     total = vown_ref[0] + vgot_ref[0].astype(F32)
     mix = (own_ref[...] + other_ref[...].astype(F32)).astype(BF)
@@ -230,21 +268,40 @@
             rest = rest - parts[-1]
     parts.append(jnp.zeros((2, tok), F32))
     sums = jnp.concatenate(parts, axis=0).astype(BF)
-    for y in range(out_ref.shape[0]):
-        out_ref[y, :tok, :] = mix
-        out_ref[y, tok:, :] = sums
-
-
-def final_body(all_ref, proj_ref, act_ref, slope_ref, saved_ref, dev_ref, out_ref, conv_ref):
+    buf_ref[:tok, :] = mix
+    buf_ref[tok:, :] = sums
+    copies = [
+        pltpu.make_async_copy(buf_ref, out_ref.at[t], sem.at[t]) for t in range(out_ref.shape[0])
+    ]
+    for copy in copies:
+        copy.start()
+    for copy in copies:
+        copy.wait()
+
+
+def final_body(
+    all_ref, proj_ref, act_ref, slope_ref, saved_ref, dev_ref, out_any, conv_ref, out_ref, sem
+):
     tok = act_ref.shape[0]
     acc = jnp.zeros((tok, tok), F32)
     sums = jnp.zeros((8, tok), F32)
+    copies = []
     for t in range(all_ref.shape[0]):
         at = slice(t * 128, (t + 1) * 128)
-        part = all_ref[t, :tok, :]
-        sums = sums + all_ref[t, tok:, :].astype(F32)
-        out_ref[at, :] = mm(part, act_ref[...], FIRST).astype(BF)
-        acc = acc + mm(part, proj_ref[:, at], LAST)
+        out_ref[at, :] = mm(all_ref[t, :tok, :], act_ref[...], FIRST).astype(BF)
+        if t % 4 == 3:
+            at = slice((t - 3) * 128, (t + 1) * 128)
+            copies.append(
+                pltpu.make_async_copy(out_ref.at[at, :], out_any.at[at, :], sem.at[t // 4])
+            )
+            copies[-1].start()
+    for t in range(0, all_ref.shape[0], 2):
+        pair = [all_ref[t + i, :tok, :] for i in range(2)]
+        acc = acc + mm(
+            jnp.concatenate(pair, axis=1), proj_ref[:, t * 128 : (t + 2) * 128], LAST
+        )
+        for i in range(2):
+            sums = sums + all_ref[t + i, tok:, :].astype(F32)
     grad = acc * slope_ref[...]
     count = all_ref.shape[0] * 128
     means = []
@@ -253,6 +310,8 @@
         means.append(jnp.broadcast_to(total, (tok, tok)).T)
     dev = jnp.broadcast_to(dev_ref[...], (tok, tok)).T
     conv_ref[...] = dev * (grad - means[0] - saved_ref[...].astype(F32) * means[1])
+    for copy in copies:
+        copy.wait()
 
 
 def sumout_body(keep_ref, given_ref, pre_ref, pass_ref):
@@ -313,16 +372,23 @@
         gate_weight[0],
         up_weight[0],
         down_weight[0],
-        far=(4, 5, 6),
-        far_out=(1,),
-        scratch=(pltpu.VMEM((3, width, 128), BF), pltpu.SemaphoreType.DMA((2 + width // 128, 2))),
+        far=(2, 3, 4, 5, 6),
+        far_out=(0, 1),
+        scratch=(
+            pltpu.VMEM((tok, width), BF),
+            pltpu.VMEM((tok, width), BF),
+            pltpu.VMEM((rows, width), BF),
+            pltpu.VMEM((3, width, 128), BF),
+            pltpu.SemaphoreType.DMA((4 + width // 128,)),
+            pltpu.SemaphoreType.DMA((3 + width // 512,)),
+        ),
     )
     by_y = hop(own, 1)
     by_c = flip_c(own)
     by_yc = flip_c(by_y)
 
     got = lax.all_to_all(sent.reshape(experts, 2 * SPAN, width), sp, 0, 0, tiled=True)
-    table = kernel(table_body, shape(2 * tok, experts * ny * 2 * SPAN), 2000000000, ids)
+    table = kernel(table_body, shape(2 * tok, experts * 4 * SPAN), 500000000, ids, limit=12 << 10)
 
     act_conv, slope, vkeep, vgive = kernel(
         slope_body,
@@ -336,6 +402,7 @@
         saved_normalized,
         channel_norm_gain[None, :],
         proj_weight,
+        limit=16 << 10,
     )
     vgiven = flip_c(vgive)
     for bit in range(3):
@@ -346,21 +413,26 @@
             1000000,
             vkeep,
             vgiven,
+            limit=12 << 10,
         )
         vgiven = flip_y(vgive, bit)
 
     slots = experts * SPAN
-    x, g, hidden, back = kernel(
+    got = got.reshape(rows, width)
+    hidden, back = kernel(
         expert_body,
-        (shape(slots, width), shape(slots, width), shape(slots, 1536), shape(experts // 2, 128, 128)),
+        (shape(slots, 1536), shape(experts // 2, 128, 128)),
         4000000000,
-        got.reshape(rows, width),
+        got,
         own,
         by_c,
         by_y,
         by_yc,
-        far=(1, 2, 3, 4),
+        any_in=(1, 2, 3, 4),
+        limit=24 << 10,
         scratch=(
+            pltpu.VMEM((slots, width), BF),
+            pltpu.VMEM((slots, width), BF),
             pltpu.VMEM((width, 1024), BF),
             pltpu.VMEM((width // 128, 512, 128), BF),
             pltpu.SemaphoreType.DMA((4, 3)),
@@ -371,7 +443,18 @@
     ).reshape(-1, 128)
 
     packed = shape(2, 3, width, 128)
-    keep, give = kernel(grads_body, (packed, packed), 8000000000, x, g, hidden)
+    quarter = pl.BlockSpec((2, 3, width // 4, 128), lambda j: (0, 0, j, 0))
+    keep, give = pl.pallas_call(
+        grads_body,
+        grid=(4,),
+        out_shape=(packed, packed),
+        in_specs=[
+            pl.BlockSpec((rows, width // 4), lambda j: (0, j)),
+            pl.BlockSpec((slots, 1536), lambda j: (0, 0)),
+        ],
+        out_specs=[quarter, quarter],
+        cost_estimate=pl.CostEstimate(flops=8000000000, bytes_accessed=7 << 20, transcendentals=0),
+    )(got, hidden)
     given = flip_c(give)
     block = pl.BlockSpec((2, 1, width, 128), lambda m: (0, m, 0, 0))
     piece = pl.BlockSpec((1, width, 128), lambda m: (m, 0, 0))
@@ -390,6 +473,7 @@
         1000000,
         before,
         passed,
+        limit=20 << 10,
     )
 
     mine, other = kernel(
@@ -399,10 +483,22 @@
         table,
         home,
         cotangent,
+        far=(2,),
+        limit=12 << 10,
+        scratch=(pltpu.VMEM((tok, 128), BF), pltpu.SemaphoreType.DMA),
     )
     other = flip_c(other)
     mix = kernel(
-        mix_body, shape(2 * ny, tok + 8, 128), 1000000, mine, other, vkeep, vgiven
+        mix_body,
+        shape(2 * ny, tok + 8, 128),
+        1000000,
+        mine,
+        other,
+        vkeep,
+        vgiven,
+        far_out=(0,),
+        limit=12 << 10,
+        scratch=(pltpu.VMEM((tok + 8, 128), BF), pltpu.SemaphoreType.DMA((2 * ny,))),
     )
     mix_all = lax.all_to_all(mix, ("y", "c"), 0, 0, tiled=True)
 
@@ -416,6 +512,9 @@
         slope,
         saved_normalized,
         inverse_deviation[None, :],
+        far_out=(0,),
+        limit=16 << 10,
+        scratch=(pltpu.VMEM((width, 128), BF), pltpu.SemaphoreType.DMA((ny // 2,))),
     )
     proj = lax.all_to_all(proj.reshape(experts, -1, 128), sp, 0, 0, tiled=True)
     grad_proj = jnp.sum(proj.astype(F32), axis=0)

time: 193 us -> 178 us (0.922)
  Pallas kernels: 43.9 us -> 28.4 us
  local copies, waits for them, and re-layouts: 7.41 us -> 3.75 us
  waiting for transfers between devices: 51.1 us -> 53.9 us
    pallas_call x12, Pallas kernels: 38.6 us -> 23 us  [the longest x11 14.6 us: kernel(): pl.pallas_call(body, out_shape=outs, in_specs=[HBM if i in far else ANY i...]
    unnamed x19 -> x29, local copies, waits for them, and re-layouts: 6.67 us -> 3.72 us
    all_to_all x1, waiting for transfers between devices: 8.64 us -> 11.1 us  [shards(): proj = lax.all_to_all(proj.reshape(experts, -1, 128), sp, 0, 0, tiled=True)]
  transfers between devices with their start and end apart: 15 -> 15, of which waited for: 8 -> 9; matrix products, arithmetic and copies ran while one was open for 2% -> 1% of each run, Pallas kernels for 12% -> 5%
where the time goes in v6:
time: 178 us; the launch traced here: 177 us
  starting transfers between devices  87.4 us (49%)
  waiting for transfers between devices  53.9 us (30%)
  Pallas kernels  28.4 us (16%)
  local copies, waits for them, and re-layouts  3.75 us (2%)
  other arithmetic  2.54 us (1%)
    ppermute x5, starting transfers between devices, flip_c(): return lax.ppermute(value, 'c', [(0, 1), (1, 0)])  18.8 us
    ppermute x3, starting transfers between devices, flip_y(): return lax.ppermute(value, 'y', [(i, i ^ 1 << bit) for i in range(ny)])  16.4 us
    pallas_call x11, Pallas kernels, kernel(): pl.pallas_call(body, out_shape=outs, in_specs=[HBM if i in far else ANY i...  14.6 us
    all_to_all x1, waiting for transfers between devices, shards(): lax.all_to_all(sent.reshape(experts, 2 * SPAN, width), sp, 0, 0, tiled=True)  13.1 us
    all_to_all x1, starting transfers between devices, shards(): lax.all_to_all(sent.reshape(experts, 2 * SPAN, width), sp, 0, 0, tiled=True)  12.9 us
    all_to_all x1, starting transfers between devices, shards(): lax.all_to_all(back.reshape(experts * ny, 2 * SPAN, 128), ('z', 'x', 'y')...  12.5 us
    ppermute x3, waiting for transfers between devices, flip_y(): return lax.ppermute(value, 'y', [(i, i ^ 1 << bit) for i in range(ny)])  11.1 us
    all_to_all x1, waiting for transfers between devices, shards(): proj = lax.all_to_all(proj.reshape(experts, -1, 128), sp, 0, 0, tiled=True)  11.1 us
  transfers between devices with their start and end apart: 15, of which 9 were waited for; matrix products, arithmetic and copies ran while one was open for 1% of the time, Pallas kernels for 5%

profile of v6, /device:TPU:1, one launch (start us, length us, event | category | flops | bytes accessed | tf_op | source)
XLA Modules:
  0.0 176.9 jit_solution(4446325489766298809)
XLA Ops:
  0.6 4.0 %shard_map.156 = (bf16[256,2048]{1,0:T(8,128)(2,1)}, bf16[3,2048,128]{2,1,0:T(8,128)(2,1)}) custom-call(s32[2,128]{1,0:T(2,128)} %bitcast.80, f32[2,128]{1,0:T(2,128)} %bitcast.91, bf16[128,2048]{1,0:T(8,128)(2,1)} %mix_any.1, bf16[128,2048]{1,0:T(8,128)(2,1)} %cot_any.3, bf16[2048,128]{1,0:T(8,128)(2,1)} %bitcast.85, bf16[2048,128]{1,0:T(8,128)(2,1)} %bitcast.86, ...), custom_call_target="tpu_custom_call" | custom-call | flops 2000000000 | bytes 1048576 | tf_op jit(solution)/shard_map/pallas_call | solution.py:31
  4.6 6.0 %collective-permute-start.1 = (bf16[3,2048,128]{2,1,0:T(8,128)(2,1)}, bf16[3,2048,128]{2,1,0:T(8,128)(2,1)}, u32[]{:S(2)}, u32[]{:S(2)}) collective-permute-start(bf16[3,2048,128]{2,1,0:T(8,128)(2,1)} %get-tuple-element.31.w0), channel_id=1, source_target_pairs={{0,2},{1,15},{2,4},{3,1},{4,6},{5,3},{6,8},{7,5},{8,10},{9,7},{10,... | collective-permute-start | bytes 4718600 | tf_op jit(solution)/shard_map/ppermute | solution.py:360
  10.7 12.9 %all-to-all-start = ((bf16[32,8,2048]{2,1,0:T(8,128)(2,1)}), bf16[32,8,2048]{2,1,0:T(8,128)(2,1)S(1)}, u32[]{:S(2)}, u32[]{:S(2)}) async-start(bf16[32,8,2048]{2,1,0:T(8,128)(2,1)} %bitcast.84), calls=%async_computation | async-start | bytes 2097152 | tf_op jit(solution)/shard_map/all_to_all | solution.py:390
  25.5 2.8 %collective-permute-done.1.w2 = bf16[3,2048,128]{2,1,0:T(8,128)(2,1)} collective-permute-done((bf16[3,2048,128]{2,1,0:T(8,128)(2,1)}, bf16[3,2048,128]{2,1,0:T(8,128)(2,1)}, u32[]{:S(2)}, u32[]{:S(2)}) %collective-permute-start.1) | collective-permute-done | bytes 1572896 | tf_op jit(solution)/shard_map/ppermute | solution.py:360
  28.3 9.0 %collective-permute-start.2 = (bf16[3,2048,128]{2,1,0:T(8,128)(2,1)}, bf16[3,2048,128]{2,1,0:T(8,128)(2,1)}, u32[]{:S(2)}, u32[]{:S(2)}) collective-permute-start(bf16[3,2048,128]{2,1,0:T(8,128)(2,1)} %collective-permute-done.1.w2), channel_id=1, source_target_pairs={{0,1},{1,0},{2,3},{3,2},{4,5},{5,4},{6,7},{7,6},{8,9},{9,8},{10,11... | collective-permute-start | bytes 4718600 | tf_op jit(solution)/shard_map/ppermute | solution.py:350
  38.5 13.1 %all-to-all-done = bf16[32,8,2048]{2,1,0:T(8,128)(2,1)S(1)} async-done(((bf16[32,8,2048]{2,1,0:T(8,128)(2,1)}), bf16[32,8,2048]{2,1,0:T(8,128)(2,1)S(1)}, u32[]{:S(2)}, u32[]{:S(2)}) %all-to-all-start) | async-done | bytes 1048608 | tf_op jit(solution)/shard_map/all_to_all | solution.py:390
  53.3 5.5 %shard_map.157 = (bf16[128,1536]{1,0:T(8,128)(2,1)S(1)}, bf16[16,128,128]{2,1,0:T(8,128)(2,1)}) custom-call(bf16[256,2048]{1,0:T(8,128)(2,1)S(1)} %bitcast.78, bf16[3,2048,128]{2,1,0:T(8,128)(2,1)S(1)} %copy-done.3, bf16[3,2048,128]{2,1,0:T(8,128)(2,1)S(1)} %copy-done.5, bf16[3,2048,128]{2,1,0:T(8,128)(2,1)} %collective-permute-done.1.w2, ...), custom_call_target="tpu_custom_call" | custom-call | flops 4000000000 | bytes 1048576 | tf_op jit(solution)/shard_map/pallas_call | solution.py:31
  59.6 8.4 %shard_map.165 = (bf16[2,3,2048,128]{3,2,1,0:T(8,128)(2,1)}, bf16[2,3,2048,128]{3,2,1,0:T(8,128)(2,1)}) custom-call(bf16[256,2048]{1,0:T(8,128)(2,1)} %bitcast.79, bf16[128,1536]{1,0:T(8,128)(2,1)} %copy-done.12), custom_call_target="tpu_custom_call" | custom-call | flops 8000000000 | bytes 7340032 | tf_op jit(solution)/shard_map/pallas_call | solution.py:447
  68.0 2.3 %collective-permute-start.9 = (bf16[2,3,2048,128]{3,2,1,0:T(8,128)(2,1)}, bf16[2,3,2048,128]{3,2,1,0:T(8,128)(2,1)}, u32[]{:S(2)}, u32[]{:S(2)}) collective-permute-start(bf16[2,3,2048,128]{3,2,1,0:T(8,128)(2,1)} %get-tuple-element.49), channel_id=1, source_target_pairs={{0,1},{1,0},{2,3},{3,2},{4,5},{5,4},{6,7},{7,6},{8,9},{9,8},{10,11... | collective-permute-start | bytes 9437192 | tf_op jit(solution)/shard_map/ppermute | solution.py:350
  70.3 12.5 %all-to-all-start.1 = ((bf16[256,8,128]{2,1,0:T(8,128)(2,1)}), bf16[256,8,128]{2,1,0:T(8,128)(2,1)S(1)}, u32[]{:S(2)}, u32[]{:S(2)}) async-start(bf16[256,8,128]{2,1,0:T(8,128)(2,1)} %bitcast.8), calls=%async_computation.1 | async-start | bytes 1048576 | tf_op jit(solution)/shard_map/all_to_all | solution.py:441
  83.6 2.2 %collective-permute-start.4 = (bf16[8,256,128]{2,1,0:T(8,128)(2,1)S(1)}, bf16[8,256,128]{2,1,0:T(8,128)(2,1)S(1)}, u32[]{:S(2)}, u32[]{:S(2)}) collective-permute-start(bf16[8,256,128]{2,1,0:T(8,128)(2,1)S(1)} %get-tuple-element.36), channel_id=1, source_target_pairs={{0,1},{1,0},{2,3},{3,2},{4,5},{5,4},{6,7},{7,6},{8,9},{9,8},{10,11... | collective-permute-start | bytes 1572872 | tf_op jit(solution)/shard_map/ppermute | solution.py:350
  87.5 2.1 %collective-permute-start.5 = (bf16[4,256,128]{2,1,0:T(8,128)(2,1)S(1)}, bf16[4,256,128]{2,1,0:T(8,128)(2,1)S(1)}, u32[]{:S(2)}, u32[]{:S(2)}) collective-permute-start(bf16[4,256,128]{2,1,0:T(8,128)(2,1)S(1)} %get-tuple-element.38), channel_id=1, source_target_pairs={{0,2},{2,0},{4,6},{6,4},{8,10},{10,8},{12,14},{14,12},{1,3},{3,1},... | collective-permute-start | bytes 786440 | tf_op jit(solution)/shard_map/ppermute | solution.py:353
  89.5 8.8 %collective-permute-done.5.given_ref = bf16[4,256,128]{2,1,0:T(8,128)(2,1)S(1)} collective-permute-done((bf16[4,256,128]{2,1,0:T(8,128)(2,1)S(1)}, bf16[4,256,128]{2,1,0:T(8,128)(2,1)S(1)}, u32[]{:S(2)}, u32[]{:S(2)}) %collective-permute-start.5) | collective-permute-done | bytes 262176 | tf_op jit(solution)/shard_map/ppermute | solution.py:353
  98.4 4.2 %collective-permute-start.6 = (bf16[2,256,128]{2,1,0:T(8,128)(2,1)S(1)}, bf16[2,256,128]{2,1,0:T(8,128)(2,1)S(1)}, u32[]{:S(2)}, u32[]{:S(2)}) collective-permute-start(bf16[2,256,128]{2,1,0:T(8,128)(2,1)S(1)} %get-tuple-element.40), channel_id=1, source_target_pairs={{0,4},{2,6},{4,0},{6,2},{8,12},{10,14},{12,8},{14,10},{1,5},{3,7},... | collective-permute-start | bytes 393224 | tf_op jit(solution)/shard_map/ppermute | solution.py:353
  102.6 2.4 %collective-permute-done.6.given_ref = bf16[2,256,128]{2,1,0:T(8,128)(2,1)S(1)} collective-permute-done((bf16[2,256,128]{2,1,0:T(8,128)(2,1)S(1)}, bf16[2,256,128]{2,1,0:T(8,128)(2,1)S(1)}, u32[]{:S(2)}, u32[]{:S(2)}) %collective-permute-start.6) | collective-permute-done | bytes 131104 | tf_op jit(solution)/shard_map/ppermute | solution.py:353
  105.0 10.1 %collective-permute-start.7 = (bf16[1,256,128]{2,1,0:T(8,128)(2,1)S(1)}, bf16[1,256,128]{2,1,0:T(8,128)(2,1)S(1)}, u32[]{:S(2)}, u32[]{:S(2)}) collective-permute-start(bf16[1,256,128]{2,1,0:T(8,128)(2,1)S(1)} %get-tuple-element.42), channel_id=1, source_target_pairs={{0,8},{2,10},{4,12},{6,14},{8,0},{10,2},{12,4},{14,6},{1,9},{3,11}... | collective-permute-start | bytes 196616 | tf_op jit(solution)/shard_map/ppermute | solution.py:353
  115.9 3.4 %collective-permute-start.3 = (bf16[128,128]{1,0:T(8,128)(2,1)S(1)}, bf16[128,128]{1,0:T(8,128)(2,1)S(1)}, u32[]{:S(2)}, u32[]{:S(2)}) collective-permute-start(bf16[128,128]{1,0:T(8,128)(2,1)S(1)} %get-tuple-element.34), channel_id=1, source_target_pairs={{0,1},{1,0},{2,3},{3,2},{4,5},{5,4},{6,7},{7,6},{8,9},{9,8},{10,11... | collective-permute-start | bytes 98312 | tf_op jit(solution)/shard_map/ppermute | solution.py:350
  121.3 5.9 %all-to-all-start.2 = ((bf16[16,136,128]{2,1,0:T(8,128)(2,1)}), bf16[16,136,128]{2,1,0:T(8,128)(2,1)S(1)}, u32[]{:S(2)}, u32[]{:S(2)}) async-start(bf16[16,136,128]{2,1,0:T(8,128)(2,1)} %shard_map.163), calls=%async_computation.2 | async-start | bytes 1114112 | tf_op jit(solution)/shard_map/all_to_all | solution.py:503
  127.2 5.4 %shard_map.166 = (bf16[3,2048,128]{2,1,0:T(8,128)(2,1)}, bf16[3,2048,128]{2,1,0:T(8,128)(2,1)}) custom-call(bf16[2,3,2048,128]{3,2,1,0:T(8,128)(2,1)} %get-tuple-element.48.keep_ref, bf16[2,3,2048,128]{3,2,1,0:T(8,128)(2,1)} %collective-permute-done.9.given_ref), custom_call_target="tpu_custom_call" | custom-call | flops 1000000 | bytes 9437184 | tf_op jit(solution)/shard_map/pallas_call | solution.py:461
  132.6 3.2 %collective-permute-start.10 = (bf16[3,2048,128]{2,1,0:T(8,128)(2,1)}, bf16[3,2048,128]{2,1,0:T(8,128)(2,1)S(1)}, u32[]{:S(2)}, u32[]{:S(2)}) collective-permute-start(bf16[3,2048,128]{2,1,0:T(8,128)(2,1)} %get-tuple-element.51), channel_id=1, source_target_pairs={{0,14},{1,3},{2,0},{3,5},{4,2},{5,7},{6,4},{7,9},{8,6},{9,11},{10,... | collective-permute-start | bytes 4718600 | tf_op jit(solution)/shard_map/ppermute | solution.py:360
  135.9 9.4 %all-to-all-done.2.all_ref = bf16[16,136,128]{2,1,0:T(8,128)(2,1)S(1)} async-done(((bf16[16,136,128]{2,1,0:T(8,128)(2,1)}), bf16[16,136,128]{2,1,0:T(8,128)(2,1)S(1)}, u32[]{:S(2)}, u32[]{:S(2)}) %all-to-all-start.2) | async-done | bytes 557088 | tf_op jit(solution)/shard_map/all_to_all | solution.py:503
  146.3 10.0 %all-to-all-start.3 = ((bf16[32,64,128]{2,1,0:T(8,128)(2,1)}), bf16[32,64,128]{2,1,0:T(8,128)(2,1)}, u32[]{:S(2)}, u32[]{:S(2)}) async-start(bf16[32,64,128]{2,1,0:T(8,128)(2,1)} %bitcast.42), calls=%async_computation.3 | async-start | bytes 1048576 | tf_op jit(solution)/shard_map/all_to_all | solution.py:519
  157.9 4.0 %collective-permute-done.8 = f32[30,128]{1,0:T(8,128)S(1)} collective-permute-done((f32[30,128]{1,0:T(8,128)S(1)}, f32[30,128]{1,0:T(8,128)S(1)}, u32[]{:S(2)}, u32[]{:S(2)}) %collective-permute-start.8) | collective-permute-done | bytes 15392 | tf_op jit(solution)/shard_map/ppermute | solution.py:523
  162.6 11.1 %all-to-all-done.3 = bf16[32,64,128]{2,1,0:T(8,128)(2,1)} async-done(((bf16[32,64,128]{2,1,0:T(8,128)(2,1)}), bf16[32,64,128]{2,1,0:T(8,128)(2,1)}, u32[]{:S(2)}, u32[]{:S(2)}) %all-to-all-start.3) | async-done | bytes 524320 | tf_op jit(solution)/shard_map/all_to_all | solution.py:519
  (54 shorter events, 17.2 us)
Async XLA Ops:
  4.6 19.0 %copy-start.3 = (bf16[3,2048,128]{2,1,0:T(8,128)(2,1)S(1)}, bf16[3,2048,128]{2,1,0:T(8,128)(2,1)}, u32[]{:S(2)}) copy-start(bf16[3,2048,128]{2,1,0:T(8,128)(2,1)} %get-tuple-element.31.w0) | copy-start | bytes 4718596
  4.6 23.7 %collective-permute-start.1 = (bf16[3,2048,128]{2,1,0:T(8,128)(2,1)}, bf16[3,2048,128]{2,1,0:T(8,128)(2,1)}, u32[]{:S(2)}, u32[]{:S(2)}) collective-permute-start(bf16[3,2048,128]{2,1,0:T(8,128)(2,1)} %get-tuple-element.31.w0), channel_id=1, source_target_pairs={{0,2},{1,15},{2,4},{3,1},{4,6},{5,3},{6,8},{7,5},{8,10},{9,7},{10,... | collective-permute-start | bytes 4718600 | tf_op jit(solution)/shard_map/ppermute | solution.py:360
  10.7 40.9 %all-to-all-start = ((bf16[32,8,2048]{2,1,0:T(8,128)(2,1)}), bf16[32,8,2048]{2,1,0:T(8,128)(2,1)S(1)}, u32[]{:S(2)}, u32[]{:S(2)}) async-start(bf16[32,8,2048]{2,1,0:T(8,128)(2,1)} %bitcast.84), calls=%async_computation | async-start | bytes 2097152 | tf_op jit(solution)/shard_map/all_to_all | solution.py:390
  23.6 13.7 %collective-permute-start = (bf16[3,2048,128]{2,1,0:T(8,128)(2,1)S(1)}, bf16[3,2048,128]{2,1,0:T(8,128)(2,1)S(1)}, u32[]{:S(2)}, u32[]{:S(2)}) collective-permute-start(bf16[3,2048,128]{2,1,0:T(8,128)(2,1)S(1)} %copy-done.3), channel_id=1, source_target_pairs={{0,1},{1,0},{2,3},{3,2},{4,5},{5,4},{6,7},{7,6},{8,9},{9,8},{10,11... | collective-permute-start | bytes 4718600 | tf_op jit(solution)/shard_map/ppermute | solution.py:350
  28.3 23.2 %collective-permute-start.2 = (bf16[3,2048,128]{2,1,0:T(8,128)(2,1)}, bf16[3,2048,128]{2,1,0:T(8,128)(2,1)}, u32[]{:S(2)}, u32[]{:S(2)}) collective-permute-start(bf16[3,2048,128]{2,1,0:T(8,128)(2,1)} %collective-permute-done.1.w2), channel_id=1, source_target_pairs={{0,1},{1,0},{2,3},{3,2},{4,5},{5,4},{6,7},{7,6},{8,9},{9,8},{10,11... | collective-permute-start | bytes 4718600 | tf_op jit(solution)/shard_map/ppermute | solution.py:350
  59.6 23.3 %copy-start.6 = (bf16[128,2048]{1,0:T(8,128)(2,1)S(1)}, bf16[128,2048]{1,0:T(8,128)(2,1)}, u32[]{:S(2)}) copy-start(bf16[128,2048]{1,0:T(8,128)(2,1)} %proj_ref.3) | copy-start | bytes 1572868
  59.6 23.3 %copy-start.8 = (bf16[128,128]{1,0:T(8,128)(2,1)S(1)}, bf16[128,128]{1,0:T(8,128)(2,1)}, u32[]{:S(2)}) copy-start(bf16[128,128]{1,0:T(8,128)(2,1)} %saved_ref.3) | copy-start | bytes 98308
  59.6 23.3 %copy-start.10 = (f32[128]{0:T(128)S(1)}, f32[128]{0:T(128)}, u32[]{:S(2)}) copy-start(f32[128]{0:T(128)} %param.18) | copy-start | bytes 1540
  68.0 59.2 %collective-permute-start.9 = (bf16[2,3,2048,128]{3,2,1,0:T(8,128)(2,1)}, bf16[2,3,2048,128]{3,2,1,0:T(8,128)(2,1)}, u32[]{:S(2)}, u32[]{:S(2)}) collective-permute-start(bf16[2,3,2048,128]{3,2,1,0:T(8,128)(2,1)} %get-tuple-element.49), channel_id=1, source_target_pairs={{0,1},{1,0},{2,3},{3,2},{4,5},{5,4},{6,7},{7,6},{8,9},{9,8},{10,11... | collective-permute-start | bytes 9437192 | tf_op jit(solution)/shard_map/ppermute | solution.py:350
  70.3 45.3 %all-to-all-start.1 = ((bf16[256,8,128]{2,1,0:T(8,128)(2,1)}), bf16[256,8,128]{2,1,0:T(8,128)(2,1)S(1)}, u32[]{:S(2)}, u32[]{:S(2)}) async-start(bf16[256,8,128]{2,1,0:T(8,128)(2,1)} %bitcast.8), calls=%async_computation.1 | async-start | bytes 1048576 | tf_op jit(solution)/shard_map/all_to_all | solution.py:441
  83.6 31.6 %copy-start.9 = (s32[128,2]{0,1:T(2,128)S(1)}, s32[128,2]{0,1:T(2,128)}, u32[]{:S(2)}) copy-start(s32[128,2]{0,1:T(2,128)} %param.14) | copy-start | bytes 3076
  83.6 3.8 %collective-permute-start.4 = (bf16[8,256,128]{2,1,0:T(8,128)(2,1)S(1)}, bf16[8,256,128]{2,1,0:T(8,128)(2,1)S(1)}, u32[]{:S(2)}, u32[]{:S(2)}) collective-permute-start(bf16[8,256,128]{2,1,0:T(8,128)(2,1)S(1)} %get-tuple-element.36), channel_id=1, source_target_pairs={{0,1},{1,0},{2,3},{3,2},{4,5},{5,4},{6,7},{7,6},{8,9},{9,8},{10,11... | collective-permute-start | bytes 1572872 | tf_op jit(solution)/shard_map/ppermute | solution.py:350
  87.5 28.1 %copy-start.2 = (bf16[128,2048]{1,0:T(8,128)(2,1)S(1)}, bf16[128,2048]{1,0:T(8,128)(2,1)}, u32[]{:S(2)}) copy-start(bf16[128,2048]{1,0:T(8,128)(2,1)} %cot_any.3) | copy-start | bytes 1572868
  87.5 10.8 %collective-permute-start.5 = (bf16[4,256,128]{2,1,0:T(8,128)(2,1)S(1)}, bf16[4,256,128]{2,1,0:T(8,128)(2,1)S(1)}, u32[]{:S(2)}, u32[]{:S(2)}) collective-permute-start(bf16[4,256,128]{2,1,0:T(8,128)(2,1)S(1)} %get-tuple-element.38), channel_id=1, source_target_pairs={{0,2},{2,0},{4,6},{6,4},{8,10},{10,8},{12,14},{14,12},{1,3},{3,1},... | collective-permute-start | bytes 786440 | tf_op jit(solution)/shard_map/ppermute | solution.py:353
  98.4 6.6 %collective-permute-start.6 = (bf16[2,256,128]{2,1,0:T(8,128)(2,1)S(1)}, bf16[2,256,128]{2,1,0:T(8,128)(2,1)S(1)}, u32[]{:S(2)}, u32[]{:S(2)}) collective-permute-start(bf16[2,256,128]{2,1,0:T(8,128)(2,1)S(1)} %get-tuple-element.40), channel_id=1, source_target_pairs={{0,4},{2,6},{4,0},{6,2},{8,12},{10,14},{12,8},{14,10},{1,5},{3,7},... | collective-permute-start | bytes 393224 | tf_op jit(solution)/shard_map/ppermute | solution.py:353
  105.0 14.3 %collective-permute-start.7 = (bf16[1,256,128]{2,1,0:T(8,128)(2,1)S(1)}, bf16[1,256,128]{2,1,0:T(8,128)(2,1)S(1)}, u32[]{:S(2)}, u32[]{:S(2)}) collective-permute-start(bf16[1,256,128]{2,1,0:T(8,128)(2,1)S(1)} %get-tuple-element.42), channel_id=1, source_target_pairs={{0,8},{2,10},{4,12},{6,14},{8,0},{10,2},{12,4},{14,6},{1,9},{3,11}... | collective-permute-start | bytes 196616 | tf_op jit(solution)/shard_map/ppermute | solution.py:353
  115.9 4.3 %collective-permute-start.3 = (bf16[128,128]{1,0:T(8,128)(2,1)S(1)}, bf16[128,128]{1,0:T(8,128)(2,1)S(1)}, u32[]{:S(2)}, u32[]{:S(2)}) collective-permute-start(bf16[128,128]{1,0:T(8,128)(2,1)S(1)} %get-tuple-element.34), channel_id=1, source_target_pairs={{0,1},{1,0},{2,3},{3,2},{4,5},{5,4},{6,7},{7,6},{8,9},{9,8},{10,11... | collective-permute-start | bytes 98312 | tf_op jit(solution)/shard_map/ppermute | solution.py:350
  121.3 24.0 %all-to-all-start.2 = ((bf16[16,136,128]{2,1,0:T(8,128)(2,1)}), bf16[16,136,128]{2,1,0:T(8,128)(2,1)S(1)}, u32[]{:S(2)}, u32[]{:S(2)}) async-start(bf16[16,136,128]{2,1,0:T(8,128)(2,1)} %shard_map.163), calls=%async_computation.2 | async-start | bytes 1114112 | tf_op jit(solution)/shard_map/all_to_all | solution.py:503
  127.2 18.0 %copy-start.7 = (bf16[128,2048]{1,0:T(8,128)(2,1)S(1)}, bf16[128,2048]{1,0:T(8,128)(2,1)}, u32[]{:S(2)}) copy-start(bf16[128,2048]{1,0:T(8,128)(2,1)} %proj_ref.3) | copy-start | bytes 1572868
  127.2 18.0 %copy-start.11 = (f32[128]{0:T(128)S(1)}, f32[128]{0:T(128)}, u32[]{:S(2)}) copy-start(f32[128]{0:T(128)} %param.17) | copy-start | bytes 1540
  132.6 42.9 %collective-permute-start.10 = (bf16[3,2048,128]{2,1,0:T(8,128)(2,1)}, bf16[3,2048,128]{2,1,0:T(8,128)(2,1)S(1)}, u32[]{:S(2)}, u32[]{:S(2)}) collective-permute-start(bf16[3,2048,128]{2,1,0:T(8,128)(2,1)} %get-tuple-element.51), channel_id=1, source_target_pairs={{0,14},{1,3},{2,0},{3,5},{4,2},{5,7},{6,4},{7,9},{8,6},{9,11},{10,... | collective-permute-start | bytes 4718600 | tf_op jit(solution)/shard_map/ppermute | solution.py:360
  146.3 27.4 %all-to-all-start.3 = ((bf16[32,64,128]{2,1,0:T(8,128)(2,1)}), bf16[32,64,128]{2,1,0:T(8,128)(2,1)}, u32[]{:S(2)}, u32[]{:S(2)}) async-start(bf16[32,64,128]{2,1,0:T(8,128)(2,1)} %bitcast.42), calls=%async_computation.3 | async-start | bytes 1048576 | tf_op jit(solution)/shard_map/all_to_all | solution.py:519
  156.4 19.1 %copy-start = (bf16[3,2048,128]{2,1,0:T(8,128)(2,1)S(1)}, bf16[3,2048,128]{2,1,0:T(8,128)(2,1)}, u32[]{:S(2)}) copy-start(bf16[3,2048,128]{2,1,0:T(8,128)(2,1)} %get-tuple-element.50.pre_ref) | copy-start | bytes 4718596
  156.4 5.4 %collective-permute-start.8 = (f32[30,128]{1,0:T(8,128)S(1)}, f32[30,128]{1,0:T(8,128)S(1)}, u32[]{:S(2)}, u32[]{:S(2)}) collective-permute-start(f32[30,128]{1,0:T(8,128)S(1)} %slice.188), channel_id=1, source_target_pairs={{16,0},{32,16},{48,32},{64,48},{80,64},{96,80},{112,96},{128,112},... | collective-permute-start | bytes 46088 | tf_op jit(solution)/shard_map/ppermute | solution.py:523
  (5 other events, 22.0 us)

commit v7 on v6

--- a/solution.py
+++ b/solution.py
@@ -13,7 +13,6 @@
 FIRST = (((0,), (0,)), ((), ()))
 SPAN = 4
 VMEM = pl.BlockSpec(memory_space=pltpu.VMEM)
-ANY = pl.BlockSpec(memory_space=pl.ANY)
 HBM = pl.BlockSpec(memory_space=pltpu.HBM)
 
 
@@ -25,14 +24,14 @@
     return lax.broadcasted_iota(I32, shape, dim)
 
 
-def kernel(body, outs, flops, *args, scratch=(), any_in=(), far=(), far_out=(), limit=60 * 1024):
+def kernel(body, outs, flops, *args, scratch=(), far=(), far_out=(), limit=60 * 1024):
     many = outs if isinstance(outs, tuple) else (outs,)
     specs = [HBM if i in far_out else VMEM for i in range(len(many))]
     return pl.pallas_call(
         body,
         out_shape=outs,
         in_specs=[
-            HBM if i in far else ANY if i in any_in else VMEM for i in range(len(args))
+            HBM if i in far else VMEM for i in range(len(args))
         ],
         out_specs=specs if isinstance(outs, tuple) else specs[0],
         scratch_shapes=list(scratch),
@@ -228,14 +227,16 @@
 def grads_body(got_ref, hid_ref, keep_ref, give_ref):
     pick_x, pick_g = pickers(got_ref.shape[0] // 2)
     places = ((keep_ref, 0), (give_ref, 0), (keep_ref, 1), (give_ref, 1))
-    for j in range(got_ref.shape[1] // 128):
-        at = slice(j * 128, (j + 1) * 128)
-        both = mm(mm(pick_x, got_ref[:, at]).astype(BF), hid_ref[:, :1024], FIRST)
-        down = mm(hid_ref[:, 1024:], mm(pick_g, got_ref[:, at]).astype(BF), FIRST)
-        for q, (ref, to) in enumerate(places):
-            ref[to, 0, at, :] = both[:, q * 256 : q * 256 + 128].astype(BF)
-            ref[to, 1, at, :] = both[:, q * 256 + 128 : (q + 1) * 256].astype(BF)
-            ref[to, 2, at, :] = down[q * 128 : (q + 1) * 128, :].astype(BF)
+    x = mm(pick_x, got_ref[...]).astype(BF)
+    g = mm(pick_g, got_ref[...]).astype(BF)
+    for q, (ref, to) in enumerate(places):
+        both = mm(x, hid_ref[:, q * 256 : (q + 1) * 256], FIRST)
+        ref[to, 0] = both[:, :128].astype(BF)
+        ref[to, 1] = both[:, 128:].astype(BF)
+        down = mm(hid_ref[:, 1024 + q * 128 : 1152 + q * 128], g, FIRST)
+        for j in range(got_ref.shape[1] // 128):
+            at = slice(j * 128, (j + 1) * 128)
+            ref[to, 2, at, :] = down[:, at].astype(BF)
 
 
 def combine_body(table_ref, home_ref, cot_any, own_ref, other_ref, cot_ref, sem):
@@ -279,13 +280,9 @@
         copy.wait()
 
 
-def final_body(
-    all_ref, proj_ref, act_ref, slope_ref, saved_ref, dev_ref, out_any, conv_ref, out_ref, sem
-):
+def proj_body(all_ref, act_ref, out_any, out_ref, sem):
+    copies = []
     tok = act_ref.shape[0]
-    acc = jnp.zeros((tok, tok), F32)
-    sums = jnp.zeros((8, tok), F32)
-    copies = []
     for t in range(all_ref.shape[0]):
         at = slice(t * 128, (t + 1) * 128)
         out_ref[at, :] = mm(all_ref[t, :tok, :], act_ref[...], FIRST).astype(BF)
@@ -295,6 +292,14 @@
                 pltpu.make_async_copy(out_ref.at[at, :], out_any.at[at, :], sem.at[t // 4])
             )
             copies[-1].start()
+    for copy in copies:
+        copy.wait()
+
+
+def norm_body(all_ref, proj_ref, slope_ref, saved_ref, dev_ref, conv_ref):
+    tok = slope_ref.shape[0]
+    acc = jnp.zeros((tok, tok), F32)
+    sums = jnp.zeros((8, tok), F32)
     for t in range(0, all_ref.shape[0], 2):
         pair = [all_ref[t + i, :tok, :] for i in range(2)]
         acc = acc + mm(
@@ -310,8 +315,10 @@
         means.append(jnp.broadcast_to(total, (tok, tok)).T)
     dev = jnp.broadcast_to(dev_ref[...], (tok, tok)).T
     conv_ref[...] = dev * (grad - means[0] - saved_ref[...].astype(F32) * means[1])
-    for copy in copies:
-        copy.wait()
+
+
+def reduce_body(parts_ref, out_ref):
+    out_ref[...] = jnp.sum(parts_ref[...].astype(F32), axis=0)
 
 
 def sumout_body(keep_ref, given_ref, pre_ref, pass_ref):
@@ -428,8 +435,8 @@
         by_c,
         by_y,
         by_yc,
-        any_in=(1, 2, 3, 4),
-        limit=24 << 10,
+        far=(1, 2, 3, 4),
+        limit=52 << 10,
         scratch=(
             pltpu.VMEM((slots, width), BF),
             pltpu.VMEM((slots, width), BF),
@@ -502,23 +509,31 @@
     )
     mix_all = lax.all_to_all(mix, ("y", "c"), 0, 0, tiled=True)
 
-    proj, conv = kernel(
-        final_body,
-        (shape(width, 128), shape(tok, 128, kind=F32)),
-        2000000000,
+    proj = kernel(
+        proj_body,
+        shape(width, 128),
+        300000000,
+        mix_all,
+        act_conv,
+        far_out=(0,),
+        limit=12 << 10,
+        scratch=(pltpu.VMEM((width, 128), BF), pltpu.SemaphoreType.DMA((ny // 2,))),
+    )
+    proj = lax.all_to_all(proj.reshape(experts, -1, 128), sp, 0, 0, tiled=True)
+    grad_proj = kernel(
+        reduce_body, shape(width // experts, 128, kind=F32), 1000000, proj, limit=12 << 10
+    )
+    conv = kernel(
+        norm_body,
+        shape(tok, 128, kind=F32),
+        500000000,
         mix_all,
         proj_weight,
-        act_conv,
         slope,
         saved_normalized,
         inverse_deviation[None, :],
-        far_out=(0,),
         limit=16 << 10,
-        scratch=(pltpu.VMEM((width, 128), BF), pltpu.SemaphoreType.DMA((ny // 2,))),
-    )
-    proj = lax.all_to_all(proj.reshape(experts, -1, 128), sp, 0, 0, tiled=True)
-    grad_proj = jnp.sum(proj.astype(F32), axis=0)
-
+    )
     reach = taps.shape[0] - 1
     beyond = lax.ppermute(conv[:reach], sp, [(i + 1, i) for i in range(experts - 1)])
     extended = jnp.concatenate([conv, beyond], axis=0)

time: 178 us -> 174 us (0.978)
  local copies, waits for them, and re-layouts: 3.75 us -> 0.81 us
    unnamed x29 -> x22, local copies, waits for them, and re-layouts: 3.72 us -> 0.78 us
    pallas_call x11 -> x13, Pallas kernels: 14.6 us -> 17.2 us  [kernel(): pl.pallas_call(body, out_shape=outs, in_specs=[HBM if i in far else VMEM...]
    pallas_call x1, Pallas kernels: 8.4 us -> 6.18 us  [shards(): pl.pallas_call(grads_body, grid=(4,), out_shape=(packed, packed), in_spec...]
  transfers between devices with their start and end apart: 15 -> 15, of which waited for: 9 -> 9; matrix products, arithmetic and copies ran while one was open for 1% -> 0% of each run, Pallas kernels for 5% -> 6%
where the time goes in v7:
time: 174 us; the launch traced here: 173 us
  starting transfers between devices  87.3 us (50%)
  waiting for transfers between devices  54.7 us (31%)
  Pallas kernels  28.6 us (16%)
    ppermute x5, starting transfers between devices, flip_c(): return lax.ppermute(value, 'c', [(0, 1), (1, 0)])  18.8 us
    pallas_call x13, Pallas kernels, kernel(): pl.pallas_call(body, out_shape=outs, in_specs=[HBM if i in far else VMEM...  17.2 us
    ppermute x3, starting transfers between devices, flip_y(): return lax.ppermute(value, 'y', [(i, i ^ 1 << bit) for i in range(ny)])  16.4 us
    all_to_all x1, waiting for transfers between devices, shards(): lax.all_to_all(sent.reshape(experts, 2 * SPAN, width), sp, 0, 0, tiled=True)  14.2 us
    all_to_all x1, starting transfers between devices, shards(): lax.all_to_all(sent.reshape(experts, 2 * SPAN, width), sp, 0, 0, tiled=True)  12.9 us
    all_to_all x1, starting transfers between devices, shards(): lax.all_to_all(back.reshape(experts * ny, 2 * SPAN, 128), ('z', 'x', 'y')...  12.5 us
    ppermute x3, waiting for transfers between devices, flip_y(): return lax.ppermute(value, 'y', [(i, i ^ 1 << bit) for i in range(ny)])  11.2 us
    all_to_all x1, waiting for transfers between devices, shards(): proj = lax.all_to_all(proj.reshape(experts, -1, 128), sp, 0, 0, tiled=True)  10.9 us
  transfers between devices with their start and end apart: 15, of which 9 were waited for; matrix products, arithmetic and copies ran while one was open for 0% of the time, Pallas kernels for 6%

profile of v7, /device:TPU:1, one launch (start us, length us, event | category | flops | bytes accessed | tf_op | source)
XLA Modules:
  0.0 173.3 jit_solution(17726469052661188037)
XLA Ops:
  0.6 3.9 %shard_map.156 = (bf16[256,2048]{1,0:T(8,128)(2,1)}, bf16[3,2048,128]{2,1,0:T(8,128)(2,1)}) custom-call(s32[2,128]{1,0:T(2,128)} %bitcast.80, f32[2,128]{1,0:T(2,128)} %bitcast.91, bf16[128,2048]{1,0:T(8,128)(2,1)} %mix_any.1, bf16[128,2048]{1,0:T(8,128)(2,1)} %cot_any.3, bf16[2048,128]{1,0:T(8,128)(2,1)} %bitcast.85, bf16[2048,128]{1,0:T(8,128)(2,1)} %bitcast.86, ...), custom_call_target="tpu_custom_call" | custom-call | flops 2000000000 | bytes 1048576 | tf_op jit(solution)/shard_map/pallas_call | solution.py:30
  4.6 6.0 %collective-permute-start.1 = (bf16[3,2048,128]{2,1,0:T(8,128)(2,1)}, bf16[3,2048,128]{2,1,0:T(8,128)(2,1)}, u32[]{:S(2)}, u32[]{:S(2)}) collective-permute-start(bf16[3,2048,128]{2,1,0:T(8,128)(2,1)} %get-tuple-element.29.w0), channel_id=1, source_target_pairs={{0,2},{1,15},{2,4},{3,1},{4,6},{5,3},{6,8},{7,5},{8,10},{9,7},{10,... | collective-permute-start | bytes 4718600 | tf_op jit(solution)/shard_map/ppermute | solution.py:367
  10.7 12.9 %all-to-all-start = ((bf16[32,8,2048]{2,1,0:T(8,128)(2,1)}), bf16[32,8,2048]{2,1,0:T(8,128)(2,1)S(1)}, u32[]{:S(2)}, u32[]{:S(2)}) async-start(bf16[32,8,2048]{2,1,0:T(8,128)(2,1)} %bitcast.84), calls=%async_computation | async-start | bytes 2097152 | tf_op jit(solution)/shard_map/all_to_all | solution.py:397
  25.5 2.8 %collective-permute-done.1.w2 = bf16[3,2048,128]{2,1,0:T(8,128)(2,1)} collective-permute-done((bf16[3,2048,128]{2,1,0:T(8,128)(2,1)}, bf16[3,2048,128]{2,1,0:T(8,128)(2,1)}, u32[]{:S(2)}, u32[]{:S(2)}) %collective-permute-start.1) | collective-permute-done | bytes 1572896 | tf_op jit(solution)/shard_map/ppermute | solution.py:367
  28.3 9.0 %collective-permute-start.2 = (bf16[3,2048,128]{2,1,0:T(8,128)(2,1)}, bf16[3,2048,128]{2,1,0:T(8,128)(2,1)}, u32[]{:S(2)}, u32[]{:S(2)}) collective-permute-start(bf16[3,2048,128]{2,1,0:T(8,128)(2,1)} %collective-permute-done.1.w2), channel_id=1, source_target_pairs={{0,1},{1,0},{2,3},{3,2},{4,5},{5,4},{6,7},{7,6},{8,9},{9,8},{10,11... | collective-permute-start | bytes 4718600 | tf_op jit(solution)/shard_map/ppermute | solution.py:357
  37.3 14.2 %all-to-all-done = bf16[32,8,2048]{2,1,0:T(8,128)(2,1)S(1)} async-done(((bf16[32,8,2048]{2,1,0:T(8,128)(2,1)}), bf16[32,8,2048]{2,1,0:T(8,128)(2,1)S(1)}, u32[]{:S(2)}, u32[]{:S(2)}) %all-to-all-start) | async-done | bytes 1048608 | tf_op jit(solution)/shard_map/all_to_all | solution.py:397
  51.5 5.8 %shard_map.157 = (bf16[128,1536]{1,0:T(8,128)(2,1)S(1)}, bf16[16,128,128]{2,1,0:T(8,128)(2,1)}) custom-call(bf16[256,2048]{1,0:T(8,128)(2,1)S(1)} %bitcast.78, bf16[3,2048,128]{2,1,0:T(8,128)(2,1)} %get-tuple-element.29.w0, bf16[3,2048,128]{2,1,0:T(8,128)(2,1)} %collective-permute-done.w1, bf16[3,2048,128]{2,1,0:T(8,128)(2,1)} %collective-permute-done.1.w2, ...), custom_call_target="tpu_custom_call" | custom-call | flops 4000000000 | bytes 1048576 | tf_op jit(solution)/shard_map/pallas_call | solution.py:30
  58.1 6.2 %shard_map.167 = (bf16[2,3,2048,128]{3,2,1,0:T(8,128)(2,1)}, bf16[2,3,2048,128]{3,2,1,0:T(8,128)(2,1)}) custom-call(bf16[256,2048]{1,0:T(8,128)(2,1)} %bitcast.79, bf16[128,1536]{1,0:T(8,128)(2,1)} %copy-done.8), custom_call_target="tpu_custom_call" | custom-call | flops 8000000000 | bytes 7340032 | tf_op jit(solution)/shard_map/pallas_call | solution.py:454
  64.3 2.3 %collective-permute-start.9 = (bf16[2,3,2048,128]{3,2,1,0:T(8,128)(2,1)}, bf16[2,3,2048,128]{3,2,1,0:T(8,128)(2,1)}, u32[]{:S(2)}, u32[]{:S(2)}) collective-permute-start(bf16[2,3,2048,128]{3,2,1,0:T(8,128)(2,1)} %get-tuple-element.45), channel_id=1, source_target_pairs={{0,1},{1,0},{2,3},{3,2},{4,5},{5,4},{6,7},{7,6},{8,9},{9,8},{10,11... | collective-permute-start | bytes 9437192 | tf_op jit(solution)/shard_map/ppermute | solution.py:357
  66.6 12.5 %all-to-all-start.1 = ((bf16[256,8,128]{2,1,0:T(8,128)(2,1)}), bf16[256,8,128]{2,1,0:T(8,128)(2,1)S(1)}, u32[]{:S(2)}, u32[]{:S(2)}) async-start(bf16[256,8,128]{2,1,0:T(8,128)(2,1)} %bitcast.8), calls=%async_computation.1 | async-start | bytes 1048576 | tf_op jit(solution)/shard_map/all_to_all | solution.py:448
  79.9 2.2 %collective-permute-start.4 = (bf16[8,256,128]{2,1,0:T(8,128)(2,1)S(1)}, bf16[8,256,128]{2,1,0:T(8,128)(2,1)S(1)}, u32[]{:S(2)}, u32[]{:S(2)}) collective-permute-start(bf16[8,256,128]{2,1,0:T(8,128)(2,1)S(1)} %get-tuple-element.34), channel_id=1, source_target_pairs={{0,1},{1,0},{2,3},{3,2},{4,5},{5,4},{6,7},{7,6},{8,9},{9,8},{10,11... | collective-permute-start | bytes 1572872 | tf_op jit(solution)/shard_map/ppermute | solution.py:357
  85.9 8.8 %collective-permute-done.5.given_ref = bf16[4,256,128]{2,1,0:T(8,128)(2,1)S(1)} collective-permute-done((bf16[4,256,128]{2,1,0:T(8,128)(2,1)S(1)}, bf16[4,256,128]{2,1,0:T(8,128)(2,1)S(1)}, u32[]{:S(2)}, u32[]{:S(2)}) %collective-permute-start.5) | collective-permute-done | bytes 262176 | tf_op jit(solution)/shard_map/ppermute | solution.py:360
  94.7 4.2 %collective-permute-start.6 = (bf16[2,256,128]{2,1,0:T(8,128)(2,1)S(1)}, bf16[2,256,128]{2,1,0:T(8,128)(2,1)S(1)}, u32[]{:S(2)}, u32[]{:S(2)}) collective-permute-start(bf16[2,256,128]{2,1,0:T(8,128)(2,1)S(1)} %get-tuple-element.38), channel_id=1, source_target_pairs={{0,4},{2,6},{4,0},{6,2},{8,12},{10,14},{12,8},{14,10},{1,5},{3,7},... | collective-permute-start | bytes 393224 | tf_op jit(solution)/shard_map/ppermute | solution.py:360
  98.9 2.4 %collective-permute-done.6.given_ref = bf16[2,256,128]{2,1,0:T(8,128)(2,1)S(1)} collective-permute-done((bf16[2,256,128]{2,1,0:T(8,128)(2,1)S(1)}, bf16[2,256,128]{2,1,0:T(8,128)(2,1)S(1)}, u32[]{:S(2)}, u32[]{:S(2)}) %collective-permute-start.6) | collective-permute-done | bytes 131104 | tf_op jit(solution)/shard_map/ppermute | solution.py:360
  101.3 10.1 %collective-permute-start.7 = (bf16[1,256,128]{2,1,0:T(8,128)(2,1)S(1)}, bf16[1,256,128]{2,1,0:T(8,128)(2,1)S(1)}, u32[]{:S(2)}, u32[]{:S(2)}) collective-permute-start(bf16[1,256,128]{2,1,0:T(8,128)(2,1)S(1)} %get-tuple-element.40), channel_id=1, source_target_pairs={{0,8},{2,10},{4,12},{6,14},{8,0},{10,2},{12,4},{14,6},{1,9},{3,11}... | collective-permute-start | bytes 196616 | tf_op jit(solution)/shard_map/ppermute | solution.py:360
  112.2 3.4 %collective-permute-start.3 = (bf16[128,128]{1,0:T(8,128)(2,1)S(1)}, bf16[128,128]{1,0:T(8,128)(2,1)S(1)}, u32[]{:S(2)}, u32[]{:S(2)}) collective-permute-start(bf16[128,128]{1,0:T(8,128)(2,1)S(1)} %get-tuple-element.32), channel_id=1, source_target_pairs={{0,1},{1,0},{2,3},{3,2},{4,5},{5,4},{6,7},{7,6},{8,9},{9,8},{10,11... | collective-permute-start | bytes 98312 | tf_op jit(solution)/shard_map/ppermute | solution.py:357
  117.6 5.9 %all-to-all-start.2 = ((bf16[16,136,128]{2,1,0:T(8,128)(2,1)}), bf16[16,136,128]{2,1,0:T(8,128)(2,1)S(1)}, u32[]{:S(2)}, u32[]{:S(2)}) async-start(bf16[16,136,128]{2,1,0:T(8,128)(2,1)} %shard_map.163), calls=%async_computation.2 | async-start | bytes 1114112 | tf_op jit(solution)/shard_map/all_to_all | solution.py:510
  123.5 5.3 %shard_map.168 = (bf16[3,2048,128]{2,1,0:T(8,128)(2,1)}, bf16[3,2048,128]{2,1,0:T(8,128)(2,1)}) custom-call(bf16[2,3,2048,128]{3,2,1,0:T(8,128)(2,1)} %get-tuple-element.44.keep_ref, bf16[2,3,2048,128]{3,2,1,0:T(8,128)(2,1)} %collective-permute-done.9.given_ref), custom_call_target="tpu_custom_call" | custom-call | flops 1000000 | bytes 9437184 | tf_op jit(solution)/shard_map/pallas_call | solution.py:468
  128.8 3.4 %collective-permute-start.10 = (bf16[3,2048,128]{2,1,0:T(8,128)(2,1)}, bf16[3,2048,128]{2,1,0:T(8,128)(2,1)}, u32[]{:S(2)}, u32[]{:S(2)}) collective-permute-start(bf16[3,2048,128]{2,1,0:T(8,128)(2,1)} %get-tuple-element.47), channel_id=1, source_target_pairs={{0,14},{1,3},{2,0},{3,5},{4,2},{5,7},{6,4},{7,9},{8,6},{9,11},{10,... | collective-permute-start | bytes 4718600 | tf_op jit(solution)/shard_map/ppermute | solution.py:367
  132.2 9.4 %all-to-all-done.2.all_ref = bf16[16,136,128]{2,1,0:T(8,128)(2,1)S(1)} async-done(((bf16[16,136,128]{2,1,0:T(8,128)(2,1)}), bf16[16,136,128]{2,1,0:T(8,128)(2,1)S(1)}, u32[]{:S(2)}, u32[]{:S(2)}) %all-to-all-start.2) | async-done | bytes 557088 | tf_op jit(solution)/shard_map/all_to_all | solution.py:510
  142.6 9.9 %all-to-all-start.3 = ((bf16[32,64,128]{2,1,0:T(8,128)(2,1)}), bf16[32,64,128]{2,1,0:T(8,128)(2,1)S(1)}, u32[]{:S(2)}, u32[]{:S(2)}) async-start(bf16[32,64,128]{2,1,0:T(8,128)(2,1)} %bitcast.42), calls=%async_computation.3 | async-start | bytes 1048576 | tf_op jit(solution)/shard_map/all_to_all | solution.py:522
  154.3 3.9 %collective-permute-done.8 = f32[30,128]{1,0:T(8,128)S(1)} collective-permute-done((f32[30,128]{1,0:T(8,128)S(1)}, f32[30,128]{1,0:T(8,128)S(1)}, u32[]{:S(2)}, u32[]{:S(2)}) %collective-permute-start.8) | collective-permute-done | bytes 15392 | tf_op jit(solution)/shard_map/ppermute | solution.py:538
  159.1 10.9 %all-to-all-done.3.parts_ref = bf16[32,64,128]{2,1,0:T(8,128)(2,1)S(1)} async-done(((bf16[32,64,128]{2,1,0:T(8,128)(2,1)}), bf16[32,64,128]{2,1,0:T(8,128)(2,1)S(1)}, u32[]{:S(2)}, u32[]{:S(2)}) %all-to-all-start.3) | async-done | bytes 524320 | tf_op jit(solution)/shard_map/all_to_all | solution.py:522
  170.6 2.7 %shard_map.169 = (bf16[2048,128]{1,0:T(8,128)(2,1)}, bf16[2048,128]{1,0:T(8,128)(2,1)}, bf16[128,2048]{1,0:T(8,128)(2,1)}) custom-call(bf16[3,2048,128]{2,1,0:T(8,128)(2,1)S(1)} %copy-done, bf16[3,2048,128]{2,1,0:T(8,128)(2,1)} %collective-permute-done.10.passed_ref), custom_call_target="tpu_custom_call" | custom-call | flops 1000000 | bytes 1048576 | tf_op jit(solution)/shard_map/pallas_call | solution.py:30
  (47 shorter events, 14.2 us)
Async XLA Ops:
  4.6 19.0 %copy-start.10 = (bf16[3,2048,128]{2,1,0:T(8,128)(2,1)S(1)}, bf16[3,2048,128]{2,1,0:T(8,128)(2,1)}, u32[]{:S(2)}) copy-start(bf16[3,2048,128]{2,1,0:T(8,128)(2,1)} %get-tuple-element.29.w0) | copy-start | bytes 4718596
  4.6 23.7 %collective-permute-start.1 = (bf16[3,2048,128]{2,1,0:T(8,128)(2,1)}, bf16[3,2048,128]{2,1,0:T(8,128)(2,1)}, u32[]{:S(2)}, u32[]{:S(2)}) collective-permute-start(bf16[3,2048,128]{2,1,0:T(8,128)(2,1)} %get-tuple-element.29.w0), channel_id=1, source_target_pairs={{0,2},{1,15},{2,4},{3,1},{4,6},{5,3},{6,8},{7,5},{8,10},{9,7},{10,... | collective-permute-start | bytes 4718600 | tf_op jit(solution)/shard_map/ppermute | solution.py:367
  10.7 40.9 %all-to-all-start = ((bf16[32,8,2048]{2,1,0:T(8,128)(2,1)}), bf16[32,8,2048]{2,1,0:T(8,128)(2,1)S(1)}, u32[]{:S(2)}, u32[]{:S(2)}) async-start(bf16[32,8,2048]{2,1,0:T(8,128)(2,1)} %bitcast.84), calls=%async_computation | async-start | bytes 2097152 | tf_op jit(solution)/shard_map/all_to_all | solution.py:397
  23.6 13.7 %collective-permute-start = (bf16[3,2048,128]{2,1,0:T(8,128)(2,1)S(1)}, bf16[3,2048,128]{2,1,0:T(8,128)(2,1)}, u32[]{:S(2)}, u32[]{:S(2)}) collective-permute-start(bf16[3,2048,128]{2,1,0:T(8,128)(2,1)S(1)} %copy-done.10), channel_id=1, source_target_pairs={{0,1},{1,0},{2,3},{3,2},{4,5},{5,4},{6,7},{7,6},{8,9},{9,8},{10,11... | collective-permute-start | bytes 4718600 | tf_op jit(solution)/shard_map/ppermute | solution.py:357
  28.3 23.2 %collective-permute-start.2 = (bf16[3,2048,128]{2,1,0:T(8,128)(2,1)}, bf16[3,2048,128]{2,1,0:T(8,128)(2,1)}, u32[]{:S(2)}, u32[]{:S(2)}) collective-permute-start(bf16[3,2048,128]{2,1,0:T(8,128)(2,1)} %collective-permute-done.1.w2), channel_id=1, source_target_pairs={{0,1},{1,0},{2,3},{3,2},{4,5},{5,4},{6,7},{7,6},{8,9},{9,8},{10,11... | collective-permute-start | bytes 4718600 | tf_op jit(solution)/shard_map/ppermute | solution.py:357
  58.1 21.0 %copy-start.3 = (bf16[128,2048]{1,0:T(8,128)(2,1)S(1)}, bf16[128,2048]{1,0:T(8,128)(2,1)}, u32[]{:S(2)}) copy-start(bf16[128,2048]{1,0:T(8,128)(2,1)} %proj_ref.3) | copy-start | bytes 1572868
  58.1 21.0 %copy-start.4 = (bf16[128,128]{1,0:T(8,128)(2,1)S(1)}, bf16[128,128]{1,0:T(8,128)(2,1)}, u32[]{:S(2)}) copy-start(bf16[128,128]{1,0:T(8,128)(2,1)} %saved_ref.3) | copy-start | bytes 98308
  58.1 21.0 %copy-start.6 = (f32[128]{0:T(128)S(1)}, f32[128]{0:T(128)}, u32[]{:S(2)}) copy-start(f32[128]{0:T(128)} %param.18) | copy-start | bytes 1540
  64.3 59.2 %collective-permute-start.9 = (bf16[2,3,2048,128]{3,2,1,0:T(8,128)(2,1)}, bf16[2,3,2048,128]{3,2,1,0:T(8,128)(2,1)}, u32[]{:S(2)}, u32[]{:S(2)}) collective-permute-start(bf16[2,3,2048,128]{3,2,1,0:T(8,128)(2,1)} %get-tuple-element.45), channel_id=1, source_target_pairs={{0,1},{1,0},{2,3},{3,2},{4,5},{5,4},{6,7},{7,6},{8,9},{9,8},{10,11... | collective-permute-start | bytes 9437192 | tf_op jit(solution)/shard_map/ppermute | solution.py:357
  66.6 45.3 %all-to-all-start.1 = ((bf16[256,8,128]{2,1,0:T(8,128)(2,1)}), bf16[256,8,128]{2,1,0:T(8,128)(2,1)S(1)}, u32[]{:S(2)}, u32[]{:S(2)}) async-start(bf16[256,8,128]{2,1,0:T(8,128)(2,1)} %bitcast.8), calls=%async_computation.1 | async-start | bytes 1048576 | tf_op jit(solution)/shard_map/all_to_all | solution.py:448
  79.9 31.6 %copy-start.5 = (s32[128,2]{0,1:T(2,128)S(1)}, s32[128,2]{0,1:T(2,128)}, u32[]{:S(2)}) copy-start(s32[128,2]{0,1:T(2,128)} %param.14) | copy-start | bytes 3076
  79.9 3.8 %collective-permute-start.4 = (bf16[8,256,128]{2,1,0:T(8,128)(2,1)S(1)}, bf16[8,256,128]{2,1,0:T(8,128)(2,1)S(1)}, u32[]{:S(2)}, u32[]{:S(2)}) collective-permute-start(bf16[8,256,128]{2,1,0:T(8,128)(2,1)S(1)} %get-tuple-element.34), channel_id=1, source_target_pairs={{0,1},{1,0},{2,3},{3,2},{4,5},{5,4},{6,7},{7,6},{8,9},{9,8},{10,11... | collective-permute-start | bytes 1572872 | tf_op jit(solution)/shard_map/ppermute | solution.py:357
  83.8 28.1 %copy-start.2 = (bf16[128,2048]{1,0:T(8,128)(2,1)S(1)}, bf16[128,2048]{1,0:T(8,128)(2,1)}, u32[]{:S(2)}) copy-start(bf16[128,2048]{1,0:T(8,128)(2,1)} %cot_any.3) | copy-start | bytes 1572868
  83.8 10.8 %collective-permute-start.5 = (bf16[4,256,128]{2,1,0:T(8,128)(2,1)S(1)}, bf16[4,256,128]{2,1,0:T(8,128)(2,1)S(1)}, u32[]{:S(2)}, u32[]{:S(2)}) collective-permute-start(bf16[4,256,128]{2,1,0:T(8,128)(2,1)S(1)} %get-tuple-element.36), channel_id=1, source_target_pairs={{0,2},{2,0},{4,6},{6,4},{8,10},{10,8},{12,14},{14,12},{1,3},{3,1},... | collective-permute-start | bytes 786440 | tf_op jit(solution)/shard_map/ppermute | solution.py:360
  94.7 6.6 %collective-permute-start.6 = (bf16[2,256,128]{2,1,0:T(8,128)(2,1)S(1)}, bf16[2,256,128]{2,1,0:T(8,128)(2,1)S(1)}, u32[]{:S(2)}, u32[]{:S(2)}) collective-permute-start(bf16[2,256,128]{2,1,0:T(8,128)(2,1)S(1)} %get-tuple-element.38), channel_id=1, source_target_pairs={{0,4},{2,6},{4,0},{6,2},{8,12},{10,14},{12,8},{14,10},{1,5},{3,7},... | collective-permute-start | bytes 393224 | tf_op jit(solution)/shard_map/ppermute | solution.py:360
  101.3 14.3 %collective-permute-start.7 = (bf16[1,256,128]{2,1,0:T(8,128)(2,1)S(1)}, bf16[1,256,128]{2,1,0:T(8,128)(2,1)S(1)}, u32[]{:S(2)}, u32[]{:S(2)}) collective-permute-start(bf16[1,256,128]{2,1,0:T(8,128)(2,1)S(1)} %get-tuple-element.40), channel_id=1, source_target_pairs={{0,8},{2,10},{4,12},{6,14},{8,0},{10,2},{12,4},{14,6},{1,9},{3,11}... | collective-permute-start | bytes 196616 | tf_op jit(solution)/shard_map/ppermute | solution.py:360
  112.2 4.3 %collective-permute-start.3 = (bf16[128,128]{1,0:T(8,128)(2,1)S(1)}, bf16[128,128]{1,0:T(8,128)(2,1)S(1)}, u32[]{:S(2)}, u32[]{:S(2)}) collective-permute-start(bf16[128,128]{1,0:T(8,128)(2,1)S(1)} %get-tuple-element.32), channel_id=1, source_target_pairs={{0,1},{1,0},{2,3},{3,2},{4,5},{5,4},{6,7},{7,6},{8,9},{9,8},{10,11... | collective-permute-start | bytes 98312 | tf_op jit(solution)/shard_map/ppermute | solution.py:357
  117.6 24.0 %all-to-all-start.2 = ((bf16[16,136,128]{2,1,0:T(8,128)(2,1)}), bf16[16,136,128]{2,1,0:T(8,128)(2,1)S(1)}, u32[]{:S(2)}, u32[]{:S(2)}) async-start(bf16[16,136,128]{2,1,0:T(8,128)(2,1)} %shard_map.163), calls=%async_computation.2 | async-start | bytes 1114112 | tf_op jit(solution)/shard_map/all_to_all | solution.py:510
  128.8 23.7 %copy-start.9 = (f32[31,128]{1,0:T(8,128)S(1)}, f32[31,128]{1,0:T(8,128)}, u32[]{:S(2)}) copy-start(f32[31,128]{1,0:T(8,128)} %param.19) | copy-start | bytes 47620
  128.8 23.7 %copy-start.7 = (f32[128]{0:T(128)S(1)}, f32[128]{0:T(128)}, u32[]{:S(2)}) copy-start(f32[128]{0:T(128)} %param.17) | copy-start | bytes 1540
  128.8 41.8 %collective-permute-start.10 = (bf16[3,2048,128]{2,1,0:T(8,128)(2,1)}, bf16[3,2048,128]{2,1,0:T(8,128)(2,1)}, u32[]{:S(2)}, u32[]{:S(2)}) collective-permute-start(bf16[3,2048,128]{2,1,0:T(8,128)(2,1)} %get-tuple-element.47), channel_id=1, source_target_pairs={{0,14},{1,3},{2,0},{3,5},{4,2},{5,7},{6,4},{7,9},{8,6},{9,11},{10,... | collective-permute-start | bytes 4718600 | tf_op jit(solution)/shard_map/ppermute | solution.py:367
  142.6 27.3 %all-to-all-start.3 = ((bf16[32,64,128]{2,1,0:T(8,128)(2,1)}), bf16[32,64,128]{2,1,0:T(8,128)(2,1)S(1)}, u32[]{:S(2)}, u32[]{:S(2)}) async-start(bf16[32,64,128]{2,1,0:T(8,128)(2,1)} %bitcast.42), calls=%async_computation.3 | async-start | bytes 1048576 | tf_op jit(solution)/shard_map/all_to_all | solution.py:522
  152.5 18.1 %copy-start = (bf16[3,2048,128]{2,1,0:T(8,128)(2,1)S(1)}, bf16[3,2048,128]{2,1,0:T(8,128)(2,1)}, u32[]{:S(2)}) copy-start(bf16[3,2048,128]{2,1,0:T(8,128)(2,1)} %get-tuple-element.46.pre_ref) | copy-start | bytes 4718596
  152.9 5.4 %collective-permute-start.8 = (f32[30,128]{1,0:T(8,128)S(1)}, f32[30,128]{1,0:T(8,128)S(1)}, u32[]{:S(2)}, u32[]{:S(2)}) collective-permute-start(f32[30,128]{1,0:T(8,128)S(1)} %slice.248), channel_id=1, source_target_pairs={{16,0},{32,16},{48,32},{64,48},{80,64},{96,80},{112,96},{128,112},... | collective-permute-start | bytes 46088 | tf_op jit(solution)/shard_map/ppermute | solution.py:538
  (2 other events, 6.6 us)
